TPU v7x, 256 devices: a whole 4x4x8 slice. The times are simulated.
256 devices in a mesh: sp: 64 (over z, y, core), tp: 4 (over x).
Axes of the slice: x: 4, y: 4, z: 8, core: 2. Of those that a mesh axis runs over, the one named last changes fastest.
Arguments:
- mixer_out: bfloat16 [8192, 2048], P('sp'), may hold values from -6 to 6
- conv_out: bfloat16 [8192, 2048], P('sp', 'tp'), may hold values from -350 to 350
- out_cot: bfloat16 [8192, 2048], P('sp'), may hold values from -16 to 16
- routes: int32 [8192, 2], P('sp'), may hold values from 0 to 63, all different within a row; in each aligned block of 128 rows (0 to 127, 128 to 255, ...) at most 8 rows name the same one
- route_weight: float32 [8192, 2], P('sp'), may hold values from 0.3 to 2.5
- gate_weight: bfloat16 [64, 2048, 1024], P('sp', None, 'tp'), may hold values from -0.125 to 0.125
- up_weight: bfloat16 [64, 2048, 1024], P('sp', None, 'tp'), may hold values from -0.125 to 0.125
- down_weight: bfloat16 [64, 1024, 2048], P('sp', 'tp'), may hold values from -0.1875 to 0.1875
- out_weight: bfloat16 [2048, 2048], P('tp'), may hold values from -0.125 to 0.125
- norm_gain: float32 [2048], P('tp'), may hold values from 0.1 to 1.9
- conv_taps: float32 [31, 2048], P(None, 'tp'), may hold values from -1 to 1
Outputs:
- gate_grad: bfloat16 [64, 2048, 1024], P('sp', None, 'tp')
- up_grad: bfloat16 [64, 2048, 1024], P('sp', None, 'tp')
- down_grad: bfloat16 [64, 1024, 2048], P('sp', 'tp')
- proj_grad: float32 [2048, 2048], P('sp', 'tp')
- gated_grad: float32 [8192, 2048], P('sp', 'tp')
Inputs may be any that keep to these rules, and one draw needn't show every extreme that they name: `routes`: each row names 2 different experts. Among the rows of one device no expert is named by more than 8 rows, and in every draw some expert is named by exactly 8 rows of some device.
All inputs are finite; a program needn't handle non-finite values.
Results may differ from a plain program's by a relative error of at most 0.0095.
Values may be sent and summed in bfloat16 or wider, within the bound.
No kernel may reach another device: no remote copies, remote signals or barrier semaphores. Data moves between devices by JAX's collectives and lax.ppermute only.
A program may use at most 64 MiB of HBM per device.

v0:
```python
import jax
import jax.numpy as jnp
from jax import lax
from jax.experimental import pallas as pl
from jax.experimental.pallas import tpu as pltpu
from jax.sharding import Mesh
from jax.sharding import PartitionSpec as P


norm_epsilon = 1e-05
SP = ("z", "y", "core")
f32 = jnp.float32
bf16 = jnp.bfloat16
VM = pl.BlockSpec(memory_space=pltpu.VMEM)
SM = pl.BlockSpec(memory_space=pltpu.SMEM)


PARAMS = pltpu.CompilerParams(vmem_limit_bytes=20 * 2**20)


def cost(flops, moved):
    return pl.CostEstimate(flops=flops, bytes_accessed=moved, transcendentals=0)


def dot(a, b, ca, cb):
    return lax.dot_general(a, b, (((ca,), (cb,)), ((), ())), preferred_element_type=f32)


def send_kernel(tp_ref, routes_ref, weight_ref, x_ref, cot_ref, send_ref, sel_ref):
    tokens = routes_ref.shape[1]
    slots = sel_ref.shape[0]
    experts = send_ref.shape[0]
    capacity = slots // experts
    expert_row = lax.broadcasted_iota(jnp.int32, (experts, tokens), 0)
    earlier = (
        lax.broadcasted_iota(jnp.int32, (tokens, tokens), 0)
        < lax.broadcasted_iota(jnp.int32, (tokens, tokens), 1)
    ).astype(bf16)
    slot_row = lax.broadcasted_iota(jnp.int32, (slots, tokens), 0)
    total = jnp.zeros((experts, 1), f32)
    picks = []
    for k in range(routes_ref.shape[0]):
        named = routes_ref[k : k + 1, :]
        hot = (expert_row == named).astype(f32)
        before = dot(hot.astype(bf16), earlier, 1, 0) + total
        total = total + jnp.sum(hot, axis=1, keepdims=True)
        within = jnp.sum(hot * before, axis=0, keepdims=True).astype(jnp.int32)
        picks.append((slot_row == named * capacity + within).astype(bf16))
    both = picks[0] + picks[1]
    sel_ref[...] = both
    shape = (experts, capacity, x_ref.shape[1])
    send_ref[:, :, : shape[2]] = dot(both, x_ref[...], 1, 0).astype(bf16).reshape(shape)
    cot = cot_ref[...].astype(f32)
    weight = jnp.broadcast_to(weight_ref[0:1, :], (8, tokens)).T, jnp.broadcast_to(
        weight_ref[1:2, :], (8, tokens)
    ).T
    scaled = [(weight[k][:, 0:1] * cot).astype(bf16) for k in range(2)]
    out = dot(picks[0], scaled[0], 1, 0) + dot(picks[1], scaled[1], 1, 0)
    send_ref[:, :, shape[2] :] = out.astype(bf16).reshape(shape)


def send_rows(tp, routes, route_weight, mixer_out, out_cot, experts, capacity, quarter):
    tokens = out_cot.shape[0]
    column = pl.BlockSpec((tokens, quarter), lambda i, t: (0, t[0]))
    whole = lambda shape: pl.BlockSpec(shape, lambda i, t: (0,) * len(shape))
    sent = jax.ShapeDtypeStruct((experts, capacity, 2 * quarter), bf16)
    return pl.pallas_call(
        send_kernel,
        grid_spec=pltpu.PrefetchScalarGridSpec(
            num_scalar_prefetch=1,
            grid=(1,),
            in_specs=[whole((2, tokens)), whole((2, tokens)), column, column],
            out_specs=[whole(sent.shape), whole((experts * capacity, tokens))],
        ),
        out_shape=[sent, jax.ShapeDtypeStruct((experts * capacity, tokens), bf16)],
        cost_estimate=cost(400_000_000, 3_000_000),
    )(tp, routes.T, route_weight.T, mixer_out, out_cot)


def block_of(t, k):
    return lax.rem(t + k, 4)


def times(block_refs, w_ref, t, width, cw):
    acc = None
    for k in range(4):
        at = pl.ds(pl.multiple_of(block_of(t, k) * width, width), width)
        w = w_ref[at, :] if cw == 0 else w_ref[:, at]
        if k == 2:
            part = jnp.concatenate([dot(r[...], w, 1, cw) for r in block_refs[2:4]], axis=0)
        else:
            part = dot(block_refs[k + (k == 3)][...], w, 1, cw)
        acc = part if acc is None else acc + part
    return acc


def forward_kernel(t_ref, *refs):
    blocks, (wg_ref, wu_ref, pg_ref, pu_ref) = refs[:5], refs[5:]
    width = blocks[0].shape[1]
    pg_ref[...] = times(blocks, wg_ref, t_ref[0], width, 0)
    pu_ref[...] = times(blocks, wu_ref, t_ref[0], width, 0)


def expert_forward(tp, x_blocks, w_gate, w_up):
    rows, hidden = x_blocks[0].shape[0], w_gate.shape[1]
    out = jax.ShapeDtypeStruct((rows, hidden), f32)
    return pl.pallas_call(
        forward_kernel,
        in_specs=[SM] + [VM] * 7,
        out_specs=[VM, VM],
        out_shape=[out, out],
        compiler_params=PARAMS,
        cost_estimate=cost(1_073_741_824, 5_000_000),
    )(tp, *x_blocks, w_gate, w_up)


def backward_kernel(t_ref, *refs):
    blocks = refs[:5]
    wd_ref, pg_ref, pu_ref, wg_ref, wu_ref, act_ref, gp_ref, up_ref = refs[5:13]
    outs = refs[13:]
    width = blocks[0].shape[1]
    half = blocks[0].shape[0] // 2
    act_grad = times(blocks, wd_ref, t_ref[0], width, 1)
    pre_gate = pg_ref[...]
    pre_up = pu_ref[...]
    sig = jax.nn.sigmoid(pre_gate)
    silu = pre_gate * sig
    act_ref[...] = (silu * pre_up).astype(bf16)
    gp_ref[...] = (act_grad * pre_up * sig * (1.0 + pre_gate * (1.0 - sig))).astype(bf16)
    up_ref[...] = (act_grad * silu).astype(bf16)
    for i, k in enumerate((2, 3, 1, 0)):
        cols = pl.ds(pl.multiple_of(block_of(t_ref[0], k) * width, width), width)
        back = dot(gp_ref[...], wg_ref[cols, :], 1, 1) + dot(up_ref[...], wu_ref[cols, :], 1, 1)
        outs[2 * i][...] = back[:half].astype(bf16)
        outs[2 * i + 1][...] = back[half:].astype(bf16)


def expert_backward(tp, c_blocks, w_down, pre_gate, pre_up, w_gate, w_up):
    half, width = c_blocks[2].shape
    rows, hidden = pre_gate.shape
    small = jax.ShapeDtypeStruct((rows, hidden), bf16)
    return pl.pallas_call(
        backward_kernel,
        in_specs=[SM] + [VM] * 10,
        out_specs=[VM] * 11,
        out_shape=[small] * 3 + [jax.ShapeDtypeStruct((half, width), bf16)] * 8,
        compiler_params=PARAMS,
        cost_estimate=cost(1_610_612_736, 9_000_000),
    )(tp, *c_blocks, w_down, pre_gate, pre_up, w_gate, w_up)


def weight_kernel(t_ref, *refs):
    xs, cs = refs[:5], refs[5:10]
    act_ref, gp_ref, up_ref, gg_ref, ug_ref, dg_ref = refs[10:]
    _, width = xs[2].shape
    for k in range(4):
        at = pl.ds(pl.multiple_of(block_of(t_ref[0], k) * width, width), width)
        i = k + (k == 3)
        x, c = (
            jnp.concatenate([b[2][...], b[3][...]], axis=0) if k == 2 else b[i][...]
            for b in (xs, cs)
        )
        gg_ref[at, :] = dot(x, gp_ref[...], 0, 0).astype(bf16)
        ug_ref[at, :] = dot(x, up_ref[...], 0, 0).astype(bf16)
        dg_ref[:, at] = dot(act_ref[...], c, 0, 0).astype(bf16)


def weight_grads(tp, x_blocks, c_blocks, act, gate_pre, up_pre):
    width = x_blocks[0].shape[1]
    hidden = act.shape[1]
    tall = jax.ShapeDtypeStruct((4 * width, hidden), bf16)
    return pl.pallas_call(
        weight_kernel,
        in_specs=[SM] + [VM] * 13,
        out_specs=[VM] * 3,
        out_shape=[tall, tall, jax.ShapeDtypeStruct((hidden, 4 * width), bf16)],
        compiler_params=PARAMS,
        cost_estimate=cost(1_610_612_736, 8_000_000),
    )(tp, *x_blocks, *c_blocks, act, gate_pre, up_pre)


def column(row):
    return jnp.broadcast_to(row, (8, row.shape[1])).T[:, 0:1]


def gate(conv, inv_rms, gain):
    normed = conv * inv_rms * gain
    sig = jax.nn.sigmoid(normed)
    return normed * sig, sig * (1.0 + normed * (1.0 - sig)) * gain


def act_kernel(t_ref, p0_ref, p1_ref, p2_ref, p3_ref, conv_ref, gain_ref, w_ref, act_ref, inv_ref, *q_refs):
    width = conv_ref.shape[1]
    power = (p0_ref[...] + p1_ref[...]) + (p2_ref[...] + p3_ref[...])
    inv_rms = column(lax.rsqrt(power / w_ref.shape[1] + norm_epsilon))
    conv = conv_ref[...].astype(f32)
    act, slope = gate(conv, inv_rms, gain_ref[...])
    act_ref[...] = act.astype(bf16)
    inv_ref[...] = inv_rms
    pulled = (conv * slope).astype(bf16)
    for k in range(4):
        at = pl.ds(pl.multiple_of(block_of(t_ref[0], k) * width, width), width)
        q_refs[k][...] = dot(pulled, w_ref[:, at], 1, 0).astype(bf16)


def act_parts(tp, powers, conv_out, gain, out_weight):
    block = jax.ShapeDtypeStruct(conv_out.shape, bf16)
    return pl.pallas_call(
        act_kernel,
        in_specs=[SM] + [VM] * 7,
        out_specs=[VM] * 6,
        out_shape=[block, jax.ShapeDtypeStruct((conv_out.shape[0], 1), f32)] + [block] * 4,
        compiler_params=PARAMS,
        cost_estimate=cost(268_435_456, 3_000_000),
    )(tp, *powers, conv_out, gain, out_weight)


def mix_kernel(t_ref, sel_ref, back_ref, q_ref, cot_ref, mix_ref, out_ref, dot_ref):
    tokens, width = cot_ref.shape
    ret = back_ref[...].reshape(sel_ref.shape[0], width)
    mix = cot_ref[...].astype(f32) + dot(sel_ref[...], ret, 0, 0)
    mix_ref[...] = mix.astype(bf16)
    turned = mix.T.astype(bf16)
    run = width // 16
    for g in range(8):
        piece = jnp.concatenate(
            [turned[(q * 8 + g) * run : (q * 8 + g + 1) * run] for q in range(2)], axis=0
        )
        for j in range(4):
            out_ref[g * 4 + j] = piece
    dots = jnp.sum(mix.astype(bf16).astype(f32) * q_ref[...], axis=1, keepdims=True)
    dot_ref[...] = jnp.broadcast_to(dots, (tokens, 128)).T[0:1, :]


def mix_parts(tp, sel, returned, q_total, out_cot):
    tokens = out_cot.shape[0]
    _, _, quarter = returned.shape
    whole = lambda shape: pl.BlockSpec(shape, lambda i, t: (0,) * len(shape))
    shapes = [(tokens, quarter), (32, quarter // 8, tokens)]
    return pl.pallas_call(
        mix_kernel,
        grid_spec=pltpu.PrefetchScalarGridSpec(
            num_scalar_prefetch=1,
            grid=(1,),
            in_specs=[
                whole(sel.shape),
                whole(returned.shape),
                whole((tokens, quarter)),
                pl.BlockSpec((tokens, quarter), lambda i, t: (0, t[0])),
            ],
            out_specs=[*[whole(s) for s in shapes], whole((1, tokens))],
        ),
        out_shape=[
            *[jax.ShapeDtypeStruct(s, bf16) for s in shapes],
            jax.ShapeDtypeStruct((1, tokens), f32),
        ],
        compiler_params=PARAMS,
        cost_estimate=cost(70_000_000, 2_000_000),
    )(tp, sel, returned, q_total, out_cot)


def sum_kernel(oa_ref, na_ref, pa_ref, ob_ref, nb_ref, pb_ref, out_ref):
    half = out_ref.shape[0] // 2
    for at, refs in ((0, (oa_ref, na_ref, pa_ref)), (half, (ob_ref, nb_ref, pb_ref))):
        total = refs[0][...].astype(f32) + refs[1][...].astype(f32) + refs[2][...].astype(f32)
        out_ref[pl.ds(at, half)] = total.astype(bf16).reshape(half, *out_ref.shape[1:])


def sum_rows(parts, experts):
    rows, width = parts[0].shape
    shape = (experts, 2 * rows // experts, width)
    return pl.pallas_call(
        sum_kernel,
        in_specs=[VM] * 6,
        out_specs=VM,
        out_shape=jax.ShapeDtypeStruct(shape, bf16),
        compiler_params=PARAMS,
        cost_estimate=cost(1_000_000, 2_000_000),
    )(*parts)


def proj_kernel(at_ref, mix_ref, *refs):
    acts, (out_ref, left_ref, right_ref, sems) = refs[:4], refs[4:]
    rows, tokens = 4 * mix_ref.shape[1], mix_ref.shape[2]
    copies = []
    for r in range(4):
        for c in range(2):
            core = at_ref[1] if c == 0 else 1 - at_ref[1]
            g = 2 * block_of(at_ref[0], r) + core
            to = right_ref.at[pl.ds(pl.multiple_of(g * tokens, tokens), tokens)]
            copies.append(pltpu.make_async_copy(acts[r].at[c], to, sems.at[2 * r + c]))
    for copy in copies:
        copy.start()
    for g in range(8):
        left_ref[:, g * tokens : (g + 1) * tokens] = mix_ref[4 * g : 4 * g + 4].reshape(rows, tokens)
    for copy in copies:
        copy.wait()
    out = dot(left_ref[...], right_ref[...], 1, 0)
    out_ref[...] = out.astype(bf16).reshape(out_ref.shape)


def proj_partial(at, mixed, acts):
    tokens, width = acts[0].shape[1:]
    rows = 4 * mixed.shape[1]
    return pl.pallas_call(
        proj_kernel,
        in_specs=[SM, VM] + [pl.BlockSpec(memory_space=pltpu.HBM)] * 4,
        out_specs=VM,
        out_shape=jax.ShapeDtypeStruct((8, rows // 8, width), bf16),
        scratch_shapes=[
            pltpu.VMEM((rows, 8 * tokens), bf16),
            pltpu.VMEM((8 * tokens, width), bf16),
            pltpu.SemaphoreType.DMA((8,)),
        ],
        compiler_params=PARAMS,
        cost_estimate=cost(268_435_456, 2_000_000),
    )(at, mixed, *acts)


def grad_kernel(t_ref, *refs):
    blocks, dots = refs[:4], refs[4:8]
    inv_ref, conv_ref, gain_ref, w_ref, out_ref, head_ref = refs[8:]
    width = blocks[0].shape[1]
    back = None
    for k in range(4):
        at = pl.ds(pl.multiple_of(block_of(t_ref[0], k) * width, width), width)
        part = dot(blocks[k][...], w_ref[:, at], 1, 1)
        back = part if back is None else back + part
    conv = conv_ref[...].astype(f32)
    inv_rms = inv_ref[...]
    scaled = back * gate(conv, inv_rms, gain_ref[...])[1]
    total = (dots[0][...] + dots[1][...]) + (dots[2][...] + dots[3][...])
    pull = column(total / w_ref.shape[1]) * inv_rms * inv_rms * inv_rms
    conv_grad = inv_rms * scaled - conv * pull
    out_ref[...] = conv_grad
    head_ref[...] = conv_grad[: head_ref.shape[0]].astype(bf16)


def conv_backward(tp, blocks, dots, inv_rms, conv_out, gain, out_weight):
    return pl.pallas_call(
        grad_kernel,
        in_specs=[SM] + [VM] * 12,
        out_specs=[VM] * 2,
        out_shape=[
            jax.ShapeDtypeStruct(conv_out.shape, f32),
            jax.ShapeDtypeStruct((32, conv_out.shape[1]), bf16),
        ],
        compiler_params=PARAMS,
        cost_estimate=cost(268_435_456, 2_000_000),
    )(tp, *blocks, *dots, inv_rms, conv_out, gain, out_weight)


def taps_kernel(grad_ref, next_ref, taps_ref, out_ref, ext_ref):
    tokens, width = grad_ref.shape
    ext_ref[pl.ds(0, tokens), :] = grad_ref[...]
    ext_ref[pl.ds(tokens, next_ref.shape[0]), :] = next_ref[...].astype(f32)
    for lane in range(0, width, 128):
        lanes = pl.ds(lane, 128)
        acc = None
        for w in range(taps_ref.shape[0]):
            part = taps_ref[w : w + 1, lanes] * ext_ref[pl.ds(w, tokens), lanes]
            acc = part if acc is None else acc + part
        out_ref[:, lanes] = acc


def taps_backward(conv_grad, following, taps):
    rows = conv_grad.shape[0] + following.shape[0]
    return pl.pallas_call(
        taps_kernel,
        in_specs=[VM] * 3,
        out_specs=VM,
        out_shape=jax.ShapeDtypeStruct(conv_grad.shape, f32),
        scratch_shapes=[pltpu.VMEM((rows, conv_grad.shape[1]), f32)],
        compiler_params=PARAMS,
        cost_estimate=cost(4_000_000, 1_000_000),
    )(conv_grad, following, taps)


def exchange(x, axis):
    return lax.all_to_all(x, axis, split_axis=0, concat_axis=0, tiled=True)


AHEAD = [(i, (i + 1) % 4) for i in range(4)]
BEHIND = [(i, (i - 1) % 4) for i in range(4)]
ACROSS = [(i, (i + 2) % 4) for i in range(4)]


def ring_gather(block):
    half = block.shape[0] // 2
    ahead = lax.ppermute(block, "tp", AHEAD)
    behind = lax.ppermute(block, "tp", BEHIND)
    across_a = lax.ppermute(ahead[:half], "tp", AHEAD)
    across_b = lax.ppermute(behind[half:], "tp", BEHIND)
    return [block, behind, across_a, across_b, ahead]


def ring_all(x, axis="tp"):
    ahead = lax.ppermute(x, axis, AHEAD)
    behind = lax.ppermute(x, axis, BEHIND)
    across = lax.ppermute(x, axis, ACROSS)
    return [x, behind, across, ahead]


def plus(*terms):
    return sum(x.astype(f32) for x in terms).astype(bf16)


def ring_scatter(far_a, far_b, prev_a, prev_b, next_a, next_b, own_a, own_b):
    far_a = lax.ppermute(far_a, "tp", AHEAD)
    far_b = lax.ppermute(far_b, "tp", BEHIND)
    next_b = lax.ppermute(next_b, "tp", AHEAD)
    prev_a = lax.ppermute(prev_a, "tp", BEHIND)
    next_a = lax.ppermute(plus(next_a, far_a), "tp", AHEAD)
    prev_b = lax.ppermute(plus(prev_b, far_b), "tp", BEHIND)
    return own_a, next_a, prev_a, own_b, next_b, prev_b


def on_device(
    mixer_out,
    conv_out,
    out_cot,
    routes,
    route_weight,
    gate_weight,
    up_weight,
    down_weight,
    out_weight,
    norm_gain,
    conv_taps,
):
    tokens_here, _ = out_cot.shape
    experts = lax.axis_size(SP)
    capacity = 2 * tokens_here * routes.shape[1] // experts
    quarter = conv_out.shape[1]
    tp = lax.axis_index("tp").astype(jnp.int32)[None]
    w_gate, w_up, w_down = gate_weight[0], up_weight[0], down_weight[0]

    send, sel = send_rows(
        tp, routes, route_weight, mixer_out, out_cot, experts, capacity, quarter
    )
    slots = experts * capacity
    arrived = exchange(send, SP).reshape(slots, 2 * quarter)
    x_slice, cot_slice = arrived[:, :quarter], arrived[:, quarter:]

    conv_vals = conv_out.astype(f32)
    powers = ring_all(jnp.sum(conv_vals * conv_vals, axis=1)[None])
    gain = norm_gain[None]
    activated, inv_rms, *q_parts = act_parts(tp, powers, conv_out, gain, out_weight)
    q_ahead = lax.ppermute(q_parts[1], "tp", AHEAD)
    q_across = lax.ppermute(q_parts[2], "tp", ACROSS)
    q_behind = lax.ppermute(q_parts[3], "tp", BEHIND)
    q_total = sum(q.astype(f32) for q in (q_parts[0], q_ahead, q_across, q_behind))
    act_other = lax.ppermute(activated, "core", [(0, 1), (1, 0)])
    act_near = ring_all(jnp.stack([activated, act_other]), "y")

    x_blocks = ring_gather(x_slice)
    pre_gate, pre_up = expert_forward(tp, x_blocks, w_gate, w_up)
    c_blocks = ring_gather(cot_slice)
    act, gate_pre, up_pre, *parts = expert_backward(
        tp, c_blocks, w_down, pre_gate, pre_up, w_gate, w_up
    )
    sums = ring_scatter(*parts)
    back = sum_rows(sums, experts)
    returned = exchange(back, SP)
    gate_g, up_g, down_g = weight_grads(tp, x_blocks, c_blocks, act, gate_pre, up_pre)

    mix_part, mix_turned, dots = mix_parts(tp, sel, returned, q_total, out_cot)
    mixed = exchange(mix_turned, ("y", "core", "tp"))
    mix_blocks = ring_all(mix_part)
    at = jnp.stack([lax.axis_index("y"), lax.axis_index("core")]).astype(jnp.int32)
    partial_proj = proj_partial(at, mixed, act_near)
    partial_proj = exchange(partial_proj, "z")
    proj_grad = jnp.sum(partial_proj.astype(f32), axis=0)

    dot_blocks = ring_all(dots)
    conv_grad, head = conv_backward(
        tp, mix_blocks, dot_blocks, inv_rms, conv_out, gain, out_weight
    )
    route = [(i, i - 1) for i in range(1, experts)]
    following = lax.ppermute(head, SP, route)
    gated_grad = taps_backward(conv_grad, following, conv_taps)
    return (gate_g[None], up_g[None], down_g[None], proj_grad, gated_grad)


def solution(mesh):
    fine = Mesh(mesh.devices.reshape(8, 4, 2, 4), ("z", "y", "core", "tp"))
    placed = (
        P(SP, None),
        P(SP, "tp"),
        P(SP, None),
        P(SP, None),
        P(SP, None),
        P(SP, None, "tp"),
        P(SP, None, "tp"),
        P(SP, "tp", None),
        P("tp", None),
        P("tp"),
        P(None, "tp"),
    )
    return jax.shard_map(
        on_device,
        mesh=fine,
        in_specs=placed,
        out_specs=(
            P(SP, None, "tp"),
            P(SP, None, "tp"),
            P(SP, "tp", None),
            P(SP, "tp"),
            P(SP, "tp"),
        ),
        check_vma=False,
    )
```

profile of v0, /device:TPU:8, one launch (start us, length us, event | category | flops | bytes accessed | tf_op | source)
XLA Modules:
  0.0 202.9 jit_solution(8418205248884734036)
XLA Ops:
  0.6 2.8 %shard_map.146 = (bf16[64,8,1024]{2,1,0:T(8,128)(2,1)}, bf16[512,128]{1,0:T(8,128)(2,1)}) custom-call(s32[1]{0:T(128)} %bitcast.tp_ref.t_ref, s32[2,128]{1,0:T(2,128)} %bitcast.28, f32[2,128]{1,0:T(2,128)} %bitcast.29, bf16[128,2048]{1,0:T(8,128)(2,1)} %x_ref.1, bf16[128,2048]{1,0:T(8,128)(2,1)} %cot_ref.3), custom_call_target="tpu_custom_call" | custom-call | flops 400000000 | bytes 3000000 | tf_op jit(solution)/shard_map/pallas_call | solution.py:67
  3.4 40.9 %all_to_all.20 = bf16[64,8,1024]{2,1,0:T(8,128)(2,1)S(1)} all-to-all(bf16[64,8,1024]{2,1,0:T(8,128)(2,1)} %get-tuple-element.34), channel_id=1, replica_groups=mesh['z'=8,'y'=4,'core'=2,'tp'=4] {'z','y','core'}, dimensions={0} | all-to-all | bytes 2097152 | tf_op jit(solution)/shard_map/all_to_all | solution.py:380
  44.4 1.6 collective-permute-start.1
  45.9 1.7 collective-permute-start
  48.0 3.0 %collective-permute-start.4 = (bf16[512,512]{1,0:T(8,128)(2,1)S(1)}, bf16[512,512]{1,0:T(8,128)(2,1)S(1)}, u32[]{:S(2)}, u32[]{:S(2)}) collective-permute-start(bf16[512,512]{1,0:T(8,128)(2,1)S(1)} %get-tuple-element.63.refs_0_.refs_5_), channel_id=1, source_target_pairs={{0,3},{1,0},{2,1},{3,2},{4,7},{5,4},{6,5},{7,6},{8,11},{9,8},{10,9... | collective-permute-start | bytes 1572872 | tf_op jit(solution)/shard_map/ppermute | solution.py:391
  50.9 9.5 %collective-permute-done.1.refs_4_ = bf16[512,512]{1,0:T(8,128)(2,1)S(1)} collective-permute-done((bf16[512,512]{1,0:T(8,128)(2,1)S(1)}, bf16[512,512]{1,0:T(8,128)(2,1)S(1)}, u32[]{:S(2)}, u32[]{:S(2)}) %collective-permute-start.1) | collective-permute-done | bytes 524320 | tf_op jit(solution)/shard_map/ppermute | solution.py:390
  60.9 3.0 %collective-permute-start.3 = (bf16[256,512]{1,0:T(8,128)(2,1)S(1)}, bf16[256,512]{1,0:T(8,128)(2,1)S(1)}, u32[]{:S(2)}, u32[]{:S(2)}) collective-permute-start(bf16[256,512]{1,0:T(8,128)(2,1)S(1)} %slice.26), channel_id=1, source_target_pairs={{0,3},{1,0},{2,1},{3,2},{4,7},{5,4},{6,5},{7,6},{8,11},{9,8},{10,9... | collective-permute-start | bytes 786440 | tf_op jit(solution)/shard_map/ppermute | solution.py:393
  63.9 7.8 %collective-permute-done.5.refs_4_.refs_9_ = bf16[512,512]{1,0:T(8,128)(2,1)S(1)} collective-permute-done((bf16[512,512]{1,0:T(8,128)(2,1)S(1)}, bf16[512,512]{1,0:T(8,128)(2,1)S(1)}, u32[]{:S(2)}, u32[]{:S(2)}) %collective-permute-start.5) | collective-permute-done | bytes 524320 | tf_op jit(solution)/shard_map/ppermute | solution.py:390
  72.1 3.0 %collective-permute-start.7 = (bf16[256,512]{1,0:T(8,128)(2,1)S(1)}, bf16[256,512]{1,0:T(8,128)(2,1)S(1)}, u32[]{:S(2)}, u32[]{:S(2)}) collective-permute-start(bf16[256,512]{1,0:T(8,128)(2,1)S(1)} %slice.29), channel_id=1, source_target_pairs={{0,3},{1,0},{2,1},{3,2},{4,7},{5,4},{6,5},{7,6},{8,11},{9,8},{10,9... | collective-permute-start | bytes 786440 | tf_op jit(solution)/shard_map/ppermute | solution.py:393
  75.1 2.2 %collective-permute-done.2.refs_2_ = bf16[256,512]{1,0:T(8,128)(2,1)S(1)} collective-permute-done((bf16[256,512]{1,0:T(8,128)(2,1)S(1)}, bf16[256,512]{1,0:T(8,128)(2,1)S(1)}, u32[]{:S(2)}, u32[]{:S(2)}) %collective-permute-start.2) | collective-permute-done | bytes 262176 | tf_op jit(solution)/shard_map/ppermute | solution.py:392
  77.6 1.3 shard_map.147
  78.9 1.9 collective-permute-done.6.refs_2_.refs_7_
  80.8 3.0 %shard_map.148 = (bf16[512,256]{1,0:T(8,128)(2,1)S(1)}, bf16[512,256]{1,0:T(8,128)(2,1)S(1)}, bf16[512,256]{1,0:T(8,128)(2,1)S(1)}, bf16[256,512]{1,0:T(8,128)(2...) custom-call(s32[1]{0:T(128)} %bitcast.tp_ref.t_ref, ...), custom_call_target="tpu_custom_call" | custom-call | flops 1610612736 | bytes 9000000 | tf_op jit(solution)/shard_map/pallas_call | solution.py:142
  83.9 3.0 %collective-permute-start.12 = (bf16[256,512]{1,0:T(8,128)(2,1)S(1)}, bf16[256,512]{1,0:T(8,128)(2,1)S(1)}, u32[]{:S(2)}, u32[]{:S(2)}) collective-permute-start(bf16[256,512]{1,0:T(8,128)(2,1)S(1)} %get-tuple-element.51), channel_id=1, source_target_pairs={{0,3},{1,0},{2,1},{3,2},{4,7},{5,4},{6,5},{7,6},{8,11},{9,8},{10,9... | collective-permute-start | bytes 786440 | tf_op jit(solution)/shard_map/ppermute | solution.py:410
  86.9 3.2 %collective-permute-start.10 = (bf16[256,512]{1,0:T(8,128)(2,1)S(1)}, bf16[256,512]{1,0:T(8,128)(2,1)S(1)}, u32[]{:S(2)}, u32[]{:S(2)}) collective-permute-start(bf16[256,512]{1,0:T(8,128)(2,1)S(1)} %get-tuple-element.47), channel_id=1, source_target_pairs={{0,3},{1,0},{2,1},{3,2},{4,7},{5,4},{6,5},{7,6},{8,11},{9,8},{10,9... | collective-permute-start | bytes 786440 | tf_op jit(solution)/shard_map/ppermute | solution.py:412
  90.1 3.5 %collective-permute-done.12 = bf16[256,512]{1,0:T(8,128)(2,1)S(1)} collective-permute-done((bf16[256,512]{1,0:T(8,128)(2,1)S(1)}, bf16[256,512]{1,0:T(8,128)(2,1)S(1)}, u32[]{:S(2)}, u32[]{:S(2)}) %collective-permute-start.12) | collective-permute-done | bytes 262176 | tf_op jit(solution)/shard_map/ppermute | solution.py:410
  93.7 3.8 %collective-permute-start.13 = (bf16[256,512]{1,0:T(8,128)(2,1)S(1)}, bf16[256,512]{1,0:T(8,128)(2,1)S(1)}, u32[]{:S(2)}, u32[]{:S(2)}) collective-permute-start(bf16[256,512]{1,0:T(8,128)(2,1)S(1)} %add_convert_fusion), channel_id=1, source_target_pairs={{0,3},{1,0},{2,1},{3,2},{4,7},{5,4},{6,5},{7,6},{8,11},{9,8},{10,9... | collective-permute-start | bytes 786440 | tf_op jit(solution)/shard_map/ppermute | solution.py:414
  97.6 1.1 collective-permute-done.10.pa_ref
  98.8 3.4 %collective-permute-done.11.nb_ref = bf16[256,512]{1,0:T(8,128)(2,1)S(1)} collective-permute-done((bf16[256,512]{1,0:T(8,128)(2,1)S(1)}, bf16[256,512]{1,0:T(8,128)(2,1)S(1)}, u32[]{:S(2)}, u32[]{:S(2)}) %collective-permute-start.11) | collective-permute-done | bytes 262176 | tf_op jit(solution)/shard_map/ppermute | solution.py:411
  102.2 3.0 %collective-permute-done.9.na_ref = bf16[256,512]{1,0:T(8,128)(2,1)S(1)} collective-permute-done((bf16[256,512]{1,0:T(8,128)(2,1)S(1)}, bf16[256,512]{1,0:T(8,128)(2,1)S(1)}, u32[]{:S(2)}, u32[]{:S(2)}) %collective-permute-start.9) | collective-permute-done | bytes 262176 | tf_op jit(solution)/shard_map/ppermute | solution.py:413
  105.4 0.8 copy-done.3
  106.2 7.7 %all-to-all-start.1 = ((bf16[64,8,512]{2,1,0:T(8,128)(2,1)}), bf16[64,8,512]{2,1,0:T(8,128)(2,1)}, u32[]{:S(2)}, u32[]{:S(2)}) async-start(bf16[64,8,512]{2,1,0:T(8,128)(2,1)} %copy-done.3), calls=%async_computation.1 | async-start | bytes 1048576 | tf_op jit(solution)/shard_map/all_to_all | solution.py:380
  114.4 0.8 collective-permute-start.15
  115.2 0.9 collective-permute-start.16
  116.1 1.5 collective-permute-done.14.p1_ref
  117.7 1.8 collective-permute-done.15.p2_ref
  119.5 0.9 collective-permute-done.16.p3_ref
  120.4 0.9 shard_map.151
  121.3 0.6 copy-done.28
  121.9 0.9 collective-permute-start.17
  122.8 2.6 %collective-permute-start.18 = (bf16[128,512]{1,0:T(8,128)(2,1)S(1)}, bf16[128,512]{1,0:T(8,128)(2,1)S(1)}, u32[]{:S(2)}, u32[]{:S(2)}) collective-permute-start(bf16[128,512]{1,0:T(8,128)(2,1)S(1)} %get-tuple-element.54), channel_id=1, source_target_pairs={{0,2},{1,3},{2,0},{3,1},{4,6},{5,7},{6,4},{7,5},{8,10},{9,11},{10,... | collective-permute-start | bytes 393224 | tf_op jit(solution)/shard_map/ppermute | solution.py:450
  125.8 4.7 %collective-permute-done.17 = bf16[128,512]{1,0:T(8,128)(2,1)S(1)} collective-permute-done((bf16[128,512]{1,0:T(8,128)(2,1)S(1)}, bf16[128,512]{1,0:T(8,128)(2,1)S(1)}, u32[]{:S(2)}, u32[]{:S(2)}) %collective-permute-start.17) | collective-permute-done | bytes 131104 | tf_op jit(solution)/shard_map/ppermute | solution.py:449
  131.4 1.0 copy-done.14
  132.4 0.9 copy-done.26
  133.3 1.5 shard_map.152
  134.8 0.8 copy-done.15
  135.6 0.7 copy-done.24
  136.3 6.9 %all-to-all-start.2 = ((bf16[32,64,128]{2,1,0:T(8,128)(2,1)}), bf16[32,64,128]{2,1,0:T(8,128)(2,1)}, u32[]{:S(2)}, u32[]{:S(2)}) async-start(bf16[32,64,128]{2,1,0:T(8,128)(2,1)} %copy-done.15), calls=%async_computation.2 | async-start | bytes 1048576 | tf_op jit(solution)/shard_map/all_to_all | solution.py:380
  143.2 1.0 pad_maximum_fusion.refs_0_
  144.6 2.6 %collective-permute-start.22 = (bf16[2,128,512]{2,1,0:T(8,128)(2,1)S(1)}, bf16[2,128,512]{2,1,0:T(8,128)(2,1)}, u32[]{:S(2)}, u32[]{:S(2)}) collective-permute-start(bf16[2,128,512]{2,1,0:T(8,128)(2,1)S(1)} %pad_maximum_fusion.refs_0_), channel_id=1, source_target_pairs={{0,16},{8,24},{16,0},{24,8},{1,17},{9,25},{17,1},{25,9},{2,18},{10... | collective-permute-start | bytes 786440 | tf_op jit(solution)/shard_map/ppermute | solution.py:400
  147.2 1.8 collective-permute-start.23
  149.1 8.5 %collective-permute-done.21.refs_1_ = bf16[2,128,512]{2,1,0:T(8,128)(2,1)} collective-permute-done((bf16[2,128,512]{2,1,0:T(8,128)(2,1)S(1)}, bf16[2,128,512]{2,1,0:T(8,128)(2,1)}, u32[]{:S(2)}, u32[]{:S(2)}) %collective-permute-start.21) | collective-permute-done | bytes 262176 | tf_op jit(solution)/shard_map/ppermute | solution.py:399
  157.5 5.7 %collective-permute-done.22.refs_2_ = bf16[2,128,512]{2,1,0:T(8,128)(2,1)} collective-permute-done((bf16[2,128,512]{2,1,0:T(8,128)(2,1)S(1)}, bf16[2,128,512]{2,1,0:T(8,128)(2,1)}, u32[]{:S(2)}, u32[]{:S(2)}) %collective-permute-start.22) | collective-permute-done | bytes 262176 | tf_op jit(solution)/shard_map/ppermute | solution.py:400
  163.3 3.8 %shard_map.153 = bf16[8,32,512]{2,1,0:T(8,128)(2,1)} custom-call(s32[2]{0:T(128)S(1)} %pad_add_fusion.at_ref, bf16[32,64,128]{2,1,0:T(8,128)(2,1)} %all-to-all-done.2.mix_ref, bf16[2,128,512]{2,1,0:T(8,128)(2,1)S(1)} %pad_maximum_fusion.refs_0_, bf16[2,128,512]{2,1,0:T(8,128)(2,1)} %collective-permute-done.21.refs_1_, ...), custom_call_target="tpu_custom_call" | custom-call | flops 268435456 | bytes 2000000 | tf_op jit(solution)/shard_map/pallas_call | solution.py:305
  167.1 6.9 %all-to-all-start.3 = ((bf16[8,32,512]{2,1,0:T(8,128)(2,1)}), bf16[8,32,512]{2,1,0:T(8,128)(2,1)}, u32[]{:S(2)}, u32[]{:S(2)}) async-start(bf16[8,32,512]{2,1,0:T(8,128)(2,1)} %shard_map.153), calls=%async_computation.3 | async-start | bytes 524288 | tf_op jit(solution)/shard_map/all_to_all | solution.py:380
  174.1 2.8 %collective-permute-start.24 = (bf16[128,512]{1,0:T(8,128)(2,1)}, bf16[128,512]{1,0:T(8,128)(2,1)S(1)}, u32[]{:S(2)}, u32[]{:S(2)}) collective-permute-start(bf16[128,512]{1,0:T(8,128)(2,1)} %copy-done.24), channel_id=1, source_target_pairs={{0,3},{1,0},{2,1},{3,2},{4,7},{5,4},{6,5},{7,6},{8,11},{9,8},{10,9... | collective-permute-start | bytes 393224 | tf_op jit(solution)/shard_map/ppermute | solution.py:399
  176.9 0.8 collective-permute-start.25
  177.7 0.9 collective-permute-start.26
  178.6 2.4 %collective-permute-start.27 = (f32[1,128]{1,0:T(1,128)S(1)}, f32[1,128]{1,0:T(1,128)S(1)}, u32[]{:S(2)}, u32[]{:S(2)}) collective-permute-start(f32[1,128]{1,0:T(1,128)S(1)} %get-tuple-element.59.refs_4_), channel_id=1, source_target_pairs={{0,3},{1,0},{2,1},{3,2},{4,7},{5,4},{6,5},{7,6},{8,11},{9,8},{10,9... | collective-permute-start | bytes 1544 | tf_op jit(solution)/shard_map/ppermute | solution.py:399
  180.9 1.5 collective-permute-start.28
  182.5 1.8 collective-permute-start.29
  184.3 1.8 collective-permute-done.28.refs_6_
  186.1 1.6 collective-permute-done.29.refs_7_
  187.7 0.9 copy-done.25
  188.6 0.8 copy-done.29
  189.5 0.8 shard_map.154
  190.3 1.9 collective-permute-start.30
  192.3 0.9 copy-done.23
  193.3 0.9 copy-done.32
  194.2 0.9 copy-done.34
  195.2 0.9 copy-done.36
  196.1 3.4 %shard_map.149 = (bf16[2048,256]{1,0:T(8,128)(2,1)}, bf16[2048,256]{1,0:T(8,128)(2,1)}, bf16[256,2048]{1,0:T(8,128)(2,1)}) custom-call(s32[1]{0:T(128)} %bitcast.tp_ref.t_ref, bf16[512,512]{1,0:T(8,128)(2,1)S(1)} %get-tuple-element.64.refs_0_, bf16[512,512]{1,0:T(8,128)(2,1)S(1)} %copy-done.7, bf16[256,512]{1,0:T(8,128)(2,1)S(1)} %copy-done.17, ...), custom_call_target="tpu_custom_call" | custom-call | flops 1610612736 | bytes 8000000 | tf_op jit(solution)/shard_map/pallas_call | solution.py:172
  199.5 1.7 shard_map.155
  201.2 1.6 convert_reduce_fusion
  (101 shorter events, 4.3 us)
Async XLA Ops:
  44.3 33.3 %copy-start.1 = (bf16[1,2048,256]{2,1,0:T(8,128)(2,1)S(1)}, bf16[1,2048,256]{2,1,0:T(8,128)(2,1)}, u32[]{:S(2)}) copy-start(bf16[1,2048,256]{2,1,0:T(8,128)(2,1)} %param.16) | copy-start | bytes 3145732
  44.3 33.3 %copy-start.2 = (bf16[1,2048,256]{2,1,0:T(8,128)(2,1)S(1)}, bf16[1,2048,256]{2,1,0:T(8,128)(2,1)}, u32[]{:S(2)}) copy-start(bf16[1,2048,256]{2,1,0:T(8,128)(2,1)} %param.17) | copy-start | bytes 3145732
  44.4 16.1 %collective-permute-start.1 = (bf16[512,512]{1,0:T(8,128)(2,1)S(1)}, bf16[512,512]{1,0:T(8,128)(2,1)S(1)}, u32[]{:S(2)}, u32[]{:S(2)}) collective-permute-start(bf16[512,512]{1,0:T(8,128)(2,1)S(1)} %get-tuple-element.64.refs_0_), channel_id=1, source_target_pairs={{0,1},{1,2},{2,3},{3,0},{4,5},{5,6},{6,7},{7,4},{8,9},{9,10},{10,1... | collective-permute-start | bytes 1572872 | tf_op jit(solution)/shard_map/ppermute | solution.py:390
  45.9 14.9 %collective-permute-start = (bf16[512,512]{1,0:T(8,128)(2,1)S(1)}, bf16[512,512]{1,0:T(8,128)(2,1)S(1)}, u32[]{:S(2)}, u32[]{:S(2)}) collective-permute-start(bf16[512,512]{1,0:T(8,128)(2,1)S(1)} %get-tuple-element.64.refs_0_), channel_id=1, source_target_pairs={{0,3},{1,0},{2,1},{3,2},{4,7},{5,4},{6,5},{7,6},{8,11},{9,8},{10,9... | collective-permute-start | bytes 1572872 | tf_op jit(solution)/shard_map/ppermute | solution.py:391
  47.7 24.0 %collective-permute-start.5 = (bf16[512,512]{1,0:T(8,128)(2,1)S(1)}, bf16[512,512]{1,0:T(8,128)(2,1)S(1)}, u32[]{:S(2)}, u32[]{:S(2)}) collective-permute-start(bf16[512,512]{1,0:T(8,128)(2,1)S(1)} %get-tuple-element.63.refs_0_.refs_5_), channel_id=1, source_target_pairs={{0,1},{1,2},{2,3},{3,0},{4,5},{5,6},{6,7},{7,4},{8,9},{9,10},{10,1... | collective-permute-start | bytes 1572872 | tf_op jit(solution)/shard_map/ppermute | solution.py:390
  48.0 24.1 %collective-permute-start.4 = (bf16[512,512]{1,0:T(8,128)(2,1)S(1)}, bf16[512,512]{1,0:T(8,128)(2,1)S(1)}, u32[]{:S(2)}, u32[]{:S(2)}) collective-permute-start(bf16[512,512]{1,0:T(8,128)(2,1)S(1)} %get-tuple-element.63.refs_0_.refs_5_), channel_id=1, source_target_pairs={{0,3},{1,0},{2,1},{3,2},{4,7},{5,4},{6,5},{7,6},{8,11},{9,8},{10,9... | collective-permute-start | bytes 1572872 | tf_op jit(solution)/shard_map/ppermute | solution.py:391
  60.4 18.4 %copy-start.4 = (bf16[512,512]{1,0:T(8,128)(2,1)}, bf16[512,512]{1,0:T(8,128)(2,1)S(1)}, u32[]{:S(2)}) copy-start(bf16[512,512]{1,0:T(8,128)(2,1)S(1)} %collective-permute-done.1.refs_4_) | copy-start | bytes 1572868
  60.5 16.8 %collective-permute-start.2 = (bf16[256,512]{1,0:T(8,128)(2,1)S(1)}, bf16[256,512]{1,0:T(8,128)(2,1)S(1)}, u32[]{:S(2)}, u32[]{:S(2)}) collective-permute-start(bf16[256,512]{1,0:T(8,128)(2,1)S(1)} %slice.25), channel_id=1, source_target_pairs={{0,1},{1,2},{2,3},{3,0},{4,5},{5,6},{6,7},{7,4},{8,9},{9,10},{10,1... | collective-permute-start | bytes 786440 | tf_op jit(solution)/shard_map/ppermute | solution.py:392
  60.8 18.0 %copy-start.6 = (bf16[512,512]{1,0:T(8,128)(2,1)}, bf16[512,512]{1,0:T(8,128)(2,1)S(1)}, u32[]{:S(2)}) copy-start(bf16[512,512]{1,0:T(8,128)(2,1)S(1)} %collective-permute-done.refs_1_) | copy-start | bytes 1572868
  60.9 16.7 %collective-permute-start.3 = (bf16[256,512]{1,0:T(8,128)(2,1)S(1)}, bf16[256,512]{1,0:T(8,128)(2,1)S(1)}, u32[]{:S(2)}, u32[]{:S(2)}) collective-permute-start(bf16[256,512]{1,0:T(8,128)(2,1)S(1)} %slice.26), channel_id=1, source_target_pairs={{0,3},{1,0},{2,1},{3,2},{4,7},{5,4},{6,5},{7,6},{8,11},{9,8},{10,9... | collective-permute-start | bytes 786440 | tf_op jit(solution)/shard_map/ppermute | solution.py:393
  71.7 9.1 %copy-start.8 = (bf16[512,512]{1,0:T(8,128)(2,1)}, bf16[512,512]{1,0:T(8,128)(2,1)S(1)}, u32[]{:S(2)}) copy-start(bf16[512,512]{1,0:T(8,128)(2,1)S(1)} %collective-permute-done.5.refs_4_.refs_9_) | copy-start | bytes 1572868
  71.7 9.1 %collective-permute-start.6 = (bf16[256,512]{1,0:T(8,128)(2,1)S(1)}, bf16[256,512]{1,0:T(8,128)(2,1)S(1)}, u32[]{:S(2)}, u32[]{:S(2)}) collective-permute-start(bf16[256,512]{1,0:T(8,128)(2,1)S(1)} %slice.28), channel_id=1, source_target_pairs={{0,1},{1,2},{2,3},{3,0},{4,5},{5,6},{6,7},{7,4},{8,9},{9,10},{10,1... | collective-permute-start | bytes 786440 | tf_op jit(solution)/shard_map/ppermute | solution.py:392
  72.1 8.8 %copy-start.10 = (bf16[512,512]{1,0:T(8,128)(2,1)}, bf16[512,512]{1,0:T(8,128)(2,1)S(1)}, u32[]{:S(2)}) copy-start(bf16[512,512]{1,0:T(8,128)(2,1)S(1)} %collective-permute-done.4.refs_1_.refs_6_) | copy-start | bytes 1572868
  72.1 8.7 %collective-permute-start.7 = (bf16[256,512]{1,0:T(8,128)(2,1)S(1)}, bf16[256,512]{1,0:T(8,128)(2,1)S(1)}, u32[]{:S(2)}, u32[]{:S(2)}) collective-permute-start(bf16[256,512]{1,0:T(8,128)(2,1)S(1)} %slice.29), channel_id=1, source_target_pairs={{0,3},{1,0},{2,1},{3,2},{4,7},{5,4},{6,5},{7,6},{8,11},{9,8},{10,9... | collective-permute-start | bytes 786440 | tf_op jit(solution)/shard_map/ppermute | solution.py:393
  77.3 1.6 copy-start.16
  77.6 1.3 copy-start.18
  77.6 3.3 %copy-start.13 = (bf16[1,256,2048]{2,1,0:T(8,128)(2,1)S(1)}, bf16[1,256,2048]{2,1,0:T(8,128)(2,1)}, u32[]{:S(2)}) copy-start(bf16[1,256,2048]{2,1,0:T(8,128)(2,1)} %param.18) | copy-start | bytes 3145732
  80.8 3.0 %copy-start.20 = (bf16[256,512]{1,0:T(8,128)(2,1)}, bf16[256,512]{1,0:T(8,128)(2,1)S(1)}, u32[]{:S(2)}) copy-start(bf16[256,512]{1,0:T(8,128)(2,1)S(1)} %collective-permute-done.6.refs_2_.refs_7_) | copy-start | bytes 786436
  80.8 3.0 %copy-start.22 = (bf16[256,512]{1,0:T(8,128)(2,1)}, bf16[256,512]{1,0:T(8,128)(2,1)S(1)}, u32[]{:S(2)}) copy-start(bf16[256,512]{1,0:T(8,128)(2,1)S(1)} %collective-permute-done.7.refs_3_.refs_8_) | copy-start | bytes 786436
  83.8 21.4 %copy-start.31 = (bf16[512,256]{1,0:T(8,128)(2,1)}, bf16[512,256]{1,0:T(8,128)(2,1)S(1)}, u32[]{:S(2)}) copy-start(bf16[512,256]{1,0:T(8,128)(2,1)S(1)} %get-tuple-element.37.refs_10_) | copy-start | bytes 786436
  83.9 21.3 %copy-start.33 = (bf16[512,256]{1,0:T(8,128)(2,1)}, bf16[512,256]{1,0:T(8,128)(2,1)S(1)}, u32[]{:S(2)}) copy-start(bf16[512,256]{1,0:T(8,128)(2,1)S(1)} %get-tuple-element.38.refs_11_) | copy-start | bytes 786436
  83.9 21.3 %copy-start.35 = (bf16[512,256]{1,0:T(8,128)(2,1)}, bf16[512,256]{1,0:T(8,128)(2,1)S(1)}, u32[]{:S(2)}) copy-start(bf16[512,256]{1,0:T(8,128)(2,1)S(1)} %get-tuple-element.39.refs_12_) | copy-start | bytes 786436
  83.9 9.7 %collective-permute-start.12 = (bf16[256,512]{1,0:T(8,128)(2,1)S(1)}, bf16[256,512]{1,0:T(8,128)(2,1)S(1)}, u32[]{:S(2)}, u32[]{:S(2)}) collective-permute-start(bf16[256,512]{1,0:T(8,128)(2,1)S(1)} %get-tuple-element.51), channel_id=1, source_target_pairs={{0,3},{1,0},{2,1},{3,2},{4,7},{5,4},{6,5},{7,6},{8,11},{9,8},{10,9... | collective-permute-start | bytes 786440 | tf_op jit(solution)/shard_map/ppermute | solution.py:410
  86.9 10.6 %collective-permute-start.8 = (bf16[256,512]{1,0:T(8,128)(2,1)S(1)}, bf16[256,512]{1,0:T(8,128)(2,1)S(1)}, u32[]{:S(2)}, u32[]{:S(2)}) collective-permute-start(bf16[256,512]{1,0:T(8,128)(2,1)S(1)} %get-tuple-element.46), channel_id=1, source_target_pairs={{0,1},{1,2},{2,3},{3,0},{4,5},{5,6},{6,7},{7,4},{8,9},{9,10},{10,1... | collective-permute-start | bytes 786440 | tf_op jit(solution)/shard_map/ppermute | solution.py:409
  86.9 11.9 %collective-permute-start.10 = (bf16[256,512]{1,0:T(8,128)(2,1)S(1)}, bf16[256,512]{1,0:T(8,128)(2,1)S(1)}, u32[]{:S(2)}, u32[]{:S(2)}) collective-permute-start(bf16[256,512]{1,0:T(8,128)(2,1)S(1)} %get-tuple-element.47), channel_id=1, source_target_pairs={{0,3},{1,0},{2,1},{3,2},{4,7},{5,4},{6,5},{7,6},{8,11},{9,8},{10,9... | collective-permute-start | bytes 786440 | tf_op jit(solution)/shard_map/ppermute | solution.py:412
  90.1 12.1 %collective-permute-start.11 = (bf16[256,512]{1,0:T(8,128)(2,1)S(1)}, bf16[256,512]{1,0:T(8,128)(2,1)S(1)}, u32[]{:S(2)}, u32[]{:S(2)}) collective-permute-start(bf16[256,512]{1,0:T(8,128)(2,1)S(1)} %get-tuple-element.49), channel_id=1, source_target_pairs={{0,1},{1,2},{2,3},{3,0},{4,5},{5,6},{6,7},{7,4},{8,9},{9,10},{10,1... | collective-permute-start | bytes 786440 | tf_op jit(solution)/shard_map/ppermute | solution.py:411
  93.7 20.2 %copy-start.12 = (bf16[128,512]{1,0:T(8,128)(2,1)S(1)}, bf16[128,512]{1,0:T(8,128)(2,1)}, u32[]{:S(2)}) copy-start(bf16[128,512]{1,0:T(8,128)(2,1)} %refs_9_.1) | copy-start | bytes 393220
  93.7 26.7 %copy-start = (bf16[512,2048]{1,0:T(8,128)(2,1)S(1)}, bf16[512,2048]{1,0:T(8,128)(2,1)}, u32[]{:S(2)}) copy-start(bf16[512,2048]{1,0:T(8,128)(2,1)} %refs_11_.1) | copy-start | bytes 6291460
  93.7 26.7 %copy-start.30 = (f32[512]{0:T(512)S(1)}, f32[512]{0:T(512)}, u32[]{:S(2)}) copy-start(f32[512]{0:T(512)} %param.20) | copy-start | bytes 6148
  93.7 8.5 %collective-permute-start.13 = (bf16[256,512]{1,0:T(8,128)(2,1)S(1)}, bf16[256,512]{1,0:T(8,128)(2,1)S(1)}, u32[]{:S(2)}, u32[]{:S(2)}) collective-permute-start(bf16[256,512]{1,0:T(8,128)(2,1)S(1)} %add_convert_fusion), channel_id=1, source_target_pairs={{0,3},{1,0},{2,1},{3,2},{4,7},{5,4},{6,5},{7,6},{8,11},{9,8},{10,9... | collective-permute-start | bytes 786440 | tf_op jit(solution)/shard_map/ppermute | solution.py:414
  97.5 7.7 %collective-permute-start.9 = (bf16[256,512]{1,0:T(8,128)(2,1)S(1)}, bf16[256,512]{1,0:T(8,128)(2,1)S(1)}, u32[]{:S(2)}, u32[]{:S(2)}) collective-permute-start(bf16[256,512]{1,0:T(8,128)(2,1)S(1)} %add_convert_fusion.1), channel_id=1, source_target_pairs={{0,1},{1,2},{2,3},{3,0},{4,5},{5,6},{6,7},{7,4},{8,9},{9,10},{10,1... | collective-permute-start | bytes 786440 | tf_op jit(solution)/shard_map/ppermute | solution.py:413
  106.2 25.1 %all-to-all-start.1 = ((bf16[64,8,512]{2,1,0:T(8,128)(2,1)}), bf16[64,8,512]{2,1,0:T(8,128)(2,1)}, u32[]{:S(2)}, u32[]{:S(2)}) async-start(bf16[64,8,512]{2,1,0:T(8,128)(2,1)} %copy-done.3), calls=%async_computation.1 | async-start | bytes 1048576 | tf_op jit(solution)/shard_map/all_to_all | solution.py:380
  114.0 3.6 %collective-permute-start.14 = (f32[1,128]{1,0:T(1,128)S(1)}, f32[1,128]{1,0:T(1,128)S(1)}, u32[]{:S(2)}, u32[]{:S(2)}) collective-permute-start(f32[1,128]{1,0:T(1,128)S(1)} %bitcast.23), channel_id=1, source_target_pairs={{0,3},{1,0},{2,1},{3,2},{4,7},{5,4},{6,5},{7,6},{8,11},{9,8},{10,9... | collective-permute-start | bytes 1544 | tf_op jit(solution)/shard_map/ppermute | solution.py:399
  114.4 5.1 %collective-permute-start.15 = (f32[1,128]{1,0:T(1,128)S(1)}, f32[1,128]{1,0:T(1,128)S(1)}, u32[]{:S(2)}, u32[]{:S(2)}) collective-permute-start(f32[1,128]{1,0:T(1,128)S(1)} %bitcast.24), channel_id=1, source_target_pairs={{0,2},{1,3},{2,0},{3,1},{4,6},{5,7},{6,4},{7,5},{8,10},{9,11},{10,... | collective-permute-start | bytes 1544 | tf_op jit(solution)/shard_map/ppermute | solution.py:400
  115.2 5.1 %collective-permute-start.16 = (f32[1,128]{1,0:T(1,128)S(1)}, f32[1,128]{1,0:T(1,128)S(1)}, u32[]{:S(2)}, u32[]{:S(2)}) collective-permute-start(f32[1,128]{1,0:T(1,128)S(1)} %bitcast.25), channel_id=1, source_target_pairs={{0,1},{1,2},{2,3},{3,0},{4,5},{5,6},{6,7},{7,4},{8,9},{9,10},{10,1... | collective-permute-start | bytes 1544 | tf_op jit(solution)/shard_map/ppermute | solution.py:398
  121.9 8.5 %collective-permute-start.17 = (bf16[128,512]{1,0:T(8,128)(2,1)S(1)}, bf16[128,512]{1,0:T(8,128)(2,1)S(1)}, u32[]{:S(2)}, u32[]{:S(2)}) collective-permute-start(bf16[128,512]{1,0:T(8,128)(2,1)S(1)} %get-tuple-element.53), channel_id=1, source_target_pairs={{0,1},{1,2},{2,3},{3,0},{4,5},{5,6},{6,7},{7,4},{8,9},{9,10},{10,1... | collective-permute-start | bytes 393224 | tf_op jit(solution)/shard_map/ppermute | solution.py:449
  122.8 7.6 %collective-permute-start.18 = (bf16[128,512]{1,0:T(8,128)(2,1)S(1)}, bf16[128,512]{1,0:T(8,128)(2,1)S(1)}, u32[]{:S(2)}, u32[]{:S(2)}) collective-permute-start(bf16[128,512]{1,0:T(8,128)(2,1)S(1)} %get-tuple-element.54), channel_id=1, source_target_pairs={{0,2},{1,3},{2,0},{3,1},{4,6},{5,7},{6,4},{7,5},{8,10},{9,11},{10,... | collective-permute-start | bytes 393224 | tf_op jit(solution)/shard_map/ppermute | solution.py:450
  125.4 5.6 %collective-permute-start.19 = (bf16[128,512]{1,0:T(8,128)(2,1)S(1)}, bf16[128,512]{1,0:T(8,128)(2,1)S(1)}, u32[]{:S(2)}, u32[]{:S(2)}) collective-permute-start(bf16[128,512]{1,0:T(8,128)(2,1)S(1)} %get-tuple-element.55), channel_id=1, source_target_pairs={{0,3},{1,0},{2,1},{3,2},{4,7},{5,4},{6,5},{7,6},{8,11},{9,8},{10,9... | collective-permute-start | bytes 393224 | tf_op jit(solution)/shard_map/ppermute | solution.py:451
  125.8 17.4 %collective-permute-start.20 = (bf16[128,512]{1,0:T(8,128)(2,1)}, bf16[128,512]{1,0:T(8,128)(2,1)}, u32[]{:S(2)}, u32[]{:S(2)}) collective-permute-start(bf16[128,512]{1,0:T(8,128)(2,1)} %get-tuple-element.57), channel_id=1, source_target_pairs={{0,4},{4,0},{1,5},{5,1},{2,6},{6,2},{3,7},{7,3},{8,12},{12,8},{9,1... | collective-permute-start | bytes 393224 | tf_op jit(solution)/shard_map/ppermute | solution.py:453
  131.4 1.0 copy-start.14
  136.3 27.0 %all-to-all-start.2 = ((bf16[32,64,128]{2,1,0:T(8,128)(2,1)}), bf16[32,64,128]{2,1,0:T(8,128)(2,1)}, u32[]{:S(2)}, u32[]{:S(2)}) async-start(bf16[32,64,128]{2,1,0:T(8,128)(2,1)} %copy-done.15), calls=%async_computation.2 | async-start | bytes 1048576 | tf_op jit(solution)/shard_map/all_to_all | solution.py:380
  144.2 13.3 %collective-permute-start.21 = (bf16[2,128,512]{2,1,0:T(8,128)(2,1)S(1)}, bf16[2,128,512]{2,1,0:T(8,128)(2,1)}, u32[]{:S(2)}, u32[]{:S(2)}) collective-permute-start(bf16[2,128,512]{2,1,0:T(8,128)(2,1)S(1)} %pad_maximum_fusion.refs_0_), channel_id=1, source_target_pairs={{0,24},{8,0},{16,8},{24,16},{1,25},{9,1},{17,9},{25,17},{2,26},{10... | collective-permute-start | bytes 786440 | tf_op jit(solution)/shard_map/ppermute | solution.py:399
  144.6 18.7 %collective-permute-start.22 = (bf16[2,128,512]{2,1,0:T(8,128)(2,1)S(1)}, bf16[2,128,512]{2,1,0:T(8,128)(2,1)}, u32[]{:S(2)}, u32[]{:S(2)}) collective-permute-start(bf16[2,128,512]{2,1,0:T(8,128)(2,1)S(1)} %pad_maximum_fusion.refs_0_), channel_id=1, source_target_pairs={{0,16},{8,24},{16,0},{24,8},{1,17},{9,25},{17,1},{25,9},{2,18},{10... | collective-permute-start | bytes 786440 | tf_op jit(solution)/shard_map/ppermute | solution.py:400
  147.2 16.1 %collective-permute-start.23 = (bf16[2,128,512]{2,1,0:T(8,128)(2,1)S(1)}, bf16[2,128,512]{2,1,0:T(8,128)(2,1)}, u32[]{:S(2)}, u32[]{:S(2)}) collective-permute-start(bf16[2,128,512]{2,1,0:T(8,128)(2,1)S(1)} %pad_maximum_fusion.refs_0_), channel_id=1, source_target_pairs={{0,8},{8,16},{16,24},{24,0},{1,9},{9,17},{17,25},{25,1},{2,10},{10... | collective-permute-start | bytes 786440 | tf_op jit(solution)/shard_map/ppermute | solution.py:398
  167.1 25.2 %copy-start.17 = (bf16[256,512]{1,0:T(8,128)(2,1)S(1)}, bf16[256,512]{1,0:T(8,128)(2,1)}, u32[]{:S(2)}) copy-start(bf16[256,512]{1,0:T(8,128)(2,1)} %copy-done.16) | copy-start | bytes 786436
  167.1 34.1 %all-to-all-start.3 = ((bf16[8,32,512]{2,1,0:T(8,128)(2,1)}), bf16[8,32,512]{2,1,0:T(8,128)(2,1)}, u32[]{:S(2)}, u32[]{:S(2)}) async-start(bf16[8,32,512]{2,1,0:T(8,128)(2,1)} %shard_map.153), calls=%async_computation.3 | async-start | bytes 524288 | tf_op jit(solution)/shard_map/all_to_all | solution.py:380
  174.0 18.2 %copy-start.5 = (bf16[512,512]{1,0:T(8,128)(2,1)S(1)}, bf16[512,512]{1,0:T(8,128)(2,1)}, u32[]{:S(2)}) copy-start(bf16[512,512]{1,0:T(8,128)(2,1)} %copy-done.4) | copy-start | bytes 1572868
  174.0 18.2 %copy-start.7 = (bf16[512,512]{1,0:T(8,128)(2,1)S(1)}, bf16[512,512]{1,0:T(8,128)(2,1)}, u32[]{:S(2)}) copy-start(bf16[512,512]{1,0:T(8,128)(2,1)} %copy-done.6) | copy-start | bytes 1572868
  174.0 18.2 %copy-start.9 = (bf16[512,512]{1,0:T(8,128)(2,1)S(1)}, bf16[512,512]{1,0:T(8,128)(2,1)}, u32[]{:S(2)}) copy-start(bf16[512,512]{1,0:T(8,128)(2,1)} %copy-done.8) | copy-start | bytes 1572868
  174.1 18.2 %copy-start.11 = (bf16[512,512]{1,0:T(8,128)(2,1)S(1)}, bf16[512,512]{1,0:T(8,128)(2,1)}, u32[]{:S(2)}) copy-start(bf16[512,512]{1,0:T(8,128)(2,1)} %copy-done.10) | copy-start | bytes 1572868
  174.1 18.2 %copy-start.19 = (bf16[256,512]{1,0:T(8,128)(2,1)S(1)}, bf16[256,512]{1,0:T(8,128)(2,1)}, u32[]{:S(2)}) copy-start(bf16[256,512]{1,0:T(8,128)(2,1)} %copy-done.18) | copy-start | bytes 786436
  174.1 18.2 %copy-start.21 = (bf16[256,512]{1,0:T(8,128)(2,1)S(1)}, bf16[256,512]{1,0:T(8,128)(2,1)}, u32[]{:S(2)}) copy-start(bf16[256,512]{1,0:T(8,128)(2,1)} %copy-done.20) | copy-start | bytes 786436
  174.1 13.6 %collective-permute-start.24 = (bf16[128,512]{1,0:T(8,128)(2,1)}, bf16[128,512]{1,0:T(8,128)(2,1)S(1)}, u32[]{:S(2)}, u32[]{:S(2)}) collective-permute-start(bf16[128,512]{1,0:T(8,128)(2,1)} %copy-done.24), channel_id=1, source_target_pairs={{0,3},{1,0},{2,1},{3,2},{4,7},{5,4},{6,5},{7,6},{8,11},{9,8},{10,9... | collective-permute-start | bytes 393224 | tf_op jit(solution)/shard_map/ppermute | solution.py:399
  176.9 10.9 %collective-permute-start.25 = (bf16[128,512]{1,0:T(8,128)(2,1)}, bf16[128,512]{1,0:T(8,128)(2,1)S(1)}, u32[]{:S(2)}, u32[]{:S(2)}) collective-permute-start(bf16[128,512]{1,0:T(8,128)(2,1)} %copy-done.24), channel_id=1, source_target_pairs={{0,2},{1,3},{2,0},{3,1},{4,6},{5,7},{6,4},{7,5},{8,10},{9,11},{10,... | collective-permute-start | bytes 393224 | tf_op jit(solution)/shard_map/ppermute | solution.py:400
  177.7 10.0 %collective-permute-start.26 = (bf16[128,512]{1,0:T(8,128)(2,1)}, bf16[128,512]{1,0:T(8,128)(2,1)S(1)}, u32[]{:S(2)}, u32[]{:S(2)}) collective-permute-start(bf16[128,512]{1,0:T(8,128)(2,1)} %copy-done.24), channel_id=1, source_target_pairs={{0,1},{1,2},{2,3},{3,0},{4,5},{5,6},{6,7},{7,4},{8,9},{9,10},{10,1... | collective-permute-start | bytes 393224 | tf_op jit(solution)/shard_map/ppermute | solution.py:398
  178.6 4.0 %collective-permute-start.27 = (f32[1,128]{1,0:T(1,128)S(1)}, f32[1,128]{1,0:T(1,128)S(1)}, u32[]{:S(2)}, u32[]{:S(2)}) collective-permute-start(f32[1,128]{1,0:T(1,128)S(1)} %get-tuple-element.59.refs_4_), channel_id=1, source_target_pairs={{0,3},{1,0},{2,1},{3,2},{4,7},{5,4},{6,5},{7,6},{8,11},{9,8},{10,9... | collective-permute-start | bytes 1544 | tf_op jit(solution)/shard_map/ppermute | solution.py:399
  180.9 5.2 %collective-permute-start.28 = (f32[1,128]{1,0:T(1,128)S(1)}, f32[1,128]{1,0:T(1,128)S(1)}, u32[]{:S(2)}, u32[]{:S(2)}) collective-permute-start(f32[1,128]{1,0:T(1,128)S(1)} %get-tuple-element.59.refs_4_), channel_id=1, source_target_pairs={{0,2},{1,3},{2,0},{3,1},{4,6},{5,7},{6,4},{7,5},{8,10},{9,11},{10,... | collective-permute-start | bytes 1544 | tf_op jit(solution)/shard_map/ppermute | solution.py:400
  182.5 5.2 %collective-permute-start.29 = (f32[1,128]{1,0:T(1,128)S(1)}, f32[1,128]{1,0:T(1,128)S(1)}, u32[]{:S(2)}, u32[]{:S(2)}) collective-permute-start(f32[1,128]{1,0:T(1,128)S(1)} %get-tuple-element.59.refs_4_), channel_id=1, source_target_pairs={{0,1},{1,2},{2,3},{3,0},{4,5},{5,6},{6,7},{7,4},{8,9},{9,10},{10,1... | collective-permute-start | bytes 1544 | tf_op jit(solution)/shard_map/ppermute | solution.py:398
  190.3 9.2 %collective-permute-start.30 = (bf16[32,512]{1,0:T(8,128)(2,1)S(1)}, bf16[32,512]{1,0:T(8,128)(2,1)S(1)}, u32[]{:S(2)}, u32[]{:S(2)}) collective-permute-start(bf16[32,512]{1,0:T(8,128)(2,1)S(1)} %get-tuple-element.62), channel_id=1, source_target_pairs={{4,0},{8,4},{12,8},{16,12},{20,16},{24,20},{28,24},{32,28},{36,32}... | collective-permute-start | bytes 98312 | tf_op jit(solution)/shard_map/ppermute | solution.py:480
  192.3 1.0 copy-start.23
  193.3 0.9 copy-start.32
  194.2 0.9 copy-start.34
  195.2 0.9 copy-start.36
  196.1 3.4 %copy-start.27 = (f32[31,512]{1,0:T(8,128)S(1)}, f32[31,512]{1,0:T(8,128)}, u32[]{:S(2)}) copy-start(f32[31,512]{1,0:T(8,128)} %taps_ref.1) | copy-start | bytes 190468
  (7 other events, 5.6 us)
where the time goes:
time: 206 us; the launch traced here: 203 us
  starting transfers between devices  67.7 us (33%)
  waiting for transfers between devices  60.2 us (29%)
  blocking collectives  40.9 us (20%)
  Pallas kernels  19.4 us (9%)
  local copies, waits for them, and re-layouts  10.7 us (5%)
  other arithmetic  2.99 us (1%)
    all_to_all x1, blocking collectives, exchange(): return lax.all_to_all(x, axis, split_axis=0, concat_axis=0, tiled=True)  40.9 us
    all_to_all x3, starting transfers between devices, exchange(): return lax.all_to_all(x, axis, split_axis=0, concat_axis=0, tiled=True)  21.5 us
    ppermute x2, waiting for transfers between devices, ring_gather(): ahead = lax.ppermute(block, 'tp', AHEAD)  17.3 us
    unnamed x74, local copies, waits for them, and re-layouts  10.5 us
    ppermute x4, waiting for transfers between devices, ring_all(): behind = lax.ppermute(x, axis, BEHIND)  10.1 us
    ppermute x4, waiting for transfers between devices, ring_all(): across = lax.ppermute(x, axis, ACROSS)  9.36 us
    ppermute x2, starting transfers between devices, ring_gather(): across_b = lax.ppermute(behind[half:], 'tp', BEHIND)  6.07 us
    ppermute x4, starting transfers between devices, ring_all(): behind = lax.ppermute(x, axis, BEHIND)  5.89 us
  transfers between devices with their start and end apart: 34, of which 20 were waited for; matrix products, arithmetic and copies ran while one was open for 1% of the time, Pallas kernels for 5%

commit v1 on v0

--- a/solution.py
+++ b/solution.py
@@ -119,7 +119,6 @@
     wd_ref, pg_ref, pu_ref, wg_ref, wu_ref, act_ref, gp_ref, up_ref = refs[5:13]
     outs = refs[13:]
     width = blocks[0].shape[1]
-    half = blocks[0].shape[0] // 2
     act_grad = times(blocks, wd_ref, t_ref[0], width, 1)
     pre_gate = pg_ref[...]
     pre_up = pu_ref[...]
@@ -128,8 +127,13 @@
     act_ref[...] = (silu * pre_up).astype(bf16)
     gp_ref[...] = (act_grad * pre_up * sig * (1.0 + pre_gate * (1.0 - sig))).astype(bf16)
     up_ref[...] = (act_grad * silu).astype(bf16)
-    for i, k in enumerate((2, 3, 1, 0)):
-        cols = pl.ds(pl.multiple_of(block_of(t_ref[0], k) * width, width), width)
+    row_parts(t_ref[0], (2,), gp_ref, up_ref, wg_ref, wu_ref, outs)
+
+
+def row_parts(t, order, gp_ref, up_ref, wg_ref, wu_ref, outs):
+    half, width = outs[0].shape
+    for i, k in enumerate(order):
+        cols = pl.ds(pl.multiple_of(block_of(t, k) * width, width), width)
         back = dot(gp_ref[...], wg_ref[cols, :], 1, 1) + dot(up_ref[...], wu_ref[cols, :], 1, 1)
         outs[2 * i][...] = back[:half].astype(bf16)
         outs[2 * i + 1][...] = back[half:].astype(bf16)
@@ -142,11 +146,27 @@
     return pl.pallas_call(
         backward_kernel,
         in_specs=[SM] + [VM] * 10,
-        out_specs=[VM] * 11,
-        out_shape=[small] * 3 + [jax.ShapeDtypeStruct((half, width), bf16)] * 8,
-        compiler_params=PARAMS,
-        cost_estimate=cost(1_610_612_736, 9_000_000),
+        out_specs=[VM] * 5,
+        out_shape=[small] * 3 + [jax.ShapeDtypeStruct((half, width), bf16)] * 2,
+        compiler_params=PARAMS,
+        cost_estimate=cost(1_000_000_000, 6_000_000),
     )(tp, *c_blocks, w_down, pre_gate, pre_up, w_gate, w_up)
+
+
+def rest_kernel(t_ref, gp_ref, up_ref, wg_ref, wu_ref, *outs):
+    row_parts(t_ref[0], (3, 1, 0), gp_ref, up_ref, wg_ref, wu_ref, outs)
+
+
+def rest_backward(tp, gate_pre, up_pre, w_gate, w_up):
+    block = jax.ShapeDtypeStruct((gate_pre.shape[0] // 2, w_gate.shape[0] // 4), bf16)
+    return pl.pallas_call(
+        rest_kernel,
+        in_specs=[SM] + [VM] * 4,
+        out_specs=[VM] * 6,
+        out_shape=[block] * 6,
+        compiler_params=PARAMS,
+        cost_estimate=cost(800_000_000, 4_000_000),
+    )(tp, gate_pre, up_pre, w_gate, w_up)
 
 
 def weight_kernel(t_ref, *refs):
@@ -280,38 +300,26 @@
 
 
 def proj_kernel(at_ref, mix_ref, *refs):
-    acts, (out_ref, left_ref, right_ref, sems) = refs[:4], refs[4:]
+    acts, out_ref = refs[:4], refs[4]
     rows, tokens = 4 * mix_ref.shape[1], mix_ref.shape[2]
-    copies = []
+    acc = None
     for r in range(4):
-        for c in range(2):
-            core = at_ref[1] if c == 0 else 1 - at_ref[1]
-            g = 2 * block_of(at_ref[0], r) + core
-            to = right_ref.at[pl.ds(pl.multiple_of(g * tokens, tokens), tokens)]
-            copies.append(pltpu.make_async_copy(acts[r].at[c], to, sems.at[2 * r + c]))
-    for copy in copies:
-        copy.start()
-    for g in range(8):
-        left_ref[:, g * tokens : (g + 1) * tokens] = mix_ref[4 * g : 4 * g + 4].reshape(rows, tokens)
-    for copy in copies:
-        copy.wait()
-    out = dot(left_ref[...], right_ref[...], 1, 0)
-    out_ref[...] = out.astype(bf16).reshape(out_ref.shape)
+        first = 8 * block_of(at_ref[0], r)
+        own, other = first + 4 * at_ref[1], first + 4 - 4 * at_ref[1]
+        left = [mix_ref[pl.ds(g, 4)].reshape(rows, tokens) for g in (own, other)]
+        right = acts[r][...].reshape(2 * tokens, acts[r].shape[2])
+        part = dot(jnp.concatenate(left, axis=1), right, 1, 0)
+        acc = part if acc is None else acc + part
+    out_ref[...] = acc.astype(bf16).reshape(out_ref.shape)
 
 
 def proj_partial(at, mixed, acts):
-    tokens, width = acts[0].shape[1:]
-    rows = 4 * mixed.shape[1]
+    width = acts[0].shape[2]
     return pl.pallas_call(
         proj_kernel,
-        in_specs=[SM, VM] + [pl.BlockSpec(memory_space=pltpu.HBM)] * 4,
+        in_specs=[SM] + [VM] * 5,
         out_specs=VM,
-        out_shape=jax.ShapeDtypeStruct((8, rows // 8, width), bf16),
-        scratch_shapes=[
-            pltpu.VMEM((rows, 8 * tokens), bf16),
-            pltpu.VMEM((8 * tokens, width), bf16),
-            pltpu.SemaphoreType.DMA((8,)),
-        ],
+        out_shape=jax.ShapeDtypeStruct((8, mixed.shape[1] // 2, width), bf16),
         compiler_params=PARAMS,
         cost_estimate=cost(268_435_456, 2_000_000),
     )(at, mixed, *acts)
@@ -456,10 +464,11 @@
     x_blocks = ring_gather(x_slice)
     pre_gate, pre_up = expert_forward(tp, x_blocks, w_gate, w_up)
     c_blocks = ring_gather(cot_slice)
-    act, gate_pre, up_pre, *parts = expert_backward(
+    act, gate_pre, up_pre, *far = expert_backward(
         tp, c_blocks, w_down, pre_gate, pre_up, w_gate, w_up
     )
-    sums = ring_scatter(*parts)
+    rest = rest_backward(tp, gate_pre, up_pre, w_gate, w_up)
+    sums = ring_scatter(*far, *rest)
     back = sum_rows(sums, experts)
     returned = exchange(back, SP)
     gate_g, up_g, down_g = weight_grads(tp, x_blocks, c_blocks, act, gate_pre, up_pre)

time: 206 us -> 203 us (0.985)
  transfers between devices with their start and end apart: 34 -> 34, of which waited for: 20 -> 21; matrix products, arithmetic and copies ran while one was open for 1% -> 1% of each run, Pallas kernels for 5% -> 5%
where the time goes in v1:
time: 203 us; the launch traced here: 200 us
  starting transfers between devices  67.4 us (33%)
  waiting for transfers between devices  59.4 us (29%)
  blocking collectives  40.9 us (20%)
  Pallas kernels  17.6 us (9%)
  local copies, waits for them, and re-layouts  10.6 us (5%)
  other arithmetic  2.99 us (1%)
    all_to_all x1, blocking collectives, exchange(): return lax.all_to_all(x, axis, split_axis=0, concat_axis=0, tiled=True)  40.9 us
    all_to_all x3, starting transfers between devices, exchange(): return lax.all_to_all(x, axis, split_axis=0, concat_axis=0, tiled=True)  20.9 us
    ppermute x2, waiting for transfers between devices, ring_gather(): ahead = lax.ppermute(block, 'tp', AHEAD)  17.3 us
    unnamed x74, local copies, waits for them, and re-layouts  10.5 us
    ppermute x4, waiting for transfers between devices, ring_all(): behind = lax.ppermute(x, axis, BEHIND)  10.1 us
    ppermute x4, waiting for transfers between devices, ring_all(): across = lax.ppermute(x, axis, ACROSS)  9.35 us
    ppermute x2, starting transfers between devices, ring_gather(): across_b = lax.ppermute(behind[half:], 'tp', BEHIND)  6.07 us
    ppermute x4, starting transfers between devices, ring_all(): behind = lax.ppermute(x, axis, BEHIND)  5.89 us
  transfers between devices with their start and end apart: 34, of which 21 were waited for; matrix products, arithmetic and copies ran while one was open for 1% of the time, Pallas kernels for 5%

profile of v1, /device:TPU:8, one launch (start us, length us, event | category | flops | bytes accessed | tf_op | source)
XLA Modules:
  0.0 200.0 jit_solution(4921102964354338463)
XLA Ops:
  0.6 2.8 %shard_map.146 = (bf16[64,8,1024]{2,1,0:T(8,128)(2,1)}, bf16[512,128]{1,0:T(8,128)(2,1)}) custom-call(s32[1]{0:T(128)} %bitcast.tp_ref.t_ref, s32[2,128]{1,0:T(2,128)} %bitcast.30, f32[2,128]{1,0:T(2,128)} %bitcast.31, bf16[128,2048]{1,0:T(8,128)(2,1)} %x_ref.1, bf16[128,2048]{1,0:T(8,128)(2,1)} %cot_ref.3), custom_call_target="tpu_custom_call" | custom-call | flops 400000000 | bytes 3000000 | tf_op jit(solution)/shard_map/pallas_call | solution.py:67
  3.4 40.9 %all_to_all.20 = bf16[64,8,1024]{2,1,0:T(8,128)(2,1)S(1)} all-to-all(bf16[64,8,1024]{2,1,0:T(8,128)(2,1)} %get-tuple-element.34), channel_id=1, replica_groups=mesh['z'=8,'y'=4,'core'=2,'tp'=4] {'z','y','core'}, dimensions={0} | all-to-all | bytes 2097152 | tf_op jit(solution)/shard_map/all_to_all | solution.py:388
  44.4 1.6 collective-permute-start.1
  45.9 1.7 collective-permute-start
  48.0 3.0 %collective-permute-start.4 = (bf16[512,512]{1,0:T(8,128)(2,1)S(1)}, bf16[512,512]{1,0:T(8,128)(2,1)S(1)}, u32[]{:S(2)}, u32[]{:S(2)}) collective-permute-start(bf16[512,512]{1,0:T(8,128)(2,1)S(1)} %get-tuple-element.63.refs_0_.refs_5_), channel_id=1, source_target_pairs={{0,3},{1,0},{2,1},{3,2},{4,7},{5,4},{6,5},{7,6},{8,11},{9,8},{10,9... | collective-permute-start | bytes 1572872 | tf_op jit(solution)/shard_map/ppermute | solution.py:399
  50.9 9.5 %collective-permute-done.1.refs_4_ = bf16[512,512]{1,0:T(8,128)(2,1)S(1)} collective-permute-done((bf16[512,512]{1,0:T(8,128)(2,1)S(1)}, bf16[512,512]{1,0:T(8,128)(2,1)S(1)}, u32[]{:S(2)}, u32[]{:S(2)}) %collective-permute-start.1) | collective-permute-done | bytes 524320 | tf_op jit(solution)/shard_map/ppermute | solution.py:398
  60.9 3.0 %collective-permute-start.3 = (bf16[256,512]{1,0:T(8,128)(2,1)S(1)}, bf16[256,512]{1,0:T(8,128)(2,1)S(1)}, u32[]{:S(2)}, u32[]{:S(2)}) collective-permute-start(bf16[256,512]{1,0:T(8,128)(2,1)S(1)} %slice.26), channel_id=1, source_target_pairs={{0,3},{1,0},{2,1},{3,2},{4,7},{5,4},{6,5},{7,6},{8,11},{9,8},{10,9... | collective-permute-start | bytes 786440 | tf_op jit(solution)/shard_map/ppermute | solution.py:401
  63.9 7.8 %collective-permute-done.5.refs_4_.refs_9_ = bf16[512,512]{1,0:T(8,128)(2,1)S(1)} collective-permute-done((bf16[512,512]{1,0:T(8,128)(2,1)S(1)}, bf16[512,512]{1,0:T(8,128)(2,1)S(1)}, u32[]{:S(2)}, u32[]{:S(2)}) %collective-permute-start.5) | collective-permute-done | bytes 524320 | tf_op jit(solution)/shard_map/ppermute | solution.py:398
  72.1 3.0 %collective-permute-start.7 = (bf16[256,512]{1,0:T(8,128)(2,1)S(1)}, bf16[256,512]{1,0:T(8,128)(2,1)S(1)}, u32[]{:S(2)}, u32[]{:S(2)}) collective-permute-start(bf16[256,512]{1,0:T(8,128)(2,1)S(1)} %slice.29), channel_id=1, source_target_pairs={{0,3},{1,0},{2,1},{3,2},{4,7},{5,4},{6,5},{7,6},{8,11},{9,8},{10,9... | collective-permute-start | bytes 786440 | tf_op jit(solution)/shard_map/ppermute | solution.py:401
  75.1 2.2 %collective-permute-done.2.refs_2_ = bf16[256,512]{1,0:T(8,128)(2,1)S(1)} collective-permute-done((bf16[256,512]{1,0:T(8,128)(2,1)S(1)}, bf16[256,512]{1,0:T(8,128)(2,1)S(1)}, u32[]{:S(2)}, u32[]{:S(2)}) %collective-permute-start.2) | collective-permute-done | bytes 262176 | tf_op jit(solution)/shard_map/ppermute | solution.py:400
  77.6 1.3 shard_map.147
  78.9 1.9 collective-permute-done.6.refs_2_.refs_7_
  80.8 1.6 shard_map.148
  82.5 3.0 %collective-permute-start.12 = (bf16[256,512]{1,0:T(8,128)(2,1)S(1)}, bf16[256,512]{1,0:T(8,128)(2,1)S(1)}, u32[]{:S(2)}, u32[]{:S(2)}) collective-permute-start(bf16[256,512]{1,0:T(8,128)(2,1)S(1)} %get-tuple-element.51), channel_id=1, source_target_pairs={{0,3},{1,0},{2,1},{3,2},{4,7},{5,4},{6,5},{7,6},{8,11},{9,8},{10,9... | collective-permute-start | bytes 786440 | tf_op jit(solution)/shard_map/ppermute | solution.py:418
  85.5 1.0 shard_map.150
  86.5 3.5 %collective-permute-start.10 = (bf16[256,512]{1,0:T(8,128)(2,1)S(1)}, bf16[256,512]{1,0:T(8,128)(2,1)S(1)}, u32[]{:S(2)}, u32[]{:S(2)}) collective-permute-start(bf16[256,512]{1,0:T(8,128)(2,1)S(1)} %get-tuple-element.47), channel_id=1, source_target_pairs={{0,3},{1,0},{2,1},{3,2},{4,7},{5,4},{6,5},{7,6},{8,11},{9,8},{10,9... | collective-permute-start | bytes 786440 | tf_op jit(solution)/shard_map/ppermute | solution.py:420
  90.0 1.5 collective-permute-done.12
  91.6 3.8 %collective-permute-start.13 = (bf16[256,512]{1,0:T(8,128)(2,1)S(1)}, bf16[256,512]{1,0:T(8,128)(2,1)S(1)}, u32[]{:S(2)}, u32[]{:S(2)}) collective-permute-start(bf16[256,512]{1,0:T(8,128)(2,1)S(1)} %add_convert_fusion), channel_id=1, source_target_pairs={{0,3},{1,0},{2,1},{3,2},{4,7},{5,4},{6,5},{7,6},{8,11},{9,8},{10,9... | collective-permute-start | bytes 786440 | tf_op jit(solution)/shard_map/ppermute | solution.py:422
  95.7 1.5 collective-permute-done.10.pa_ref
  97.1 4.0 %collective-permute-done.11.nb_ref = bf16[256,512]{1,0:T(8,128)(2,1)S(1)} collective-permute-done((bf16[256,512]{1,0:T(8,128)(2,1)S(1)}, bf16[256,512]{1,0:T(8,128)(2,1)S(1)}, u32[]{:S(2)}, u32[]{:S(2)}) %collective-permute-start.11) | collective-permute-done | bytes 262176 | tf_op jit(solution)/shard_map/ppermute | solution.py:419
  101.1 3.2 %collective-permute-done.9.na_ref = bf16[256,512]{1,0:T(8,128)(2,1)S(1)} collective-permute-done((bf16[256,512]{1,0:T(8,128)(2,1)S(1)}, bf16[256,512]{1,0:T(8,128)(2,1)S(1)}, u32[]{:S(2)}, u32[]{:S(2)}) %collective-permute-start.9) | collective-permute-done | bytes 262176 | tf_op jit(solution)/shard_map/ppermute | solution.py:421
  104.5 0.8 copy-done.3
  105.3 7.2 %all-to-all-start.1 = ((bf16[64,8,512]{2,1,0:T(8,128)(2,1)}), bf16[64,8,512]{2,1,0:T(8,128)(2,1)}, u32[]{:S(2)}, u32[]{:S(2)}) async-start(bf16[64,8,512]{2,1,0:T(8,128)(2,1)} %copy-done.3), calls=%async_computation.1 | async-start | bytes 1048576 | tf_op jit(solution)/shard_map/all_to_all | solution.py:388
  113.0 0.9 collective-permute-start.15
  113.8 0.9 collective-permute-start.16
  114.7 1.5 collective-permute-done.14.p1_ref
  116.3 1.8 collective-permute-done.15.p2_ref
  118.1 0.9 collective-permute-done.16.p3_ref
  119.0 0.9 shard_map.152
  120.5 0.9 collective-permute-start.17
  121.4 2.6 %collective-permute-start.18 = (bf16[128,512]{1,0:T(8,128)(2,1)S(1)}, bf16[128,512]{1,0:T(8,128)(2,1)S(1)}, u32[]{:S(2)}, u32[]{:S(2)}) collective-permute-start(bf16[128,512]{1,0:T(8,128)(2,1)S(1)} %get-tuple-element.54), channel_id=1, source_target_pairs={{0,2},{1,3},{2,0},{3,1},{4,6},{5,7},{6,4},{7,5},{8,10},{9,11},{10,... | collective-permute-start | bytes 393224 | tf_op jit(solution)/shard_map/ppermute | solution.py:458
  124.4 4.7 %collective-permute-done.17 = bf16[128,512]{1,0:T(8,128)(2,1)S(1)} collective-permute-done((bf16[128,512]{1,0:T(8,128)(2,1)S(1)}, bf16[128,512]{1,0:T(8,128)(2,1)S(1)}, u32[]{:S(2)}, u32[]{:S(2)}) %collective-permute-start.17) | collective-permute-done | bytes 131104 | tf_op jit(solution)/shard_map/ppermute | solution.py:457
  130.0 1.0 copy-done.14
  131.0 0.9 copy-done.26
  131.9 1.5 shard_map.153
  133.4 0.8 copy-done.15
  134.2 0.7 copy-done.24
  134.9 6.9 %all-to-all-start.2 = ((bf16[32,64,128]{2,1,0:T(8,128)(2,1)}), bf16[32,64,128]{2,1,0:T(8,128)(2,1)}, u32[]{:S(2)}, u32[]{:S(2)}) async-start(bf16[32,64,128]{2,1,0:T(8,128)(2,1)} %copy-done.15), calls=%async_computation.2 | async-start | bytes 1048576 | tf_op jit(solution)/shard_map/all_to_all | solution.py:388
  141.8 1.0 pad_maximum_fusion.refs_0_
  143.1 2.6 %collective-permute-start.22 = (bf16[2,128,512]{2,1,0:T(8,128)(2,1)S(1)}, bf16[2,128,512]{2,1,0:T(8,128)(2,1)}, u32[]{:S(2)}, u32[]{:S(2)}) collective-permute-start(bf16[2,128,512]{2,1,0:T(8,128)(2,1)S(1)} %pad_maximum_fusion.refs_0_), channel_id=1, source_target_pairs={{0,16},{8,24},{16,0},{24,8},{1,17},{9,25},{17,1},{25,9},{2,18},{10... | collective-permute-start | bytes 786440 | tf_op jit(solution)/shard_map/ppermute | solution.py:408
  145.8 1.8 collective-permute-start.23
  147.7 8.5 %collective-permute-done.21.refs_1_ = bf16[2,128,512]{2,1,0:T(8,128)(2,1)} collective-permute-done((bf16[2,128,512]{2,1,0:T(8,128)(2,1)S(1)}, bf16[2,128,512]{2,1,0:T(8,128)(2,1)}, u32[]{:S(2)}, u32[]{:S(2)}) %collective-permute-start.21) | collective-permute-done | bytes 262176 | tf_op jit(solution)/shard_map/ppermute | solution.py:407
  156.1 5.7 %collective-permute-done.22.refs_2_ = bf16[2,128,512]{2,1,0:T(8,128)(2,1)} collective-permute-done((bf16[2,128,512]{2,1,0:T(8,128)(2,1)S(1)}, bf16[2,128,512]{2,1,0:T(8,128)(2,1)}, u32[]{:S(2)}, u32[]{:S(2)}) %collective-permute-start.22) | collective-permute-done | bytes 262176 | tf_op jit(solution)/shard_map/ppermute | solution.py:408
  161.9 2.4 %shard_map.154 = bf16[8,32,512]{2,1,0:T(8,128)(2,1)} custom-call(s32[2]{0:T(128)S(1)} %pad_add_fusion.at_ref, bf16[32,64,128]{2,1,0:T(8,128)(2,1)} %all-to-all-done.2.mix_ref, bf16[2,128,512]{2,1,0:T(8,128)(2,1)S(1)} %pad_maximum_fusion.refs_0_, bf16[2,128,512]{2,1,0:T(8,128)(2,1)} %collective-permute-done.21.refs_1_, ...), custom_call_target="tpu_custom_call" | custom-call | flops 268435456 | bytes 2000000 | tf_op jit(solution)/shard_map/pallas_call | solution.py:318
  164.3 6.9 %all-to-all-start.3 = ((bf16[8,32,512]{2,1,0:T(8,128)(2,1)}), bf16[8,32,512]{2,1,0:T(8,128)(2,1)}, u32[]{:S(2)}, u32[]{:S(2)}) async-start(bf16[8,32,512]{2,1,0:T(8,128)(2,1)} %shard_map.154), calls=%async_computation.3 | async-start | bytes 524288 | tf_op jit(solution)/shard_map/all_to_all | solution.py:388
  171.2 2.8 %collective-permute-start.24 = (bf16[128,512]{1,0:T(8,128)(2,1)}, bf16[128,512]{1,0:T(8,128)(2,1)S(1)}, u32[]{:S(2)}, u32[]{:S(2)}) collective-permute-start(bf16[128,512]{1,0:T(8,128)(2,1)} %copy-done.24), channel_id=1, source_target_pairs={{0,3},{1,0},{2,1},{3,2},{4,7},{5,4},{6,5},{7,6},{8,11},{9,8},{10,9... | collective-permute-start | bytes 393224 | tf_op jit(solution)/shard_map/ppermute | solution.py:407
  174.0 0.8 collective-permute-start.25
  174.9 0.9 collective-permute-start.26
  175.7 2.4 %collective-permute-start.27 = (f32[1,128]{1,0:T(1,128)S(1)}, f32[1,128]{1,0:T(1,128)S(1)}, u32[]{:S(2)}, u32[]{:S(2)}) collective-permute-start(f32[1,128]{1,0:T(1,128)S(1)} %get-tuple-element.59.refs_4_), channel_id=1, source_target_pairs={{0,3},{1,0},{2,1},{3,2},{4,7},{5,4},{6,5},{7,6},{8,11},{9,8},{10,9... | collective-permute-start | bytes 1544 | tf_op jit(solution)/shard_map/ppermute | solution.py:407
  178.1 1.5 collective-permute-start.28
  179.7 1.8 collective-permute-start.29
  181.4 1.8 collective-permute-done.28.refs_6_
  183.2 1.6 collective-permute-done.29.refs_7_
  184.9 0.9 copy-done.25
  185.8 0.8 copy-done.29
  186.6 0.8 shard_map.155
  187.5 1.9 collective-permute-start.30
  189.5 0.9 copy-done.23
  190.4 0.9 copy-done.32
  191.4 0.9 copy-done.34
  192.3 0.9 copy-done.36
  193.3 3.4 %shard_map.149 = (bf16[2048,256]{1,0:T(8,128)(2,1)}, bf16[2048,256]{1,0:T(8,128)(2,1)}, bf16[256,2048]{1,0:T(8,128)(2,1)}) custom-call(s32[1]{0:T(128)} %bitcast.tp_ref.t_ref, bf16[512,512]{1,0:T(8,128)(2,1)S(1)} %get-tuple-element.64.refs_0_, bf16[512,512]{1,0:T(8,128)(2,1)S(1)} %copy-done.7, bf16[256,512]{1,0:T(8,128)(2,1)S(1)} %copy-done.17, ...), custom_call_target="tpu_custom_call" | custom-call | flops 1610612736 | bytes 8000000 | tf_op jit(solution)/shard_map/pallas_call | solution.py:192
  196.6 1.7 shard_map.156
  198.4 1.6 convert_reduce_fusion
  (102 shorter events, 5.0 us)
Async XLA Ops:
  44.3 33.3 %copy-start.1 = (bf16[1,2048,256]{2,1,0:T(8,128)(2,1)S(1)}, bf16[1,2048,256]{2,1,0:T(8,128)(2,1)}, u32[]{:S(2)}) copy-start(bf16[1,2048,256]{2,1,0:T(8,128)(2,1)} %param.16) | copy-start | bytes 3145732
  44.3 33.3 %copy-start.2 = (bf16[1,2048,256]{2,1,0:T(8,128)(2,1)S(1)}, bf16[1,2048,256]{2,1,0:T(8,128)(2,1)}, u32[]{:S(2)}) copy-start(bf16[1,2048,256]{2,1,0:T(8,128)(2,1)} %param.17) | copy-start | bytes 3145732
  44.4 16.1 %collective-permute-start.1 = (bf16[512,512]{1,0:T(8,128)(2,1)S(1)}, bf16[512,512]{1,0:T(8,128)(2,1)S(1)}, u32[]{:S(2)}, u32[]{:S(2)}) collective-permute-start(bf16[512,512]{1,0:T(8,128)(2,1)S(1)} %get-tuple-element.64.refs_0_), channel_id=1, source_target_pairs={{0,1},{1,2},{2,3},{3,0},{4,5},{5,6},{6,7},{7,4},{8,9},{9,10},{10,1... | collective-permute-start | bytes 1572872 | tf_op jit(solution)/shard_map/ppermute | solution.py:398
  45.9 14.9 %collective-permute-start = (bf16[512,512]{1,0:T(8,128)(2,1)S(1)}, bf16[512,512]{1,0:T(8,128)(2,1)S(1)}, u32[]{:S(2)}, u32[]{:S(2)}) collective-permute-start(bf16[512,512]{1,0:T(8,128)(2,1)S(1)} %get-tuple-element.64.refs_0_), channel_id=1, source_target_pairs={{0,3},{1,0},{2,1},{3,2},{4,7},{5,4},{6,5},{7,6},{8,11},{9,8},{10,9... | collective-permute-start | bytes 1572872 | tf_op jit(solution)/shard_map/ppermute | solution.py:399
  47.7 24.0 %collective-permute-start.5 = (bf16[512,512]{1,0:T(8,128)(2,1)S(1)}, bf16[512,512]{1,0:T(8,128)(2,1)S(1)}, u32[]{:S(2)}, u32[]{:S(2)}) collective-permute-start(bf16[512,512]{1,0:T(8,128)(2,1)S(1)} %get-tuple-element.63.refs_0_.refs_5_), channel_id=1, source_target_pairs={{0,1},{1,2},{2,3},{3,0},{4,5},{5,6},{6,7},{7,4},{8,9},{9,10},{10,1... | collective-permute-start | bytes 1572872 | tf_op jit(solution)/shard_map/ppermute | solution.py:398
  48.0 24.1 %collective-permute-start.4 = (bf16[512,512]{1,0:T(8,128)(2,1)S(1)}, bf16[512,512]{1,0:T(8,128)(2,1)S(1)}, u32[]{:S(2)}, u32[]{:S(2)}) collective-permute-start(bf16[512,512]{1,0:T(8,128)(2,1)S(1)} %get-tuple-element.63.refs_0_.refs_5_), channel_id=1, source_target_pairs={{0,3},{1,0},{2,1},{3,2},{4,7},{5,4},{6,5},{7,6},{8,11},{9,8},{10,9... | collective-permute-start | bytes 1572872 | tf_op jit(solution)/shard_map/ppermute | solution.py:399
  60.4 18.4 %copy-start.4 = (bf16[512,512]{1,0:T(8,128)(2,1)}, bf16[512,512]{1,0:T(8,128)(2,1)S(1)}, u32[]{:S(2)}) copy-start(bf16[512,512]{1,0:T(8,128)(2,1)S(1)} %collective-permute-done.1.refs_4_) | copy-start | bytes 1572868
  60.5 16.8 %collective-permute-start.2 = (bf16[256,512]{1,0:T(8,128)(2,1)S(1)}, bf16[256,512]{1,0:T(8,128)(2,1)S(1)}, u32[]{:S(2)}, u32[]{:S(2)}) collective-permute-start(bf16[256,512]{1,0:T(8,128)(2,1)S(1)} %slice.25), channel_id=1, source_target_pairs={{0,1},{1,2},{2,3},{3,0},{4,5},{5,6},{6,7},{7,4},{8,9},{9,10},{10,1... | collective-permute-start | bytes 786440 | tf_op jit(solution)/shard_map/ppermute | solution.py:400
  60.8 18.0 %copy-start.6 = (bf16[512,512]{1,0:T(8,128)(2,1)}, bf16[512,512]{1,0:T(8,128)(2,1)S(1)}, u32[]{:S(2)}) copy-start(bf16[512,512]{1,0:T(8,128)(2,1)S(1)} %collective-permute-done.refs_1_) | copy-start | bytes 1572868
  60.9 16.7 %collective-permute-start.3 = (bf16[256,512]{1,0:T(8,128)(2,1)S(1)}, bf16[256,512]{1,0:T(8,128)(2,1)S(1)}, u32[]{:S(2)}, u32[]{:S(2)}) collective-permute-start(bf16[256,512]{1,0:T(8,128)(2,1)S(1)} %slice.26), channel_id=1, source_target_pairs={{0,3},{1,0},{2,1},{3,2},{4,7},{5,4},{6,5},{7,6},{8,11},{9,8},{10,9... | collective-permute-start | bytes 786440 | tf_op jit(solution)/shard_map/ppermute | solution.py:401
  71.7 9.1 %copy-start.8 = (bf16[512,512]{1,0:T(8,128)(2,1)}, bf16[512,512]{1,0:T(8,128)(2,1)S(1)}, u32[]{:S(2)}) copy-start(bf16[512,512]{1,0:T(8,128)(2,1)S(1)} %collective-permute-done.5.refs_4_.refs_9_) | copy-start | bytes 1572868
  71.7 9.1 %collective-permute-start.6 = (bf16[256,512]{1,0:T(8,128)(2,1)S(1)}, bf16[256,512]{1,0:T(8,128)(2,1)S(1)}, u32[]{:S(2)}, u32[]{:S(2)}) collective-permute-start(bf16[256,512]{1,0:T(8,128)(2,1)S(1)} %slice.28), channel_id=1, source_target_pairs={{0,1},{1,2},{2,3},{3,0},{4,5},{5,6},{6,7},{7,4},{8,9},{9,10},{10,1... | collective-permute-start | bytes 786440 | tf_op jit(solution)/shard_map/ppermute | solution.py:400
  72.1 8.8 %copy-start.10 = (bf16[512,512]{1,0:T(8,128)(2,1)}, bf16[512,512]{1,0:T(8,128)(2,1)S(1)}, u32[]{:S(2)}) copy-start(bf16[512,512]{1,0:T(8,128)(2,1)S(1)} %collective-permute-done.4.refs_1_.refs_6_) | copy-start | bytes 1572868
  72.1 8.7 %collective-permute-start.7 = (bf16[256,512]{1,0:T(8,128)(2,1)S(1)}, bf16[256,512]{1,0:T(8,128)(2,1)S(1)}, u32[]{:S(2)}, u32[]{:S(2)}) collective-permute-start(bf16[256,512]{1,0:T(8,128)(2,1)S(1)} %slice.29), channel_id=1, source_target_pairs={{0,3},{1,0},{2,1},{3,2},{4,7},{5,4},{6,5},{7,6},{8,11},{9,8},{10,9... | collective-permute-start | bytes 786440 | tf_op jit(solution)/shard_map/ppermute | solution.py:401
  77.3 1.6 copy-start.16
  77.6 1.3 copy-start.18
  77.6 3.3 %copy-start.13 = (bf16[1,256,2048]{2,1,0:T(8,128)(2,1)S(1)}, bf16[1,256,2048]{2,1,0:T(8,128)(2,1)}, u32[]{:S(2)}) copy-start(bf16[1,256,2048]{2,1,0:T(8,128)(2,1)} %param.18) | copy-start | bytes 3145732
  80.8 1.6 copy-start.20
  80.8 1.6 copy-start.22
  82.5 13.1 %copy-start.31 = (bf16[512,256]{1,0:T(8,128)(2,1)}, bf16[512,256]{1,0:T(8,128)(2,1)S(1)}, u32[]{:S(2)}) copy-start(bf16[512,256]{1,0:T(8,128)(2,1)S(1)} %get-tuple-element.37.refs_10_) | copy-start | bytes 786436
  82.5 13.1 %copy-start.33 = (bf16[512,256]{1,0:T(8,128)(2,1)}, bf16[512,256]{1,0:T(8,128)(2,1)S(1)}, u32[]{:S(2)}) copy-start(bf16[512,256]{1,0:T(8,128)(2,1)S(1)} %get-tuple-element.38.refs_11_.gp_ref) | copy-start | bytes 786436
  82.5 13.1 %copy-start.35 = (bf16[512,256]{1,0:T(8,128)(2,1)}, bf16[512,256]{1,0:T(8,128)(2,1)S(1)}, u32[]{:S(2)}) copy-start(bf16[512,256]{1,0:T(8,128)(2,1)S(1)} %get-tuple-element.39.refs_12_.up_ref) | copy-start | bytes 786436
  82.5 9.0 %collective-permute-start.12 = (bf16[256,512]{1,0:T(8,128)(2,1)S(1)}, bf16[256,512]{1,0:T(8,128)(2,1)S(1)}, u32[]{:S(2)}, u32[]{:S(2)}) collective-permute-start(bf16[256,512]{1,0:T(8,128)(2,1)S(1)} %get-tuple-element.51), channel_id=1, source_target_pairs={{0,3},{1,0},{2,1},{3,2},{4,7},{5,4},{6,5},{7,6},{8,11},{9,8},{10,9... | collective-permute-start | bytes 786440 | tf_op jit(solution)/shard_map/ppermute | solution.py:418
  85.5 10.0 %collective-permute-start.8 = (bf16[256,512]{1,0:T(8,128)(2,1)S(1)}, bf16[256,512]{1,0:T(8,128)(2,1)S(1)}, u32[]{:S(2)}, u32[]{:S(2)}) collective-permute-start(bf16[256,512]{1,0:T(8,128)(2,1)S(1)} %get-tuple-element.46), channel_id=1, source_target_pairs={{0,1},{1,2},{2,3},{3,0},{4,5},{5,6},{6,7},{7,4},{8,9},{9,10},{10,1... | collective-permute-start | bytes 786440 | tf_op jit(solution)/shard_map/ppermute | solution.py:417
  86.5 10.6 %collective-permute-start.10 = (bf16[256,512]{1,0:T(8,128)(2,1)S(1)}, bf16[256,512]{1,0:T(8,128)(2,1)S(1)}, u32[]{:S(2)}, u32[]{:S(2)}) collective-permute-start(bf16[256,512]{1,0:T(8,128)(2,1)S(1)} %get-tuple-element.47), channel_id=1, source_target_pairs={{0,3},{1,0},{2,1},{3,2},{4,7},{5,4},{6,5},{7,6},{8,11},{9,8},{10,9... | collective-permute-start | bytes 786440 | tf_op jit(solution)/shard_map/ppermute | solution.py:420
  90.0 11.1 %collective-permute-start.11 = (bf16[256,512]{1,0:T(8,128)(2,1)S(1)}, bf16[256,512]{1,0:T(8,128)(2,1)S(1)}, u32[]{:S(2)}, u32[]{:S(2)}) collective-permute-start(bf16[256,512]{1,0:T(8,128)(2,1)S(1)} %get-tuple-element.49), channel_id=1, source_target_pairs={{0,1},{1,2},{2,3},{3,0},{4,5},{5,6},{6,7},{7,4},{8,9},{9,10},{10,1... | collective-permute-start | bytes 786440 | tf_op jit(solution)/shard_map/ppermute | solution.py:419
  91.6 20.9 %copy-start.12 = (bf16[128,512]{1,0:T(8,128)(2,1)S(1)}, bf16[128,512]{1,0:T(8,128)(2,1)}, u32[]{:S(2)}) copy-start(bf16[128,512]{1,0:T(8,128)(2,1)} %refs_9_.1) | copy-start | bytes 393220
  91.6 27.4 %copy-start = (bf16[512,2048]{1,0:T(8,128)(2,1)S(1)}, bf16[512,2048]{1,0:T(8,128)(2,1)}, u32[]{:S(2)}) copy-start(bf16[512,2048]{1,0:T(8,128)(2,1)} %refs_11_.1) | copy-start | bytes 6291460
  91.6 27.4 %copy-start.30 = (f32[512]{0:T(512)S(1)}, f32[512]{0:T(512)}, u32[]{:S(2)}) copy-start(f32[512]{0:T(512)} %param.20) | copy-start | bytes 6148
  91.6 9.5 %collective-permute-start.13 = (bf16[256,512]{1,0:T(8,128)(2,1)S(1)}, bf16[256,512]{1,0:T(8,128)(2,1)S(1)}, u32[]{:S(2)}, u32[]{:S(2)}) collective-permute-start(bf16[256,512]{1,0:T(8,128)(2,1)S(1)} %add_convert_fusion), channel_id=1, source_target_pairs={{0,3},{1,0},{2,1},{3,2},{4,7},{5,4},{6,5},{7,6},{8,11},{9,8},{10,9... | collective-permute-start | bytes 786440 | tf_op jit(solution)/shard_map/ppermute | solution.py:422
  95.6 8.8 %collective-permute-start.9 = (bf16[256,512]{1,0:T(8,128)(2,1)S(1)}, bf16[256,512]{1,0:T(8,128)(2,1)S(1)}, u32[]{:S(2)}, u32[]{:S(2)}) collective-permute-start(bf16[256,512]{1,0:T(8,128)(2,1)S(1)} %add_convert_fusion.1), channel_id=1, source_target_pairs={{0,1},{1,2},{2,3},{3,0},{4,5},{5,6},{6,7},{7,4},{8,9},{9,10},{10,1... | collective-permute-start | bytes 786440 | tf_op jit(solution)/shard_map/ppermute | solution.py:421
  105.3 24.6 %all-to-all-start.1 = ((bf16[64,8,512]{2,1,0:T(8,128)(2,1)}), bf16[64,8,512]{2,1,0:T(8,128)(2,1)}, u32[]{:S(2)}, u32[]{:S(2)}) async-start(bf16[64,8,512]{2,1,0:T(8,128)(2,1)} %copy-done.3), calls=%async_computation.1 | async-start | bytes 1048576 | tf_op jit(solution)/shard_map/all_to_all | solution.py:388
  112.6 3.6 %collective-permute-start.14 = (f32[1,128]{1,0:T(1,128)S(1)}, f32[1,128]{1,0:T(1,128)S(1)}, u32[]{:S(2)}, u32[]{:S(2)}) collective-permute-start(f32[1,128]{1,0:T(1,128)S(1)} %bitcast.25), channel_id=1, source_target_pairs={{0,3},{1,0},{2,1},{3,2},{4,7},{5,4},{6,5},{7,6},{8,11},{9,8},{10,9... | collective-permute-start | bytes 1544 | tf_op jit(solution)/shard_map/ppermute | solution.py:407
  113.0 5.1 %collective-permute-start.15 = (f32[1,128]{1,0:T(1,128)S(1)}, f32[1,128]{1,0:T(1,128)S(1)}, u32[]{:S(2)}, u32[]{:S(2)}) collective-permute-start(f32[1,128]{1,0:T(1,128)S(1)} %bitcast.26), channel_id=1, source_target_pairs={{0,2},{1,3},{2,0},{3,1},{4,6},{5,7},{6,4},{7,5},{8,10},{9,11},{10,... | collective-permute-start | bytes 1544 | tf_op jit(solution)/shard_map/ppermute | solution.py:408
  113.8 5.1 %collective-permute-start.16 = (f32[1,128]{1,0:T(1,128)S(1)}, f32[1,128]{1,0:T(1,128)S(1)}, u32[]{:S(2)}, u32[]{:S(2)}) collective-permute-start(f32[1,128]{1,0:T(1,128)S(1)} %bitcast.27), channel_id=1, source_target_pairs={{0,1},{1,2},{2,3},{3,0},{4,5},{5,6},{6,7},{7,4},{8,9},{9,10},{10,1... | collective-permute-start | bytes 1544 | tf_op jit(solution)/shard_map/ppermute | solution.py:406
  120.5 8.5 %collective-permute-start.17 = (bf16[128,512]{1,0:T(8,128)(2,1)S(1)}, bf16[128,512]{1,0:T(8,128)(2,1)S(1)}, u32[]{:S(2)}, u32[]{:S(2)}) collective-permute-start(bf16[128,512]{1,0:T(8,128)(2,1)S(1)} %get-tuple-element.53), channel_id=1, source_target_pairs={{0,1},{1,2},{2,3},{3,0},{4,5},{5,6},{6,7},{7,4},{8,9},{9,10},{10,1... | collective-permute-start | bytes 393224 | tf_op jit(solution)/shard_map/ppermute | solution.py:457
  121.4 7.6 %collective-permute-start.18 = (bf16[128,512]{1,0:T(8,128)(2,1)S(1)}, bf16[128,512]{1,0:T(8,128)(2,1)S(1)}, u32[]{:S(2)}, u32[]{:S(2)}) collective-permute-start(bf16[128,512]{1,0:T(8,128)(2,1)S(1)} %get-tuple-element.54), channel_id=1, source_target_pairs={{0,2},{1,3},{2,0},{3,1},{4,6},{5,7},{6,4},{7,5},{8,10},{9,11},{10,... | collective-permute-start | bytes 393224 | tf_op jit(solution)/shard_map/ppermute | solution.py:458
  124.0 5.6 %collective-permute-start.19 = (bf16[128,512]{1,0:T(8,128)(2,1)S(1)}, bf16[128,512]{1,0:T(8,128)(2,1)S(1)}, u32[]{:S(2)}, u32[]{:S(2)}) collective-permute-start(bf16[128,512]{1,0:T(8,128)(2,1)S(1)} %get-tuple-element.55), channel_id=1, source_target_pairs={{0,3},{1,0},{2,1},{3,2},{4,7},{5,4},{6,5},{7,6},{8,11},{9,8},{10,9... | collective-permute-start | bytes 393224 | tf_op jit(solution)/shard_map/ppermute | solution.py:459
  124.4 17.4 %collective-permute-start.20 = (bf16[128,512]{1,0:T(8,128)(2,1)}, bf16[128,512]{1,0:T(8,128)(2,1)}, u32[]{:S(2)}, u32[]{:S(2)}) collective-permute-start(bf16[128,512]{1,0:T(8,128)(2,1)} %get-tuple-element.57), channel_id=1, source_target_pairs={{0,4},{4,0},{1,5},{5,1},{2,6},{6,2},{3,7},{7,3},{8,12},{12,8},{9,1... | collective-permute-start | bytes 393224 | tf_op jit(solution)/shard_map/ppermute | solution.py:461
  130.0 1.0 copy-start.14
  134.9 27.0 %all-to-all-start.2 = ((bf16[32,64,128]{2,1,0:T(8,128)(2,1)}), bf16[32,64,128]{2,1,0:T(8,128)(2,1)}, u32[]{:S(2)}, u32[]{:S(2)}) async-start(bf16[32,64,128]{2,1,0:T(8,128)(2,1)} %copy-done.15), calls=%async_computation.2 | async-start | bytes 1048576 | tf_op jit(solution)/shard_map/all_to_all | solution.py:388
  142.8 13.3 %collective-permute-start.21 = (bf16[2,128,512]{2,1,0:T(8,128)(2,1)S(1)}, bf16[2,128,512]{2,1,0:T(8,128)(2,1)}, u32[]{:S(2)}, u32[]{:S(2)}) collective-permute-start(bf16[2,128,512]{2,1,0:T(8,128)(2,1)S(1)} %pad_maximum_fusion.refs_0_), channel_id=1, source_target_pairs={{0,24},{8,0},{16,8},{24,16},{1,25},{9,1},{17,9},{25,17},{2,26},{10... | collective-permute-start | bytes 786440 | tf_op jit(solution)/shard_map/ppermute | solution.py:407
  143.1 18.7 %collective-permute-start.22 = (bf16[2,128,512]{2,1,0:T(8,128)(2,1)S(1)}, bf16[2,128,512]{2,1,0:T(8,128)(2,1)}, u32[]{:S(2)}, u32[]{:S(2)}) collective-permute-start(bf16[2,128,512]{2,1,0:T(8,128)(2,1)S(1)} %pad_maximum_fusion.refs_0_), channel_id=1, source_target_pairs={{0,16},{8,24},{16,0},{24,8},{1,17},{9,25},{17,1},{25,9},{2,18},{10... | collective-permute-start | bytes 786440 | tf_op jit(solution)/shard_map/ppermute | solution.py:408
  145.8 16.1 %collective-permute-start.23 = (bf16[2,128,512]{2,1,0:T(8,128)(2,1)S(1)}, bf16[2,128,512]{2,1,0:T(8,128)(2,1)}, u32[]{:S(2)}, u32[]{:S(2)}) collective-permute-start(bf16[2,128,512]{2,1,0:T(8,128)(2,1)S(1)} %pad_maximum_fusion.refs_0_), channel_id=1, source_target_pairs={{0,8},{8,16},{16,24},{24,0},{1,9},{9,17},{17,25},{25,1},{2,10},{10... | collective-permute-start | bytes 786440 | tf_op jit(solution)/shard_map/ppermute | solution.py:406
  164.3 25.1 %copy-start.17 = (bf16[256,512]{1,0:T(8,128)(2,1)S(1)}, bf16[256,512]{1,0:T(8,128)(2,1)}, u32[]{:S(2)}) copy-start(bf16[256,512]{1,0:T(8,128)(2,1)} %copy-done.16) | copy-start | bytes 786436
  164.3 34.1 %all-to-all-start.3 = ((bf16[8,32,512]{2,1,0:T(8,128)(2,1)}), bf16[8,32,512]{2,1,0:T(8,128)(2,1)}, u32[]{:S(2)}, u32[]{:S(2)}) async-start(bf16[8,32,512]{2,1,0:T(8,128)(2,1)} %shard_map.154), calls=%async_computation.3 | async-start | bytes 524288 | tf_op jit(solution)/shard_map/all_to_all | solution.py:388
  171.2 18.2 %copy-start.5 = (bf16[512,512]{1,0:T(8,128)(2,1)S(1)}, bf16[512,512]{1,0:T(8,128)(2,1)}, u32[]{:S(2)}) copy-start(bf16[512,512]{1,0:T(8,128)(2,1)} %copy-done.4) | copy-start | bytes 1572868
  171.2 18.2 %copy-start.7 = (bf16[512,512]{1,0:T(8,128)(2,1)S(1)}, bf16[512,512]{1,0:T(8,128)(2,1)}, u32[]{:S(2)}) copy-start(bf16[512,512]{1,0:T(8,128)(2,1)} %copy-done.6) | copy-start | bytes 1572868
  171.2 18.2 %copy-start.9 = (bf16[512,512]{1,0:T(8,128)(2,1)S(1)}, bf16[512,512]{1,0:T(8,128)(2,1)}, u32[]{:S(2)}) copy-start(bf16[512,512]{1,0:T(8,128)(2,1)} %copy-done.8) | copy-start | bytes 1572868
  171.2 18.2 %copy-start.11 = (bf16[512,512]{1,0:T(8,128)(2,1)S(1)}, bf16[512,512]{1,0:T(8,128)(2,1)}, u32[]{:S(2)}) copy-start(bf16[512,512]{1,0:T(8,128)(2,1)} %copy-done.10) | copy-start | bytes 1572868
  171.2 18.2 %copy-start.19 = (bf16[256,512]{1,0:T(8,128)(2,1)S(1)}, bf16[256,512]{1,0:T(8,128)(2,1)}, u32[]{:S(2)}) copy-start(bf16[256,512]{1,0:T(8,128)(2,1)} %copy-done.18) | copy-start | bytes 786436
  171.2 18.2 %copy-start.21 = (bf16[256,512]{1,0:T(8,128)(2,1)S(1)}, bf16[256,512]{1,0:T(8,128)(2,1)}, u32[]{:S(2)}) copy-start(bf16[256,512]{1,0:T(8,128)(2,1)} %copy-done.20) | copy-start | bytes 786436
  171.2 13.6 %collective-permute-start.24 = (bf16[128,512]{1,0:T(8,128)(2,1)}, bf16[128,512]{1,0:T(8,128)(2,1)S(1)}, u32[]{:S(2)}, u32[]{:S(2)}) collective-permute-start(bf16[128,512]{1,0:T(8,128)(2,1)} %copy-done.24), channel_id=1, source_target_pairs={{0,3},{1,0},{2,1},{3,2},{4,7},{5,4},{6,5},{7,6},{8,11},{9,8},{10,9... | collective-permute-start | bytes 393224 | tf_op jit(solution)/shard_map/ppermute | solution.py:407
  174.0 10.9 %collective-permute-start.25 = (bf16[128,512]{1,0:T(8,128)(2,1)}, bf16[128,512]{1,0:T(8,128)(2,1)S(1)}, u32[]{:S(2)}, u32[]{:S(2)}) collective-permute-start(bf16[128,512]{1,0:T(8,128)(2,1)} %copy-done.24), channel_id=1, source_target_pairs={{0,2},{1,3},{2,0},{3,1},{4,6},{5,7},{6,4},{7,5},{8,10},{9,11},{10,... | collective-permute-start | bytes 393224 | tf_op jit(solution)/shard_map/ppermute | solution.py:408
  174.9 10.0 %collective-permute-start.26 = (bf16[128,512]{1,0:T(8,128)(2,1)}, bf16[128,512]{1,0:T(8,128)(2,1)S(1)}, u32[]{:S(2)}, u32[]{:S(2)}) collective-permute-start(bf16[128,512]{1,0:T(8,128)(2,1)} %copy-done.24), channel_id=1, source_target_pairs={{0,1},{1,2},{2,3},{3,0},{4,5},{5,6},{6,7},{7,4},{8,9},{9,10},{10,1... | collective-permute-start | bytes 393224 | tf_op jit(solution)/shard_map/ppermute | solution.py:406
  175.7 4.0 %collective-permute-start.27 = (f32[1,128]{1,0:T(1,128)S(1)}, f32[1,128]{1,0:T(1,128)S(1)}, u32[]{:S(2)}, u32[]{:S(2)}) collective-permute-start(f32[1,128]{1,0:T(1,128)S(1)} %get-tuple-element.59.refs_4_), channel_id=1, source_target_pairs={{0,3},{1,0},{2,1},{3,2},{4,7},{5,4},{6,5},{7,6},{8,11},{9,8},{10,9... | collective-permute-start | bytes 1544 | tf_op jit(solution)/shard_map/ppermute | solution.py:407
  178.1 5.2 %collective-permute-start.28 = (f32[1,128]{1,0:T(1,128)S(1)}, f32[1,128]{1,0:T(1,128)S(1)}, u32[]{:S(2)}, u32[]{:S(2)}) collective-permute-start(f32[1,128]{1,0:T(1,128)S(1)} %get-tuple-element.59.refs_4_), channel_id=1, source_target_pairs={{0,2},{1,3},{2,0},{3,1},{4,6},{5,7},{6,4},{7,5},{8,10},{9,11},{10,... | collective-permute-start | bytes 1544 | tf_op jit(solution)/shard_map/ppermute | solution.py:408
  179.7 5.2 %collective-permute-start.29 = (f32[1,128]{1,0:T(1,128)S(1)}, f32[1,128]{1,0:T(1,128)S(1)}, u32[]{:S(2)}, u32[]{:S(2)}) collective-permute-start(f32[1,128]{1,0:T(1,128)S(1)} %get-tuple-element.59.refs_4_), channel_id=1, source_target_pairs={{0,1},{1,2},{2,3},{3,0},{4,5},{5,6},{6,7},{7,4},{8,9},{9,10},{10,1... | collective-permute-start | bytes 1544 | tf_op jit(solution)/shard_map/ppermute | solution.py:406
  187.5 9.2 %collective-permute-start.30 = (bf16[32,512]{1,0:T(8,128)(2,1)S(1)}, bf16[32,512]{1,0:T(8,128)(2,1)S(1)}, u32[]{:S(2)}, u32[]{:S(2)}) collective-permute-start(bf16[32,512]{1,0:T(8,128)(2,1)S(1)} %get-tuple-element.62), channel_id=1, source_target_pairs={{4,0},{8,4},{12,8},{16,12},{20,16},{24,20},{28,24},{32,28},{36,32}... | collective-permute-start | bytes 98312 | tf_op jit(solution)/shard_map/ppermute | solution.py:489
  189.5 1.0 copy-start.23
  190.4 0.9 copy-start.32
  191.4 0.9 copy-start.34
  192.3 0.9 copy-start.36
  193.3 3.4 %copy-start.27 = (f32[31,512]{1,0:T(8,128)S(1)}, f32[31,512]{1,0:T(8,128)}, u32[]{:S(2)}) copy-start(f32[31,512]{1,0:T(8,128)} %taps_ref.1) | copy-start | bytes 190468
  (7 other events, 5.6 us)

commit v2 on v1

--- a/solution.py
+++ b/solution.py
@@ -55,7 +55,7 @@
         weight_ref[1:2, :], (8, tokens)
     ).T
     scaled = [(weight[k][:, 0:1] * cot).astype(bf16) for k in range(2)]
-    out = dot(picks[0], scaled[0], 1, 0) + dot(picks[1], scaled[1], 1, 0)
+    out = dot(jnp.concatenate(picks, axis=1), jnp.concatenate(scaled, axis=0), 1, 0)
     send_ref[:, :, shape[2] :] = out.astype(bf16).reshape(shape)
 
 
@@ -75,6 +75,10 @@
         out_shape=[sent, jax.ShapeDtypeStruct((experts * capacity, tokens), bf16)],
         cost_estimate=cost(400_000_000, 3_000_000),
     )(tp, routes.T, route_weight.T, mixer_out, out_cot)
+
+
+def by_slice(w):
+    return w.reshape(w.shape[0] // 32, 4, 8, w.shape[1])
 
 
 def block_of(t, k):
@@ -133,8 +137,8 @@
 def row_parts(t, order, gp_ref, up_ref, wg_ref, wu_ref, outs):
     half, width = outs[0].shape
     for i, k in enumerate(order):
-        cols = pl.ds(pl.multiple_of(block_of(t, k) * width, width), width)
-        back = dot(gp_ref[...], wg_ref[cols, :], 1, 1) + dot(up_ref[...], wu_ref[cols, :], 1, 1)
+        wg, wu = (w[:, block_of(t, k)].reshape(width, w.shape[3]) for w in (wg_ref, wu_ref))
+        back = dot(gp_ref[...], wg, 1, 1) + dot(up_ref[...], wu, 1, 1)
         outs[2 * i][...] = back[:half].astype(bf16)
         outs[2 * i + 1][...] = back[half:].astype(bf16)
 
@@ -158,7 +162,7 @@
 
 
 def rest_backward(tp, gate_pre, up_pre, w_gate, w_up):
-    block = jax.ShapeDtypeStruct((gate_pre.shape[0] // 2, w_gate.shape[0] // 4), bf16)
+    block = jax.ShapeDtypeStruct((gate_pre.shape[0] // 2, w_gate.shape[0] * 8), bf16)
     return pl.pallas_call(
         rest_kernel,
         in_specs=[SM] + [VM] * 4,
@@ -173,16 +177,22 @@
     xs, cs = refs[:5], refs[5:10]
     act_ref, gp_ref, up_ref, gg_ref, ug_ref, dg_ref = refs[10:]
     _, width = xs[2].shape
-    for k in range(4):
-        at = pl.ds(pl.multiple_of(block_of(t_ref[0], k) * width, width), width)
-        i = k + (k == 3)
-        x, c = (
-            jnp.concatenate([b[2][...], b[3][...]], axis=0) if k == 2 else b[i][...]
-            for b in (xs, cs)
-        )
-        gg_ref[at, :] = dot(x, gp_ref[...], 0, 0).astype(bf16)
-        ug_ref[at, :] = dot(x, up_ref[...], 0, 0).astype(bf16)
-        dg_ref[:, at] = dot(act_ref[...], c, 0, 0).astype(bf16)
+    step = 256
+
+    @pl.loop(0, width // step)
+    def _(h):
+        lanes = pl.ds(pl.multiple_of(h * step, step), step)
+        for k in range(4):
+            first = block_of(t_ref[0], k) * width + h * step
+            at = pl.ds(pl.multiple_of(first, step), step)
+            i = k + (k == 3)
+            x, c = (
+                jnp.concatenate([b[2][:, lanes], b[3][:, lanes]], axis=0) if k == 2 else b[i][:, lanes]
+                for b in (xs, cs)
+            )
+            gg_ref[at, :] = dot(x, gp_ref[...], 0, 0).astype(bf16)
+            ug_ref[at, :] = dot(x, up_ref[...], 0, 0).astype(bf16)
+            dg_ref[:, at] = dot(act_ref[...], c, 0, 0).astype(bf16)
 
 
 def weight_grads(tp, x_blocks, c_blocks, act, gate_pre, up_pre):
@@ -209,74 +219,73 @@
     return normed * sig, sig * (1.0 + normed * (1.0 - sig)) * gain
 
 
-def act_kernel(t_ref, p0_ref, p1_ref, p2_ref, p3_ref, conv_ref, gain_ref, w_ref, act_ref, inv_ref, *q_refs):
-    width = conv_ref.shape[1]
+def act_kernel(t_ref, p0_ref, p1_ref, p2_ref, p3_ref, conv_ref, gain_ref, w_ref, cot_ref, act_ref, inv_ref, cott_ref, *q_refs):
     power = (p0_ref[...] + p1_ref[...]) + (p2_ref[...] + p3_ref[...])
     inv_rms = column(lax.rsqrt(power / w_ref.shape[1] + norm_epsilon))
     conv = conv_ref[...].astype(f32)
     act, slope = gate(conv, inv_rms, gain_ref[...])
-    act_ref[...] = act.astype(bf16)
+    act_ref[...] = act.T.astype(bf16)
     inv_ref[...] = inv_rms
-    pulled = (conv * slope).astype(bf16)
+    q = dot((conv * slope).astype(bf16), w_ref[...], 1, 0).T
+    q = q.reshape(q.shape[0] // 32, 4, 8, q.shape[1])
+    scratch = q_refs[4]
+    scratch[...] = q
     for k in range(4):
-        at = pl.ds(pl.multiple_of(block_of(t_ref[0], k) * width, width), width)
-        q_refs[k][...] = dot(pulled, w_ref[:, at], 1, 0).astype(bf16)
-
-
-def act_parts(tp, powers, conv_out, gain, out_weight):
-    block = jax.ShapeDtypeStruct(conv_out.shape, bf16)
+        q_refs[k][...] = scratch[:, block_of(t_ref[0], k)].astype(bf16)
+    scratch[...] = cot_ref[...].astype(f32).T.reshape(q.shape)
+    cott_ref[...] = scratch[:, t_ref[0]]
+
+
+def act_parts(tp, powers, conv_out, gain, out_weight, out_cot):
+    tokens, model_width = out_cot.shape
+    block = jax.ShapeDtypeStruct((model_width // 32, 8, tokens), bf16)
     return pl.pallas_call(
         act_kernel,
-        in_specs=[SM] + [VM] * 7,
-        out_specs=[VM] * 6,
-        out_shape=[block, jax.ShapeDtypeStruct((conv_out.shape[0], 1), f32)] + [block] * 4,
+        in_specs=[SM] + [VM] * 8,
+        out_specs=[VM] * 7,
+        out_shape=[
+            jax.ShapeDtypeStruct((conv_out.shape[1], tokens), bf16),
+            jax.ShapeDtypeStruct((tokens, 1), f32),
+            jax.ShapeDtypeStruct(block.shape, f32),
+            *[block] * 4,
+        ],
+        scratch_shapes=[pltpu.VMEM((model_width // 32, 4, 8, tokens), f32)],
         compiler_params=PARAMS,
         cost_estimate=cost(268_435_456, 3_000_000),
-    )(tp, *powers, conv_out, gain, out_weight)
-
-
-def mix_kernel(t_ref, sel_ref, back_ref, q_ref, cot_ref, mix_ref, out_ref, dot_ref):
-    tokens, width = cot_ref.shape
-    ret = back_ref[...].reshape(sel_ref.shape[0], width)
-    mix = cot_ref[...].astype(f32) + dot(sel_ref[...], ret, 0, 0)
-    mix_ref[...] = mix.astype(bf16)
-    turned = mix.T.astype(bf16)
-    run = width // 16
-    for g in range(8):
-        piece = jnp.concatenate(
-            [turned[(q * 8 + g) * run : (q * 8 + g + 1) * run] for q in range(2)], axis=0
-        )
-        for j in range(4):
-            out_ref[g * 4 + j] = piece
-    dots = jnp.sum(mix.astype(bf16).astype(f32) * q_ref[...], axis=1, keepdims=True)
-    dot_ref[...] = jnp.broadcast_to(dots, (tokens, 128)).T[0:1, :]
-
-
-def mix_parts(tp, sel, returned, q_total, out_cot):
-    tokens = out_cot.shape[0]
-    _, _, quarter = returned.shape
-    whole = lambda shape: pl.BlockSpec(shape, lambda i, t: (0,) * len(shape))
-    shapes = [(tokens, quarter), (32, quarter // 8, tokens)]
+    )(tp, *powers, conv_out, gain, out_weight, out_cot)
+
+
+def mix_kernel(at_ref, sel_ref, back_ref, q_ref, cot_ref, mix_ref, own_ref, other_ref, split_ref):
+    slices, rows, tokens = cot_ref.shape
+    ret = back_ref[...].reshape(sel_ref.shape[0], back_ref.shape[2])
+    mix = (dot(ret, sel_ref[...], 0, 0).reshape(cot_ref.shape) + cot_ref[...]).astype(bf16)
+    mix_ref[:slices] = mix
+    split_ref[...] = mix.reshape(split_ref.shape)
+    for r in range(4):
+        to = 2 * block_of(at_ref[0], r)
+        own_ref[r] = split_ref[:, to + at_ref[1]]
+        other_ref[r] = split_ref[:, to + 1 - at_ref[1]]
+    dots = mix.astype(f32) * q_ref[...]
+    dots = jnp.sum(jnp.sum(dots, axis=0), axis=0, keepdims=True)
+    high = dots.astype(bf16)
+    low = (dots - high.astype(f32)).astype(bf16)
+    row = lax.broadcasted_iota(jnp.int32, (rows, tokens), 0)
+    pair = jnp.where(row == 0, high.astype(f32), jnp.where(row == 1, low.astype(f32), 0.0))
+    mix_ref[slices] = pair.astype(bf16)
+
+
+def mix_parts(at, sel, returned, q_total, cot_turned):
+    slices, rows, tokens = cot_turned.shape
+    near = jax.ShapeDtypeStruct((4, slices // 8, rows, tokens), bf16)
     return pl.pallas_call(
         mix_kernel,
-        grid_spec=pltpu.PrefetchScalarGridSpec(
-            num_scalar_prefetch=1,
-            grid=(1,),
-            in_specs=[
-                whole(sel.shape),
-                whole(returned.shape),
-                whole((tokens, quarter)),
-                pl.BlockSpec((tokens, quarter), lambda i, t: (0, t[0])),
-            ],
-            out_specs=[*[whole(s) for s in shapes], whole((1, tokens))],
-        ),
-        out_shape=[
-            *[jax.ShapeDtypeStruct(s, bf16) for s in shapes],
-            jax.ShapeDtypeStruct((1, tokens), f32),
-        ],
+        in_specs=[SM] + [VM] * 4,
+        out_specs=[VM] * 3,
+        out_shape=[jax.ShapeDtypeStruct((slices + 1, rows, tokens), bf16), near, near],
+        scratch_shapes=[pltpu.VMEM((slices // 8, 8, rows, tokens), bf16)],
         compiler_params=PARAMS,
         cost_estimate=cost(70_000_000, 2_000_000),
-    )(tp, sel, returned, q_total, out_cot)
+    )(at, sel, returned, q_total, cot_turned)
 
 
 def sum_kernel(oa_ref, na_ref, pa_ref, ob_ref, nb_ref, pb_ref, out_ref):
@@ -299,71 +308,77 @@
     )(*parts)
 
 
-def proj_kernel(at_ref, mix_ref, *refs):
-    acts, out_ref = refs[:4], refs[4]
-    rows, tokens = 4 * mix_ref.shape[1], mix_ref.shape[2]
-    acc = None
-    for r in range(4):
-        first = 8 * block_of(at_ref[0], r)
-        own, other = first + 4 * at_ref[1], first + 4 - 4 * at_ref[1]
-        left = [mix_ref[pl.ds(g, 4)].reshape(rows, tokens) for g in (own, other)]
-        right = acts[r][...].reshape(2 * tokens, acts[r].shape[2])
-        part = dot(jnp.concatenate(left, axis=1), right, 1, 0)
-        acc = part if acc is None else acc + part
-    out_ref[...] = acc.astype(bf16).reshape(out_ref.shape)
-
-
-def proj_partial(at, mixed, acts):
-    width = acts[0].shape[2]
+def proj_kernel(at_ref, *refs):
+    mixes, acts, out_ref = refs[:4], refs[4:8], refs[8]
+    far, rows, tokens = mixes[0].shape[1:]
+    width = out_ref.shape[3]
+    right = [
+        jnp.concatenate([m[c].reshape(far * rows, tokens) for c in range(2)], axis=1) for m in mixes
+    ]
+
+    @pl.loop(0, 4)
+    def _(k):
+        acc = None
+        for r in range(4):
+            left = jnp.concatenate([acts[r][c, k] for c in range(2)], axis=1)
+            part = dot(left, right[r], 1, 1)
+            acc = part if acc is None else acc + part
+        out_ref[:, block_of(at_ref[2], k)] = acc.T.astype(bf16).reshape(far, rows, width)
+
+
+def proj_partial(at, mixes, acts):
+    _, far, rows, _ = mixes[0].shape
     return pl.pallas_call(
         proj_kernel,
-        in_specs=[SM] + [VM] * 5,
+        in_specs=[SM] + [VM] * 8,
         out_specs=VM,
-        out_shape=jax.ShapeDtypeStruct((8, mixed.shape[1] // 2, width), bf16),
-        compiler_params=PARAMS,
-        cost_estimate=cost(268_435_456, 2_000_000),
-    )(at, mixed, *acts)
+        out_shape=jax.ShapeDtypeStruct((far, 4, rows, acts[0].shape[2]), bf16),
+        compiler_params=PARAMS,
+        cost_estimate=cost(268_435_456, 5_000_000),
+    )(at, *mixes, *acts)
 
 
 def grad_kernel(t_ref, *refs):
-    blocks, dots = refs[:4], refs[4:8]
-    inv_ref, conv_ref, gain_ref, w_ref, out_ref, head_ref = refs[8:]
-    width = blocks[0].shape[1]
-    back = None
+    blocks = refs[:4]
+    inv_ref, conv_ref, gain_ref, w_ref, out_ref, head_ref, all_ref = refs[4:]
+    slices = all_ref.shape[0]
+    total = 0.0
     for k in range(4):
-        at = pl.ds(pl.multiple_of(block_of(t_ref[0], k) * width, width), width)
-        part = dot(blocks[k][...], w_ref[:, at], 1, 1)
-        back = part if back is None else back + part
+        all_ref[:, block_of(t_ref[0], k)] = blocks[k][:slices]
+        total = total + jnp.sum(blocks[k][slices].astype(f32), axis=0, keepdims=True)
+    back = dot(w_ref[...], all_ref[...].reshape(w_ref.shape[1], all_ref.shape[3]), 1, 0).T
     conv = conv_ref[...].astype(f32)
     inv_rms = inv_ref[...]
     scaled = back * gate(conv, inv_rms, gain_ref[...])[1]
-    total = (dots[0][...] + dots[1][...]) + (dots[2][...] + dots[3][...])
     pull = column(total / w_ref.shape[1]) * inv_rms * inv_rms * inv_rms
     conv_grad = inv_rms * scaled - conv * pull
     out_ref[...] = conv_grad
     head_ref[...] = conv_grad[: head_ref.shape[0]].astype(bf16)
 
 
-def conv_backward(tp, blocks, dots, inv_rms, conv_out, gain, out_weight):
+def conv_backward(tp, blocks, inv_rms, conv_out, gain, out_weight):
     return pl.pallas_call(
         grad_kernel,
-        in_specs=[SM] + [VM] * 12,
+        in_specs=[SM] + [VM] * 8,
         out_specs=[VM] * 2,
         out_shape=[
             jax.ShapeDtypeStruct(conv_out.shape, f32),
             jax.ShapeDtypeStruct((32, conv_out.shape[1]), bf16),
         ],
+        scratch_shapes=[pltpu.VMEM((blocks[0].shape[0] - 1, 4, *blocks[0].shape[1:]), bf16)],
         compiler_params=PARAMS,
         cost_estimate=cost(268_435_456, 2_000_000),
-    )(tp, *blocks, *dots, inv_rms, conv_out, gain, out_weight)
+    )(tp, *blocks, inv_rms, conv_out, gain, out_weight)
 
 
 def taps_kernel(grad_ref, next_ref, taps_ref, out_ref, ext_ref):
     tokens, width = grad_ref.shape
     ext_ref[pl.ds(0, tokens), :] = grad_ref[...]
     ext_ref[pl.ds(tokens, next_ref.shape[0]), :] = next_ref[...].astype(f32)
-    for lane in range(0, width, 128):
-        lanes = pl.ds(lane, 128)
+
+    @pl.loop(0, width // 128)
+    def _(lane):
+        lanes = pl.ds(pl.multiple_of(lane * 128, 128), 128)
         acc = None
         for w in range(taps_ref.shape[0]):
             part = taps_ref[w : w + 1, lanes] * ext_ref[pl.ds(w, tokens), lanes]
@@ -443,9 +458,8 @@
     tp = lax.axis_index("tp").astype(jnp.int32)[None]
     w_gate, w_up, w_down = gate_weight[0], up_weight[0], down_weight[0]
 
-    send, sel = send_rows(
-        tp, routes, route_weight, mixer_out, out_cot, experts, capacity, quarter
-    )
+    at = jnp.stack([lax.axis_index(a) for a in ("y", "core", "tp")]).astype(jnp.int32)
+    send, sel = send_rows(tp, routes, route_weight, mixer_out, out_cot, experts, capacity, quarter)
     slots = experts * capacity
     arrived = exchange(send, SP).reshape(slots, 2 * quarter)
     x_slice, cot_slice = arrived[:, :quarter], arrived[:, quarter:]
@@ -453,37 +467,46 @@
     conv_vals = conv_out.astype(f32)
     powers = ring_all(jnp.sum(conv_vals * conv_vals, axis=1)[None])
     gain = norm_gain[None]
-    activated, inv_rms, *q_parts = act_parts(tp, powers, conv_out, gain, out_weight)
+    activated, inv_rms, cot_turned, *q_parts = act_parts(
+        tp, powers, conv_out, gain, out_weight, out_cot
+    )
     q_ahead = lax.ppermute(q_parts[1], "tp", AHEAD)
     q_across = lax.ppermute(q_parts[2], "tp", ACROSS)
     q_behind = lax.ppermute(q_parts[3], "tp", BEHIND)
     q_total = sum(q.astype(f32) for q in (q_parts[0], q_ahead, q_across, q_behind))
-    act_other = lax.ppermute(activated, "core", [(0, 1), (1, 0)])
-    act_near = ring_all(jnp.stack([activated, act_other]), "y")
+    act_row = jnp.stack(ring_all(activated))
+    act_other = lax.ppermute(act_row, "core", [(0, 1), (1, 0)])
+    act_near = ring_all(jnp.stack([act_row, act_other]), "y")
 
     x_blocks = ring_gather(x_slice)
     pre_gate, pre_up = expert_forward(tp, x_blocks, w_gate, w_up)
     c_blocks = ring_gather(cot_slice)
     act, gate_pre, up_pre, *far = expert_backward(
-        tp, c_blocks, w_down, pre_gate, pre_up, w_gate, w_up
+        tp, c_blocks, w_down, pre_gate, pre_up, by_slice(w_gate), by_slice(w_up)
     )
-    rest = rest_backward(tp, gate_pre, up_pre, w_gate, w_up)
+    rest = rest_backward(tp, gate_pre, up_pre, by_slice(w_gate), by_slice(w_up))
     sums = ring_scatter(*far, *rest)
     back = sum_rows(sums, experts)
     returned = exchange(back, SP)
     gate_g, up_g, down_g = weight_grads(tp, x_blocks, c_blocks, act, gate_pre, up_pre)
 
-    mix_part, mix_turned, dots = mix_parts(tp, sel, returned, q_total, out_cot)
-    mixed = exchange(mix_turned, ("y", "core", "tp"))
+    mix_part, mix_own, mix_other = mix_parts(at, sel, returned, q_total, cot_turned)
+    mix_other = lax.ppermute(mix_other, "core", [(0, 1), (1, 0)])
+    mix_pairs = jnp.stack([mix_own, mix_other], axis=1)
+    mixes = [
+        mix_pairs[0],
+        lax.ppermute(mix_pairs[3], "y", BEHIND),
+        lax.ppermute(mix_pairs[2], "y", ACROSS),
+        lax.ppermute(mix_pairs[1], "y", AHEAD),
+    ]
     mix_blocks = ring_all(mix_part)
-    at = jnp.stack([lax.axis_index("y"), lax.axis_index("core")]).astype(jnp.int32)
-    partial_proj = proj_partial(at, mixed, act_near)
-    partial_proj = exchange(partial_proj, "z")
+    partial_proj = proj_partial(at, mixes, act_near)
+    partial_proj = exchange(partial_proj.reshape(-1, *partial_proj.shape[2:]), ("z", "tp"))
+    partial_proj = partial_proj.reshape(lax.axis_size("z"), -1, quarter)
     proj_grad = jnp.sum(partial_proj.astype(f32), axis=0)
 
-    dot_blocks = ring_all(dots)
     conv_grad, head = conv_backward(
-        tp, mix_blocks, dot_blocks, inv_rms, conv_out, gain, out_weight
+        tp, mix_blocks, inv_rms, conv_out, gain, out_weight
     )
     route = [(i, i - 1) for i in range(1, experts)]
     following = lax.ppermute(head, SP, route)

time: 203 us -> 237 us (1.17)
  waiting for transfers between devices: 59.4 us -> 90.5 us
  starting transfers between devices: 67.4 us -> 61.5 us
  Pallas kernels: 17.6 us -> 21 us
    ppermute x4, waiting for transfers between devices: 9.35 us -> 28.1 us  [ring_all(): across = lax.ppermute(x, axis, ACROSS)]
    all_to_all x3 -> x2, starting transfers between devices: 20.9 us -> 14.5 us  [exchange(): return lax.all_to_all(x, axis, split_axis=0, concat_axis=0, tiled=True)]
    ppermute x1, waiting for transfers between devices: 0.57 us -> 5.04 us  [on_device(): q_behind = lax.ppermute(q_parts[3], 'tp', BEHIND)]
    ppermute x2, waiting for transfers between devices: 4.1 us -> 0.01 us  [ring_gather(): across_a = lax.ppermute(ahead[:half], 'tp', AHEAD)]
    ppermute x1, waiting for transfers between devices: 3.97 us -> 0.01 us  [ring_scatter(): next_b = lax.ppermute(next_b, 'tp', AHEAD)]
    ppermute x4, waiting for transfers between devices: 10.1 us -> 13.9 us  [ring_all(): behind = lax.ppermute(x, axis, BEHIND)]
    ppermute x1 -> x5, starting transfers between devices: 0.01 us -> 3.2 us  [the longest x1 1.53 us: on_device(): lax.ppermute(mix_pairs[2], 'y', ACROSS)]
    ppermute x4, starting transfers between devices: 5.8 us -> 8.92 us  [ring_all(): across = lax.ppermute(x, axis, ACROSS)]
  transfers between devices with their start and end apart: 34 -> 37, of which waited for: 21 -> 21; matrix products, arithmetic and copies ran while one was open for 1% -> 2% of each run, Pallas kernels for 5% -> 6%
where the time goes in v2:
time: 237 us; the launch traced here: 233 us
  waiting for transfers between devices  90.5 us (38%)
  starting transfers between devices  61.5 us (26%)
  blocking collectives  40.9 us (17%)
  Pallas kernels  21 us (9%)
  local copies, waits for them, and re-layouts  12.9 us (5%)
  other arithmetic  5.32 us (2%)
    all_to_all x1, blocking collectives, exchange(): return lax.all_to_all(x, axis, split_axis=0, concat_axis=0, tiled=True)  40.9 us
    ppermute x4, waiting for transfers between devices, ring_all(): across = lax.ppermute(x, axis, ACROSS)  28.1 us
    ppermute x2, waiting for transfers between devices, ring_gather(): ahead = lax.ppermute(block, 'tp', AHEAD)  17.3 us
    all_to_all x2, starting transfers between devices, exchange(): return lax.all_to_all(x, axis, split_axis=0, concat_axis=0, tiled=True)  14.5 us
    ppermute x4, waiting for transfers between devices, ring_all(): behind = lax.ppermute(x, axis, BEHIND)  13.9 us
    unnamed x92, local copies, waits for them, and re-layouts  12.8 us
    ppermute x4, starting transfers between devices, ring_all(): across = lax.ppermute(x, axis, ACROSS)  8.92 us
    ppermute x2, starting transfers between devices, ring_gather(): across_b = lax.ppermute(behind[half:], 'tp', BEHIND)  6.04 us
  transfers between devices with their start and end apart: 37, of which 21 were waited for; matrix products, arithmetic and copies ran while one was open for 2% of the time, Pallas kernels for 6%

profile of v2, /device:TPU:8, one launch (start us, length us, event | category | flops | bytes accessed | tf_op | source)
XLA Modules:
  0.0 233.3 jit_solution(13588900823983006458)
XLA Ops:
  0.6 2.6 %shard_map.146 = (bf16[64,8,1024]{2,1,0:T(8,128)(2,1)}, bf16[512,128]{1,0:T(8,128)(2,1)}) custom-call(s32[1]{0:T(128)} %bitcast.tp_ref.t_ref, s32[2,128]{1,0:T(2,128)} %bitcast.59, f32[2,128]{1,0:T(2,128)} %bitcast.60, bf16[128,2048]{1,0:T(8,128)(2,1)} %x_ref.1, bf16[128,2048]{1,0:T(8,128)(2,1)} %cot_ref.3), custom_call_target="tpu_custom_call" | custom-call | flops 400000000 | bytes 3000000 | tf_op jit(solution)/shard_map/pallas_call | solution.py:67
  3.3 40.9 %all_to_all.15 = bf16[64,8,1024]{2,1,0:T(8,128)(2,1)S(1)} all-to-all(bf16[64,8,1024]{2,1,0:T(8,128)(2,1)} %get-tuple-element.35), channel_id=1, replica_groups=mesh['z'=8,'y'=4,'core'=2,'tp'=4] {'z','y','core'}, dimensions={0} | all-to-all | bytes 2097152 | tf_op jit(solution)/shard_map/all_to_all | solution.py:403
  44.2 1.6 collective-permute-start.1
  45.8 1.7 collective-permute-start
  47.9 2.9 %collective-permute-start.4 = (bf16[512,512]{1,0:T(8,128)(2,1)S(1)}, bf16[512,512]{1,0:T(8,128)(2,1)S(1)}, u32[]{:S(2)}, u32[]{:S(2)}) collective-permute-start(bf16[512,512]{1,0:T(8,128)(2,1)S(1)} %get-tuple-element.65.refs_0_.refs_5_), channel_id=1, source_target_pairs={{0,3},{1,0},{2,1},{3,2},{4,7},{5,4},{6,5},{7,6},{8,11},{9,8},{10,9... | collective-permute-start | bytes 1572872 | tf_op jit(solution)/shard_map/ppermute | solution.py:414
  50.8 9.5 %collective-permute-done.1.refs_4_ = bf16[512,512]{1,0:T(8,128)(2,1)S(1)} collective-permute-done((bf16[512,512]{1,0:T(8,128)(2,1)S(1)}, bf16[512,512]{1,0:T(8,128)(2,1)S(1)}, u32[]{:S(2)}, u32[]{:S(2)}) %collective-permute-start.1) | collective-permute-done | bytes 524320 | tf_op jit(solution)/shard_map/ppermute | solution.py:413
  60.8 3.0 %collective-permute-start.3 = (bf16[256,512]{1,0:T(8,128)(2,1)S(1)}, bf16[256,512]{1,0:T(8,128)(2,1)S(1)}, u32[]{:S(2)}, u32[]{:S(2)}) collective-permute-start(bf16[256,512]{1,0:T(8,128)(2,1)S(1)} %slice.42), channel_id=1, source_target_pairs={{0,3},{1,0},{2,1},{3,2},{4,7},{5,4},{6,5},{7,6},{8,11},{9,8},{10,9... | collective-permute-start | bytes 786440 | tf_op jit(solution)/shard_map/ppermute | solution.py:416
  63.8 7.8 %collective-permute-done.5.refs_4_.refs_9_ = bf16[512,512]{1,0:T(8,128)(2,1)S(1)} collective-permute-done((bf16[512,512]{1,0:T(8,128)(2,1)S(1)}, bf16[512,512]{1,0:T(8,128)(2,1)S(1)}, u32[]{:S(2)}, u32[]{:S(2)}) %collective-permute-start.5) | collective-permute-done | bytes 524320 | tf_op jit(solution)/shard_map/ppermute | solution.py:413
  72.0 3.0 %collective-permute-start.7 = (bf16[256,512]{1,0:T(8,128)(2,1)S(1)}, bf16[256,512]{1,0:T(8,128)(2,1)S(1)}, u32[]{:S(2)}, u32[]{:S(2)}) collective-permute-start(bf16[256,512]{1,0:T(8,128)(2,1)S(1)} %slice.45), channel_id=1, source_target_pairs={{0,3},{1,0},{2,1},{3,2},{4,7},{5,4},{6,5},{7,6},{8,11},{9,8},{10,9... | collective-permute-start | bytes 786440 | tf_op jit(solution)/shard_map/ppermute | solution.py:416
  75.5 5.3 %collective-permute-done.14.p1_ref = f32[1,128]{1,0:T(1,128)S(1)} collective-permute-done((f32[1,128]{1,0:T(1,128)S(1)}, f32[1,128]{1,0:T(1,128)S(1)}, u32[]{:S(2)}, u32[]{:S(2)}) %collective-permute-start.14) | collective-permute-done | bytes 544 | tf_op jit(solution)/shard_map/ppermute | solution.py:422
  80.8 2.7 %collective-permute-start.15 = (f32[1,128]{1,0:T(1,128)S(1)}, f32[1,128]{1,0:T(1,128)S(1)}, u32[]{:S(2)}, u32[]{:S(2)}) collective-permute-start(f32[1,128]{1,0:T(1,128)S(1)} %bitcast.50), channel_id=1, source_target_pairs={{0,2},{1,3},{2,0},{3,1},{4,6},{5,7},{6,4},{7,5},{8,10},{9,11},{10,... | collective-permute-start | bytes 1544 | tf_op jit(solution)/shard_map/ppermute | solution.py:423
  83.5 2.4 %collective-permute-done.15.p2_ref = f32[1,128]{1,0:T(1,128)S(1)} collective-permute-done((f32[1,128]{1,0:T(1,128)S(1)}, f32[1,128]{1,0:T(1,128)S(1)}, u32[]{:S(2)}, u32[]{:S(2)}) %collective-permute-start.15) | collective-permute-done | bytes 544 | tf_op jit(solution)/shard_map/ppermute | solution.py:423
  85.9 1.5 collective-permute-start.16
  87.4 3.3 %collective-permute-done.16.p3_ref = f32[1,128]{1,0:T(1,128)S(1)} collective-permute-done((f32[1,128]{1,0:T(1,128)S(1)}, f32[1,128]{1,0:T(1,128)S(1)}, u32[]{:S(2)}, u32[]{:S(2)}) %collective-permute-start.16) | collective-permute-done | bytes 544 | tf_op jit(solution)/shard_map/ppermute | solution.py:421
  90.7 1.1 shard_map.152
  94.0 2.9 %collective-permute-start.25 = (bf16[512,128]{1,0:T(8,128)(2,1)S(1)}, bf16[512,128]{1,0:T(8,128)(2,1)S(1)}, u32[]{:S(2)}, u32[]{:S(2)}) collective-permute-start(bf16[512,128]{1,0:T(8,128)(2,1)S(1)} %get-tuple-element.60), channel_id=1, source_target_pairs={{0,2},{1,3},{2,0},{3,1},{4,6},{5,7},{6,4},{7,5},{8,10},{9,11},{10,... | collective-permute-start | bytes 393224 | tf_op jit(solution)/shard_map/ppermute | solution.py:423
  96.9 0.9 collective-permute-start.24
  97.9 1.3 shard_map.147
  99.3 1.6 shard_map.148
  101.0 1.2 collective-permute-start.8
  102.1 1.9 collective-permute-done.25
  104.1 0.9 fusion.7
  105.7 1.0 shard_map.150
  107.4 1.5 collective-permute-start.11
  109.0 1.4 collective-permute-start.9
  110.3 3.8 %collective-permute-done.12 = bf16[256,512]{1,0:T(8,128)(2,1)S(1)} collective-permute-done((bf16[256,512]{1,0:T(8,128)(2,1)S(1)}, bf16[256,512]{1,0:T(8,128)(2,1)S(1)}, u32[]{:S(2)}, u32[]{:S(2)}) %collective-permute-start.12) | collective-permute-done | bytes 262176 | tf_op jit(solution)/shard_map/ppermute | solution.py:433
  114.2 2.0 collective-permute-start.13
  116.3 3.5 %collective-permute-done.10.pa_ref = bf16[256,512]{1,0:T(8,128)(2,1)S(1)} collective-permute-done((bf16[256,512]{1,0:T(8,128)(2,1)S(1)}, bf16[256,512]{1,0:T(8,128)(2,1)S(1)}, u32[]{:S(2)}, u32[]{:S(2)}) %collective-permute-start.10) | collective-permute-done | bytes 262176 | tf_op jit(solution)/shard_map/ppermute | solution.py:435
  119.8 2.6 %collective-permute-done.9.na_ref = bf16[256,512]{1,0:T(8,128)(2,1)S(1)} collective-permute-done((bf16[256,512]{1,0:T(8,128)(2,1)S(1)}, bf16[256,512]{1,0:T(8,128)(2,1)S(1)}, u32[]{:S(2)}, u32[]{:S(2)}) %collective-permute-start.9) | collective-permute-done | bytes 262176 | tf_op jit(solution)/shard_map/ppermute | solution.py:436
  122.4 2.6 %collective-permute-done.13.pb_ref = bf16[256,512]{1,0:T(8,128)(2,1)S(1)} collective-permute-done((bf16[256,512]{1,0:T(8,128)(2,1)S(1)}, bf16[256,512]{1,0:T(8,128)(2,1)S(1)}, u32[]{:S(2)}, u32[]{:S(2)}) %collective-permute-start.13) | collective-permute-done | bytes 262176 | tf_op jit(solution)/shard_map/ppermute | solution.py:437
  124.9 1.0 shard_map.151
  125.9 5.6 %all-to-all-start.1 = ((bf16[64,8,512]{2,1,0:T(8,128)(2,1)}), bf16[64,8,512]{2,1,0:T(8,128)(2,1)}, u32[]{:S(2)}, u32[]{:S(2)}) async-start(bf16[64,8,512]{2,1,0:T(8,128)(2,1)} %shard_map.151), calls=%async_computation.1 | async-start | bytes 1048576 | tf_op jit(solution)/shard_map/all_to_all | solution.py:403
  132.4 1.3 pad_maximum_fusion.refs_4_
  134.3 2.4 %collective-permute-start.29 = (bf16[2,4,512,128]{3,2,1,0:T(8,128)(2,1)S(1)}, bf16[2,4,512,128]{3,2,1,0:T(8,128)(2,1)}, u32[]{:S(2)}, u32[]{:S(2)}) collective-permute-start(bf16[2,4,512,128]{3,2,1,0:T(8,128)(2,1)S(1)} %pad_maximum_fusion.refs_4_), channel_id=1, source_target_pairs={{0,16},{8,24},{16,0},{24,8},{1,17},{9,25},{17,1},{25,9},{2,18},{10... | collective-permute-start | bytes 3145736 | tf_op jit(solution)/shard_map/ppermute | solution.py:423
  136.7 1.8 collective-permute-start.30
  138.5 2.9 %collective-permute-start.19 = (bf16[64,8,128]{2,1,0:T(8,128)(2,1)S(1)}, bf16[64,8,128]{2,1,0:T(8,128)(2,1)S(1)}, u32[]{:S(2)}, u32[]{:S(2)}) collective-permute-start(bf16[64,8,128]{2,1,0:T(8,128)(2,1)S(1)} %copy-done.43), channel_id=1, source_target_pairs={{0,3},{1,0},{2,1},{3,2},{4,7},{5,4},{6,5},{7,6},{8,11},{9,8},{10,9... | collective-permute-start | bytes 393224 | tf_op jit(solution)/shard_map/ppermute | solution.py:475
  141.4 5.0 %collective-permute-done.19 = bf16[64,8,128]{2,1,0:T(8,128)(2,1)S(1)} collective-permute-done((bf16[64,8,128]{2,1,0:T(8,128)(2,1)S(1)}, bf16[64,8,128]{2,1,0:T(8,128)(2,1)S(1)}, u32[]{:S(2)}, u32[]{:S(2)}) %collective-permute-start.19) | collective-permute-done | bytes 131104 | tf_op jit(solution)/shard_map/ppermute | solution.py:475
  148.0 5.8 %collective-permute-done.17 = bf16[64,8,128]{2,1,0:T(8,128)(2,1)} collective-permute-done((bf16[64,8,128]{2,1,0:T(8,128)(2,1)S(1)}, bf16[64,8,128]{2,1,0:T(8,128)(2,1)}, u32[]{:S(2)}, u32[]{:S(2)}) %collective-permute-start.17) | collective-permute-done | bytes 131104 | tf_op jit(solution)/shard_map/ppermute | solution.py:473
  153.8 1.2 convert_add_fusion.q_ref
  155.0 0.9 copy-done.27
  155.9 0.9 copy-done.30
  156.8 1.4 shard_map.153
  158.4 1.2 collective-permute-done.20
  160.0 1.5 collective-permute-start.22
  161.5 2.9 %collective-permute-done.28.refs_5_ = bf16[2,4,512,128]{3,2,1,0:T(8,128)(2,1)} collective-permute-done((bf16[2,4,512,128]{3,2,1,0:T(8,128)(2,1)S(1)}, bf16[2,4,512,128]{3,2,1,0:T(8,128)(2,1)}, u32[]{:S(2)}, u32[]{:S(2)}) %collective-permute-start.28) | collective-permute-done | bytes 1048608 | tf_op jit(solution)/shard_map/ppermute | solution.py:422
  164.4 1.2 collective-permute-start.23
  165.6 21.9 %collective-permute-done.29.refs_6_ = bf16[2,4,512,128]{3,2,1,0:T(8,128)(2,1)} collective-permute-done((bf16[2,4,512,128]{3,2,1,0:T(8,128)(2,1)S(1)}, bf16[2,4,512,128]{3,2,1,0:T(8,128)(2,1)}, u32[]{:S(2)}, u32[]{:S(2)}) %collective-permute-start.29) | collective-permute-done | bytes 1048608 | tf_op jit(solution)/shard_map/ppermute | solution.py:423
  188.4 4.5 %shard_map.154 = bf16[8,4,8,512]{3,2,1,0:T(8,128)(2,1)} custom-call(s32[3]{0:T(128)S(1)} %pad_add_fusion.at_ref, bf16[2,8,8,128]{3,2,1,0:T(8,128)(2,1)S(1)} %get-tuple-element.70.refs_0_, bf16[2,8,8,128]{3,2,1,0:T(8,128)(2,1)S(1)} %collective-permute-done.21.refs_1_, bf16[2,8,8,128]{3,2,1,0:T(8,128)(2,1)S(1)} %collective-permute-done.22.refs_2_, ...), custom_call_target="tpu_custom_call" | custom-call | flops 268435456 | bytes 5000000 | tf_op jit(solution)/shard_map/pallas_call | solution.py:331
  192.9 8.9 %all-to-all-start.2 = ((bf16[32,8,512]{2,1,0:T(8,128)(2,1)}), bf16[32,8,512]{2,1,0:T(8,128)(2,1)}, u32[]{:S(2)}, u32[]{:S(2)}) async-start(bf16[32,8,512]{2,1,0:T(8,128)(2,1)} %bitcast.28), calls=%async_computation.2 | async-start | bytes 524288 | tf_op jit(solution)/shard_map/all_to_all | solution.py:403
  201.8 3.0 %collective-permute-start.31 = (bf16[65,8,128]{2,1,0:T(8,128)(2,1)}, bf16[65,8,128]{2,1,0:T(8,128)(2,1)S(1)}, u32[]{:S(2)}, u32[]{:S(2)}) collective-permute-start(bf16[65,8,128]{2,1,0:T(8,128)(2,1)} %copy-done.28), channel_id=1, source_target_pairs={{0,3},{1,0},{2,1},{3,2},{4,7},{5,4},{6,5},{7,6},{8,11},{9,8},{10,9... | collective-permute-start | bytes 399368 | tf_op jit(solution)/shard_map/ppermute | solution.py:422
  206.6 5.8 %collective-permute-done.31.refs_1_ = bf16[65,8,128]{2,1,0:T(8,128)(2,1)S(1)} collective-permute-done((bf16[65,8,128]{2,1,0:T(8,128)(2,1)}, bf16[65,8,128]{2,1,0:T(8,128)(2,1)S(1)}, u32[]{:S(2)}, u32[]{:S(2)}) %collective-permute-start.31) | collective-permute-done | bytes 133152 | tf_op jit(solution)/shard_map/ppermute | solution.py:422
  212.3 1.9 collective-permute-done.32.refs_2_
  214.2 1.5 collective-permute-done.33.refs_3_
  215.7 0.9 copy-done.29
  218.4 1.9 collective-permute-start.34
  220.4 0.9 copy-done.21
  221.3 0.9 copy-done.23
  222.3 0.9 copy-done.25
  223.2 0.9 copy-done.37
  224.2 0.9 copy-done.39
  225.1 0.9 copy-done.41
  226.1 3.6 %shard_map.149 = (bf16[2048,256]{1,0:T(8,128)(2,1)}, bf16[2048,256]{1,0:T(8,128)(2,1)}, bf16[256,2048]{1,0:T(8,128)(2,1)}) custom-call(s32[1]{0:T(128)} %bitcast.tp_ref.t_ref, bf16[512,512]{1,0:T(8,128)(2,1)S(1)} %copy-done.6, bf16[512,512]{1,0:T(8,128)(2,1)S(1)} %copy-done.10, bf16[256,512]{1,0:T(8,128)(2,1)S(1)} %copy-done.19, ...), custom_call_target="tpu_custom_call" | custom-call | flops 1610612736 | bytes 8000000 | tf_op jit(solution)/shard_map/pallas_call | solution.py:202
  229.6 2.0 shard_map.156
  231.6 1.6 convert_reduce_fusion
  (128 shorter events, 13.3 us)
Async XLA Ops:
  44.1 30.9 %copy-start.15 = (bf16[128,512]{1,0:T(8,128)(2,1)S(1)}, bf16[128,512]{1,0:T(8,128)(2,1)}, u32[]{:S(2)}) copy-start(bf16[128,512]{1,0:T(8,128)(2,1)} %refs_5_.1) | copy-start | bytes 393220
  44.1 46.5 %copy-start = (bf16[512,2048]{1,0:T(8,128)(2,1)S(1)}, bf16[512,2048]{1,0:T(8,128)(2,1)}, u32[]{:S(2)}) copy-start(bf16[512,2048]{1,0:T(8,128)(2,1)} %refs_7_.1) | copy-start | bytes 6291460
  44.1 46.5 %copy-start.17 = (bf16[128,2048]{1,0:T(8,128)(2,1)S(1)}, bf16[128,2048]{1,0:T(8,128)(2,1)}, u32[]{:S(2)}) copy-start(bf16[128,2048]{1,0:T(8,128)(2,1)} %cot_ref.3) | copy-start | bytes 1572868
  44.1 46.5 %copy-start.35 = (f32[512]{0:T(512)S(1)}, f32[512]{0:T(512)}, u32[]{:S(2)}) copy-start(f32[512]{0:T(512)} %param.20) | copy-start | bytes 6148
  44.2 53.6 %copy-start.5 = (bf16[512,512]{1,0:T(8,128)(2,1)}, bf16[512,512]{1,0:T(8,128)(2,1)S(1)}, u32[]{:S(2)}) copy-start(bf16[512,512]{1,0:T(8,128)(2,1)S(1)} %get-tuple-element.66.refs_0_) | copy-start | bytes 1572868
  44.2 55.0 %copy-start.3 = (bf16[512,512]{1,0:T(8,128)(2,1)}, bf16[512,512]{1,0:T(8,128)(2,1)S(1)}, u32[]{:S(2)}) copy-start(bf16[512,512]{1,0:T(8,128)(2,1)S(1)} %get-tuple-element.65.refs_0_.refs_5_) | copy-start | bytes 1572868
  44.2 16.1 %collective-permute-start.1 = (bf16[512,512]{1,0:T(8,128)(2,1)S(1)}, bf16[512,512]{1,0:T(8,128)(2,1)S(1)}, u32[]{:S(2)}, u32[]{:S(2)}) collective-permute-start(bf16[512,512]{1,0:T(8,128)(2,1)S(1)} %get-tuple-element.66.refs_0_), channel_id=1, source_target_pairs={{0,1},{1,2},{2,3},{3,0},{4,5},{5,6},{6,7},{7,4},{8,9},{9,10},{10,1... | collective-permute-start | bytes 1572872 | tf_op jit(solution)/shard_map/ppermute | solution.py:413
  45.8 14.9 %collective-permute-start = (bf16[512,512]{1,0:T(8,128)(2,1)S(1)}, bf16[512,512]{1,0:T(8,128)(2,1)S(1)}, u32[]{:S(2)}, u32[]{:S(2)}) collective-permute-start(bf16[512,512]{1,0:T(8,128)(2,1)S(1)} %get-tuple-element.66.refs_0_), channel_id=1, source_target_pairs={{0,3},{1,0},{2,1},{3,2},{4,7},{5,4},{6,5},{7,6},{8,11},{9,8},{10,9... | collective-permute-start | bytes 1572872 | tf_op jit(solution)/shard_map/ppermute | solution.py:414
  47.6 24.0 %collective-permute-start.5 = (bf16[512,512]{1,0:T(8,128)(2,1)S(1)}, bf16[512,512]{1,0:T(8,128)(2,1)S(1)}, u32[]{:S(2)}, u32[]{:S(2)}) collective-permute-start(bf16[512,512]{1,0:T(8,128)(2,1)S(1)} %get-tuple-element.65.refs_0_.refs_5_), channel_id=1, source_target_pairs={{0,1},{1,2},{2,3},{3,0},{4,5},{5,6},{6,7},{7,4},{8,9},{9,10},{10,1... | collective-permute-start | bytes 1572872 | tf_op jit(solution)/shard_map/ppermute | solution.py:413
  47.9 24.1 %collective-permute-start.4 = (bf16[512,512]{1,0:T(8,128)(2,1)S(1)}, bf16[512,512]{1,0:T(8,128)(2,1)S(1)}, u32[]{:S(2)}, u32[]{:S(2)}) collective-permute-start(bf16[512,512]{1,0:T(8,128)(2,1)S(1)} %get-tuple-element.65.refs_0_.refs_5_), channel_id=1, source_target_pairs={{0,3},{1,0},{2,1},{3,2},{4,7},{5,4},{6,5},{7,6},{8,11},{9,8},{10,9... | collective-permute-start | bytes 1572872 | tf_op jit(solution)/shard_map/ppermute | solution.py:414
  60.3 37.5 %copy-start.7 = (bf16[512,512]{1,0:T(8,128)(2,1)}, bf16[512,512]{1,0:T(8,128)(2,1)S(1)}, u32[]{:S(2)}) copy-start(bf16[512,512]{1,0:T(8,128)(2,1)S(1)} %collective-permute-done.1.refs_4_) | copy-start | bytes 1572868
  60.4 33.6 %collective-permute-start.2 = (bf16[256,512]{1,0:T(8,128)(2,1)S(1)}, bf16[256,512]{1,0:T(8,128)(2,1)S(1)}, u32[]{:S(2)}, u32[]{:S(2)}) collective-permute-start(bf16[256,512]{1,0:T(8,128)(2,1)S(1)} %slice.41), channel_id=1, source_target_pairs={{0,1},{1,2},{2,3},{3,0},{4,5},{5,6},{6,7},{7,4},{8,9},{9,10},{10,1... | collective-permute-start | bytes 786440 | tf_op jit(solution)/shard_map/ppermute | solution.py:415
  60.7 37.1 %copy-start.9 = (bf16[512,512]{1,0:T(8,128)(2,1)}, bf16[512,512]{1,0:T(8,128)(2,1)S(1)}, u32[]{:S(2)}) copy-start(bf16[512,512]{1,0:T(8,128)(2,1)S(1)} %collective-permute-done.refs_1_) | copy-start | bytes 1572868
  60.8 37.1 %copy-start.1 = (bf16[1,2048,256]{2,1,0:T(8,128)(2,1)S(1)}, bf16[1,2048,256]{2,1,0:T(8,128)(2,1)}, u32[]{:S(2)}) copy-start(bf16[1,2048,256]{2,1,0:T(8,128)(2,1)} %param.16) | copy-start | bytes 3145732
  60.8 37.1 %copy-start.2 = (bf16[1,2048,256]{2,1,0:T(8,128)(2,1)S(1)}, bf16[1,2048,256]{2,1,0:T(8,128)(2,1)}, u32[]{:S(2)}) copy-start(bf16[1,2048,256]{2,1,0:T(8,128)(2,1)} %param.17) | copy-start | bytes 3145732
  60.8 36.1 %collective-permute-start.3 = (bf16[256,512]{1,0:T(8,128)(2,1)S(1)}, bf16[256,512]{1,0:T(8,128)(2,1)S(1)}, u32[]{:S(2)}, u32[]{:S(2)}) collective-permute-start(bf16[256,512]{1,0:T(8,128)(2,1)S(1)} %slice.42), channel_id=1, source_target_pairs={{0,3},{1,0},{2,1},{3,2},{4,7},{5,4},{6,5},{7,6},{8,11},{9,8},{10,9... | collective-permute-start | bytes 786440 | tf_op jit(solution)/shard_map/ppermute | solution.py:416
  71.6 27.7 %copy-start.11 = (bf16[512,512]{1,0:T(8,128)(2,1)}, bf16[512,512]{1,0:T(8,128)(2,1)S(1)}, u32[]{:S(2)}) copy-start(bf16[512,512]{1,0:T(8,128)(2,1)S(1)} %collective-permute-done.5.refs_4_.refs_9_) | copy-start | bytes 1572868
  71.6 27.6 %collective-permute-start.6 = (bf16[256,512]{1,0:T(8,128)(2,1)S(1)}, bf16[256,512]{1,0:T(8,128)(2,1)S(1)}, u32[]{:S(2)}, u32[]{:S(2)}) collective-permute-start(bf16[256,512]{1,0:T(8,128)(2,1)S(1)} %slice.44), channel_id=1, source_target_pairs={{0,1},{1,2},{2,3},{3,0},{4,5},{5,6},{6,7},{7,4},{8,9},{9,10},{10,1... | collective-permute-start | bytes 786440 | tf_op jit(solution)/shard_map/ppermute | solution.py:415
  72.0 27.3 %copy-start.13 = (bf16[512,512]{1,0:T(8,128)(2,1)}, bf16[512,512]{1,0:T(8,128)(2,1)S(1)}, u32[]{:S(2)}) copy-start(bf16[512,512]{1,0:T(8,128)(2,1)S(1)} %collective-permute-done.4.refs_1_.refs_6_) | copy-start | bytes 1572868
  72.0 27.2 %collective-permute-start.7 = (bf16[256,512]{1,0:T(8,128)(2,1)S(1)}, bf16[256,512]{1,0:T(8,128)(2,1)S(1)}, u32[]{:S(2)}, u32[]{:S(2)}) collective-permute-start(bf16[256,512]{1,0:T(8,128)(2,1)S(1)} %slice.45), channel_id=1, source_target_pairs={{0,3},{1,0},{2,1},{3,2},{4,7},{5,4},{6,5},{7,6},{8,11},{9,8},{10,9... | collective-permute-start | bytes 786440 | tf_op jit(solution)/shard_map/ppermute | solution.py:416
  75.1 5.7 %collective-permute-start.14 = (f32[1,128]{1,0:T(1,128)S(1)}, f32[1,128]{1,0:T(1,128)S(1)}, u32[]{:S(2)}, u32[]{:S(2)}) collective-permute-start(f32[1,128]{1,0:T(1,128)S(1)} %bitcast.49), channel_id=1, source_target_pairs={{0,3},{1,0},{2,1},{3,2},{4,7},{5,4},{6,5},{7,6},{8,11},{9,8},{10,9... | collective-permute-start | bytes 1544 | tf_op jit(solution)/shard_map/ppermute | solution.py:422
  80.8 5.1 %collective-permute-start.15 = (f32[1,128]{1,0:T(1,128)S(1)}, f32[1,128]{1,0:T(1,128)S(1)}, u32[]{:S(2)}, u32[]{:S(2)}) collective-permute-start(f32[1,128]{1,0:T(1,128)S(1)} %bitcast.50), channel_id=1, source_target_pairs={{0,2},{1,3},{2,0},{3,1},{4,6},{5,7},{6,4},{7,5},{8,10},{9,11},{10,... | collective-permute-start | bytes 1544 | tf_op jit(solution)/shard_map/ppermute | solution.py:423
  85.9 4.8 %collective-permute-start.16 = (f32[1,128]{1,0:T(1,128)S(1)}, f32[1,128]{1,0:T(1,128)S(1)}, u32[]{:S(2)}, u32[]{:S(2)}) collective-permute-start(f32[1,128]{1,0:T(1,128)S(1)} %bitcast.51), channel_id=1, source_target_pairs={{0,1},{1,2},{2,3},{3,0},{4,5},{5,6},{6,7},{7,4},{8,9},{9,10},{10,1... | collective-permute-start | bytes 1544 | tf_op jit(solution)/shard_map/ppermute | solution.py:421
  93.7 5.5 %copy-start.26 = (f32[64,8,128]{2,1,0:T(8,128)}, f32[64,8,128]{2,1,0:T(8,128)S(1)}, u32[]{:S(2)}) copy-start(f32[64,8,128]{2,1,0:T(8,128)S(1)} %get-tuple-element.57.cot_ref) | copy-start | bytes 786436
  93.7 8.4 %collective-permute-start.26 = (bf16[512,128]{1,0:T(8,128)(2,1)S(1)}, bf16[512,128]{1,0:T(8,128)(2,1)S(1)}, u32[]{:S(2)}, u32[]{:S(2)}) collective-permute-start(bf16[512,128]{1,0:T(8,128)(2,1)S(1)} %get-tuple-element.60), channel_id=1, source_target_pairs={{0,1},{1,2},{2,3},{3,0},{4,5},{5,6},{6,7},{7,4},{8,9},{9,10},{10,1... | collective-permute-start | bytes 393224 | tf_op jit(solution)/shard_map/ppermute | solution.py:421
  94.0 5.2 %copy-start.18 = (bf16[256,512]{1,0:T(8,128)(2,1)}, bf16[256,512]{1,0:T(8,128)(2,1)S(1)}, u32[]{:S(2)}) copy-start(bf16[256,512]{1,0:T(8,128)(2,1)S(1)} %collective-permute-done.2.refs_2_) | copy-start | bytes 786436
  94.0 10.1 %collective-permute-start.25 = (bf16[512,128]{1,0:T(8,128)(2,1)S(1)}, bf16[512,128]{1,0:T(8,128)(2,1)S(1)}, u32[]{:S(2)}, u32[]{:S(2)}) collective-permute-start(bf16[512,128]{1,0:T(8,128)(2,1)S(1)} %get-tuple-element.60), channel_id=1, source_target_pairs={{0,2},{1,3},{2,0},{3,1},{4,6},{5,7},{6,4},{7,5},{8,10},{9,11},{10,... | collective-permute-start | bytes 393224 | tf_op jit(solution)/shard_map/ppermute | solution.py:423
  96.9 7.2 %collective-permute-start.24 = (bf16[512,128]{1,0:T(8,128)(2,1)S(1)}, bf16[512,128]{1,0:T(8,128)(2,1)S(1)}, u32[]{:S(2)}, u32[]{:S(2)}) collective-permute-start(bf16[512,128]{1,0:T(8,128)(2,1)S(1)} %get-tuple-element.60), channel_id=1, source_target_pairs={{0,3},{1,0},{2,1},{3,2},{4,7},{5,4},{6,5},{7,6},{8,11},{9,8},{10,9... | collective-permute-start | bytes 393224 | tf_op jit(solution)/shard_map/ppermute | solution.py:422
  100.9 5.8 %copy-start.36 = (bf16[512,256]{1,0:T(8,128)(2,1)}, bf16[512,256]{1,0:T(8,128)(2,1)S(1)}, u32[]{:S(2)}) copy-start(bf16[512,256]{1,0:T(8,128)(2,1)S(1)} %get-tuple-element.38.refs_10_) | copy-start | bytes 786436
  100.9 5.8 %copy-start.38 = (bf16[512,256]{1,0:T(8,128)(2,1)}, bf16[512,256]{1,0:T(8,128)(2,1)S(1)}, u32[]{:S(2)}) copy-start(bf16[512,256]{1,0:T(8,128)(2,1)S(1)} %get-tuple-element.39.refs_11_.gp_ref) | copy-start | bytes 786436
  100.9 5.8 %copy-start.40 = (bf16[512,256]{1,0:T(8,128)(2,1)}, bf16[512,256]{1,0:T(8,128)(2,1)S(1)}, u32[]{:S(2)}) copy-start(bf16[512,256]{1,0:T(8,128)(2,1)S(1)} %get-tuple-element.40.refs_12_.up_ref) | copy-start | bytes 786436
  101.0 7.9 %collective-permute-start.8 = (bf16[256,512]{1,0:T(8,128)(2,1)S(1)}, bf16[256,512]{1,0:T(8,128)(2,1)S(1)}, u32[]{:S(2)}, u32[]{:S(2)}) collective-permute-start(bf16[256,512]{1,0:T(8,128)(2,1)S(1)} %get-tuple-element.47), channel_id=1, source_target_pairs={{0,1},{1,2},{2,3},{3,0},{4,5},{5,6},{6,7},{7,4},{8,9},{9,10},{10,1... | collective-permute-start | bytes 786440 | tf_op jit(solution)/shard_map/ppermute | solution.py:432
  105.0 26.6 %collective-permute-start.27 = (bf16[4,512,128]{2,1,0:T(8,128)(2,1)S(1)}, bf16[4,512,128]{2,1,0:T(8,128)(2,1)S(1)}, u32[]{:S(2)}, u32[]{:S(2)}) collective-permute-start(bf16[4,512,128]{2,1,0:T(8,128)(2,1)S(1)} %get-tuple-element.68), channel_id=1, source_target_pairs={{0,4},{4,0},{1,5},{5,1},{2,6},{6,2},{3,7},{7,3},{8,12},{12,8},{9,1... | collective-permute-start | bytes 1572872 | tf_op jit(solution)/shard_map/ppermute | solution.py:478
  105.0 9.2 %collective-permute-start.12 = (bf16[256,512]{1,0:T(8,128)(2,1)S(1)}, bf16[256,512]{1,0:T(8,128)(2,1)S(1)}, u32[]{:S(2)}, u32[]{:S(2)}) collective-permute-start(bf16[256,512]{1,0:T(8,128)(2,1)S(1)} %get-tuple-element.52), channel_id=1, source_target_pairs={{0,3},{1,0},{2,1},{3,2},{4,7},{5,4},{6,5},{7,6},{8,11},{9,8},{10,9... | collective-permute-start | bytes 786440 | tf_op jit(solution)/shard_map/ppermute | solution.py:433
  106.8 13.0 %collective-permute-start.10 = (bf16[256,512]{1,0:T(8,128)(2,1)S(1)}, bf16[256,512]{1,0:T(8,128)(2,1)S(1)}, u32[]{:S(2)}, u32[]{:S(2)}) collective-permute-start(bf16[256,512]{1,0:T(8,128)(2,1)S(1)} %get-tuple-element.48), channel_id=1, source_target_pairs={{0,3},{1,0},{2,1},{3,2},{4,7},{5,4},{6,5},{7,6},{8,11},{9,8},{10,9... | collective-permute-start | bytes 786440 | tf_op jit(solution)/shard_map/ppermute | solution.py:435
  107.4 12.4 %collective-permute-start.11 = (bf16[256,512]{1,0:T(8,128)(2,1)S(1)}, bf16[256,512]{1,0:T(8,128)(2,1)S(1)}, u32[]{:S(2)}, u32[]{:S(2)}) collective-permute-start(bf16[256,512]{1,0:T(8,128)(2,1)S(1)} %get-tuple-element.50), channel_id=1, source_target_pairs={{0,1},{1,2},{2,3},{3,0},{4,5},{5,6},{6,7},{7,4},{8,9},{9,10},{10,1... | collective-permute-start | bytes 786440 | tf_op jit(solution)/shard_map/ppermute | solution.py:434
  109.0 13.4 %collective-permute-start.9 = (bf16[256,512]{1,0:T(8,128)(2,1)S(1)}, bf16[256,512]{1,0:T(8,128)(2,1)S(1)}, u32[]{:S(2)}, u32[]{:S(2)}) collective-permute-start(bf16[256,512]{1,0:T(8,128)(2,1)S(1)} %add_convert_fusion.1), channel_id=1, source_target_pairs={{0,1},{1,2},{2,3},{3,0},{4,5},{5,6},{6,7},{7,4},{8,9},{9,10},{10,1... | collective-permute-start | bytes 786440 | tf_op jit(solution)/shard_map/ppermute | solution.py:436
  114.2 10.7 %collective-permute-start.13 = (bf16[256,512]{1,0:T(8,128)(2,1)S(1)}, bf16[256,512]{1,0:T(8,128)(2,1)S(1)}, u32[]{:S(2)}, u32[]{:S(2)}) collective-permute-start(bf16[256,512]{1,0:T(8,128)(2,1)S(1)} %add_convert_fusion), channel_id=1, source_target_pairs={{0,3},{1,0},{2,1},{3,2},{4,7},{5,4},{6,5},{7,6},{8,11},{9,8},{10,9... | collective-permute-start | bytes 786440 | tf_op jit(solution)/shard_map/ppermute | solution.py:437
  125.9 29.0 %all-to-all-start.1 = ((bf16[64,8,512]{2,1,0:T(8,128)(2,1)}), bf16[64,8,512]{2,1,0:T(8,128)(2,1)}, u32[]{:S(2)}, u32[]{:S(2)}) async-start(bf16[64,8,512]{2,1,0:T(8,128)(2,1)} %shard_map.151), calls=%async_computation.1 | async-start | bytes 1048576 | tf_op jit(solution)/shard_map/all_to_all | solution.py:403
  131.6 6.9 %copy-start.43 = (bf16[64,8,128]{2,1,0:T(8,128)(2,1)S(1)}, bf16[64,8,128]{2,1,0:T(8,128)(2,1)}, u32[]{:S(2)}) copy-start(bf16[64,8,128]{2,1,0:T(8,128)(2,1)} %copy-done.42) | copy-start | bytes 393220
  133.7 30.7 %collective-permute-start.28 = (bf16[2,4,512,128]{3,2,1,0:T(8,128)(2,1)S(1)}, bf16[2,4,512,128]{3,2,1,0:T(8,128)(2,1)}, u32[]{:S(2)}, u32[]{:S(2)}) collective-permute-start(bf16[2,4,512,128]{3,2,1,0:T(8,128)(2,1)S(1)} %pad_maximum_fusion.refs_4_), channel_id=1, source_target_pairs={{0,24},{8,0},{16,8},{24,16},{1,25},{9,1},{17,9},{25,17},{2,26},{10... | collective-permute-start | bytes 3145736 | tf_op jit(solution)/shard_map/ppermute | solution.py:422
  134.3 53.2 %collective-permute-start.29 = (bf16[2,4,512,128]{3,2,1,0:T(8,128)(2,1)S(1)}, bf16[2,4,512,128]{3,2,1,0:T(8,128)(2,1)}, u32[]{:S(2)}, u32[]{:S(2)}) collective-permute-start(bf16[2,4,512,128]{3,2,1,0:T(8,128)(2,1)S(1)} %pad_maximum_fusion.refs_4_), channel_id=1, source_target_pairs={{0,16},{8,24},{16,0},{24,8},{1,17},{9,25},{17,1},{25,9},{2,18},{10... | collective-permute-start | bytes 3145736 | tf_op jit(solution)/shard_map/ppermute | solution.py:423
  136.7 50.8 %collective-permute-start.30 = (bf16[2,4,512,128]{3,2,1,0:T(8,128)(2,1)S(1)}, bf16[2,4,512,128]{3,2,1,0:T(8,128)(2,1)}, u32[]{:S(2)}, u32[]{:S(2)}) collective-permute-start(bf16[2,4,512,128]{3,2,1,0:T(8,128)(2,1)S(1)} %pad_maximum_fusion.refs_4_), channel_id=1, source_target_pairs={{0,8},{8,16},{16,24},{24,0},{1,9},{9,17},{17,25},{25,1},{2,10},{10... | collective-permute-start | bytes 3145736 | tf_op jit(solution)/shard_map/ppermute | solution.py:421
  138.5 7.9 %collective-permute-start.19 = (bf16[64,8,128]{2,1,0:T(8,128)(2,1)S(1)}, bf16[64,8,128]{2,1,0:T(8,128)(2,1)S(1)}, u32[]{:S(2)}, u32[]{:S(2)}) collective-permute-start(bf16[64,8,128]{2,1,0:T(8,128)(2,1)S(1)} %copy-done.43), channel_id=1, source_target_pairs={{0,3},{1,0},{2,1},{3,2},{4,7},{5,4},{6,5},{7,6},{8,11},{9,8},{10,9... | collective-permute-start | bytes 393224 | tf_op jit(solution)/shard_map/ppermute | solution.py:475
  141.4 6.6 %collective-permute-start.18 = (bf16[64,8,128]{2,1,0:T(8,128)(2,1)S(1)}, bf16[64,8,128]{2,1,0:T(8,128)(2,1)}, u32[]{:S(2)}, u32[]{:S(2)}) collective-permute-start(bf16[64,8,128]{2,1,0:T(8,128)(2,1)S(1)} %get-tuple-element.55), channel_id=1, source_target_pairs={{0,2},{1,3},{2,0},{3,1},{4,6},{5,7},{6,4},{7,5},{8,10},{9,11},{10,... | collective-permute-start | bytes 393224 | tf_op jit(solution)/shard_map/ppermute | solution.py:474
  147.1 6.7 %collective-permute-start.17 = (bf16[64,8,128]{2,1,0:T(8,128)(2,1)S(1)}, bf16[64,8,128]{2,1,0:T(8,128)(2,1)}, u32[]{:S(2)}, u32[]{:S(2)}) collective-permute-start(bf16[64,8,128]{2,1,0:T(8,128)(2,1)S(1)} %get-tuple-element.54), channel_id=1, source_target_pairs={{0,1},{1,2},{2,3},{3,0},{4,5},{5,6},{6,7},{7,4},{8,9},{9,10},{10,1... | collective-permute-start | bytes 393224 | tf_op jit(solution)/shard_map/ppermute | solution.py:473
  158.3 30.2 %copy-start.28 = (bf16[65,8,128]{2,1,0:T(8,128)(2,1)}, bf16[65,8,128]{2,1,0:T(8,128)(2,1)S(1)}, u32[]{:S(2)}) copy-start(bf16[65,8,128]{2,1,0:T(8,128)(2,1)S(1)} %get-tuple-element.61.refs_0_) | copy-start | bytes 399364
  158.3 1.3 collective-permute-start.20
  159.6 27.9 %collective-permute-start.21 = (bf16[2,8,8,128]{3,2,1,0:T(8,128)(2,1)S(1)}, bf16[2,8,8,128]{3,2,1,0:T(8,128)(2,1)S(1)}, u32[]{:S(2)}, u32[]{:S(2)}) collective-permute-start(bf16[2,8,8,128]{3,2,1,0:T(8,128)(2,1)S(1)} %get-tuple-element.71), channel_id=1, source_target_pairs={{0,24},{8,0},{16,8},{24,16},{1,25},{9,1},{17,9},{25,17},{2,26},{10... | collective-permute-start | bytes 98312 | tf_op jit(solution)/shard_map/ppermute | solution.py:498
  160.0 28.3 %collective-permute-start.22 = (bf16[2,8,8,128]{3,2,1,0:T(8,128)(2,1)S(1)}, bf16[2,8,8,128]{3,2,1,0:T(8,128)(2,1)S(1)}, u32[]{:S(2)}, u32[]{:S(2)}) collective-permute-start(bf16[2,8,8,128]{3,2,1,0:T(8,128)(2,1)S(1)} %get-tuple-element.72), channel_id=1, source_target_pairs={{0,16},{8,24},{16,0},{24,8},{1,17},{9,25},{17,1},{25,9},{2,18},{10... | collective-permute-start | bytes 98312 | tf_op jit(solution)/shard_map/ppermute | solution.py:499
  164.4 24.1 %collective-permute-start.23 = (bf16[2,8,8,128]{3,2,1,0:T(8,128)(2,1)S(1)}, bf16[2,8,8,128]{3,2,1,0:T(8,128)(2,1)S(1)}, u32[]{:S(2)}, u32[]{:S(2)}) collective-permute-start(bf16[2,8,8,128]{3,2,1,0:T(8,128)(2,1)S(1)} %get-tuple-element.69), channel_id=1, source_target_pairs={{0,8},{8,16},{16,24},{24,0},{1,9},{9,17},{17,25},{25,1},{2,10},{10... | collective-permute-start | bytes 98312 | tf_op jit(solution)/shard_map/ppermute | solution.py:500
  188.4 31.9 %copy-start.19 = (bf16[256,512]{1,0:T(8,128)(2,1)S(1)}, bf16[256,512]{1,0:T(8,128)(2,1)}, u32[]{:S(2)}) copy-start(bf16[256,512]{1,0:T(8,128)(2,1)} %copy-done.18) | copy-start | bytes 786436
  192.9 27.4 %copy-start.4 = (bf16[512,512]{1,0:T(8,128)(2,1)S(1)}, bf16[512,512]{1,0:T(8,128)(2,1)}, u32[]{:S(2)}) copy-start(bf16[512,512]{1,0:T(8,128)(2,1)} %copy-done.3) | copy-start | bytes 1572868
  192.9 27.4 %copy-start.6 = (bf16[512,512]{1,0:T(8,128)(2,1)S(1)}, bf16[512,512]{1,0:T(8,128)(2,1)}, u32[]{:S(2)}) copy-start(bf16[512,512]{1,0:T(8,128)(2,1)} %copy-done.5) | copy-start | bytes 1572868
  192.9 38.7 %all-to-all-start.2 = ((bf16[32,8,512]{2,1,0:T(8,128)(2,1)}), bf16[32,8,512]{2,1,0:T(8,128)(2,1)}, u32[]{:S(2)}, u32[]{:S(2)}) async-start(bf16[32,8,512]{2,1,0:T(8,128)(2,1)} %bitcast.28), calls=%async_computation.2 | async-start | bytes 524288 | tf_op jit(solution)/shard_map/all_to_all | solution.py:403
  201.8 18.5 %copy-start.8 = (bf16[512,512]{1,0:T(8,128)(2,1)S(1)}, bf16[512,512]{1,0:T(8,128)(2,1)}, u32[]{:S(2)}) copy-start(bf16[512,512]{1,0:T(8,128)(2,1)} %copy-done.7) | copy-start | bytes 1572868
  201.8 18.5 %copy-start.10 = (bf16[512,512]{1,0:T(8,128)(2,1)S(1)}, bf16[512,512]{1,0:T(8,128)(2,1)}, u32[]{:S(2)}) copy-start(bf16[512,512]{1,0:T(8,128)(2,1)} %copy-done.9) | copy-start | bytes 1572868
  201.8 18.5 %copy-start.12 = (bf16[512,512]{1,0:T(8,128)(2,1)S(1)}, bf16[512,512]{1,0:T(8,128)(2,1)}, u32[]{:S(2)}) copy-start(bf16[512,512]{1,0:T(8,128)(2,1)} %copy-done.11) | copy-start | bytes 1572868
  201.8 18.5 %copy-start.14 = (bf16[512,512]{1,0:T(8,128)(2,1)S(1)}, bf16[512,512]{1,0:T(8,128)(2,1)}, u32[]{:S(2)}) copy-start(bf16[512,512]{1,0:T(8,128)(2,1)} %copy-done.13) | copy-start | bytes 1572868
  201.8 10.5 %collective-permute-start.31 = (bf16[65,8,128]{2,1,0:T(8,128)(2,1)}, bf16[65,8,128]{2,1,0:T(8,128)(2,1)S(1)}, u32[]{:S(2)}, u32[]{:S(2)}) collective-permute-start(bf16[65,8,128]{2,1,0:T(8,128)(2,1)} %copy-done.28), channel_id=1, source_target_pairs={{0,3},{1,0},{2,1},{3,2},{4,7},{5,4},{6,5},{7,6},{8,11},{9,8},{10,9... | collective-permute-start | bytes 399368 | tf_op jit(solution)/shard_map/ppermute | solution.py:422
  204.8 9.4 %collective-permute-start.32 = (bf16[65,8,128]{2,1,0:T(8,128)(2,1)}, bf16[65,8,128]{2,1,0:T(8,128)(2,1)S(1)}, u32[]{:S(2)}, u32[]{:S(2)}) collective-permute-start(bf16[65,8,128]{2,1,0:T(8,128)(2,1)} %copy-done.28), channel_id=1, source_target_pairs={{0,2},{1,3},{2,0},{3,1},{4,6},{5,7},{6,4},{7,5},{8,10},{9,11},{10,... | collective-permute-start | bytes 399368 | tf_op jit(solution)/shard_map/ppermute | solution.py:423
  205.7 10.0 %collective-permute-start.33 = (bf16[65,8,128]{2,1,0:T(8,128)(2,1)}, bf16[65,8,128]{2,1,0:T(8,128)(2,1)S(1)}, u32[]{:S(2)}, u32[]{:S(2)}) collective-permute-start(bf16[65,8,128]{2,1,0:T(8,128)(2,1)} %copy-done.28), channel_id=1, source_target_pairs={{0,1},{1,2},{2,3},{3,0},{4,5},{5,6},{6,7},{7,4},{8,9},{9,10},{10,1... | collective-permute-start | bytes 399368 | tf_op jit(solution)/shard_map/ppermute | solution.py:421
  218.4 11.3 %collective-permute-start.34 = (bf16[32,512]{1,0:T(8,128)(2,1)S(1)}, bf16[32,512]{1,0:T(8,128)(2,1)S(1)}, u32[]{:S(2)}, u32[]{:S(2)}) collective-permute-start(bf16[32,512]{1,0:T(8,128)(2,1)S(1)} %get-tuple-element.64), channel_id=1, source_target_pairs={{4,0},{8,4},{12,8},{16,12},{20,16},{24,20},{28,24},{32,28},{36,32}... | collective-permute-start | bytes 98312 | tf_op jit(solution)/shard_map/ppermute | solution.py:512
  226.1 3.6 %copy-start.32 = (f32[31,512]{1,0:T(8,128)S(1)}, f32[31,512]{1,0:T(8,128)}, u32[]{:S(2)}) copy-start(f32[31,512]{1,0:T(8,128)} %taps_ref.1) | copy-start | bytes 190468
  (19 other events, 19.8 us)

commit v3 on v2

--- a/solution.py
+++ b/solution.py
@@ -499,7 +499,10 @@
         lax.ppermute(mix_pairs[2], "y", ACROSS),
         lax.ppermute(mix_pairs[1], "y", AHEAD),
     ]
-    mix_blocks = ring_all(mix_part)
+    mix_ahead = lax.ppermute(mix_part, "tp", AHEAD)
+    mix_behind = lax.ppermute(mix_part, "tp", BEHIND)
+    mix_across = lax.ppermute(mix_part, "tp", ACROSS)
+    mix_blocks = [mix_part, mix_behind, mix_across, mix_ahead]
     partial_proj = proj_partial(at, mixes, act_near)
     partial_proj = exchange(partial_proj.reshape(-1, *partial_proj.shape[2:]), ("z", "tp"))
     partial_proj = partial_proj.reshape(lax.axis_size("z"), -1, quarter)

time: 237 us -> 237 us (level)
    ppermute x0 -> x3, waiting for transfers between devices: none -> 9.17 us  [the longest x1 5.78 us: on_device(): mix_behind = lax.ppermute(mix_part, 'tp', BEHIND)]
    ppermute x4 -> x3, waiting for transfers between devices: 13.9 us -> 8.14 us  [ring_all(): behind = lax.ppermute(x, axis, BEHIND)]
    ppermute x0 -> x3, starting transfers between devices: none -> 4.72 us  [the longest x1 3 us: on_device(): mix_behind = lax.ppermute(mix_part, 'tp', BEHIND)]
    ppermute x4 -> x3, starting transfers between devices: 4.96 us -> 1.95 us  [ring_all(): behind = lax.ppermute(x, axis, BEHIND)]
    ppermute x4 -> x3, waiting for transfers between devices: 28.1 us -> 26.2 us  [ring_all(): across = lax.ppermute(x, axis, ACROSS)]
    ppermute x4 -> x3, waiting for transfers between devices: 4.83 us -> 3.3 us  [ring_all(): ahead = lax.ppermute(x, axis, AHEAD)]
    ppermute x4 -> x3, starting transfers between devices: 8.92 us -> 8.06 us  [ring_all(): across = lax.ppermute(x, axis, ACROSS)]
where the time goes in v3:
time: 237 us; the launch traced here: 233 us
  waiting for transfers between devices  90.5 us (38%)
  starting transfers between devices  61.5 us (26%)
  blocking collectives  40.9 us (17%)
  Pallas kernels  21 us (9%)
  local copies, waits for them, and re-layouts  12.9 us (5%)
  other arithmetic  5.32 us (2%)
    all_to_all x1, blocking collectives, exchange(): return lax.all_to_all(x, axis, split_axis=0, concat_axis=0, tiled=True)  40.9 us
    ppermute x3, waiting for transfers between devices, ring_all(): across = lax.ppermute(x, axis, ACROSS)  26.2 us
    ppermute x2, waiting for transfers between devices, ring_gather(): ahead = lax.ppermute(block, 'tp', AHEAD)  17.3 us
    all_to_all x2, starting transfers between devices, exchange(): return lax.all_to_all(x, axis, split_axis=0, concat_axis=0, tiled=True)  14.5 us
    unnamed x92, local copies, waits for them, and re-layouts  12.8 us
    ppermute x3, waiting for transfers between devices, ring_all(): behind = lax.ppermute(x, axis, BEHIND)  8.14 us
    ppermute x3, starting transfers between devices, ring_all(): across = lax.ppermute(x, axis, ACROSS)  8.06 us
    ppermute x2, starting transfers between devices, ring_gather(): across_b = lax.ppermute(behind[half:], 'tp', BEHIND)  6.04 us
  transfers between devices with their start and end apart: 37, of which 21 were waited for; matrix products, arithmetic and copies ran while one was open for 2% of the time, Pallas kernels for 6%

profile of v3, /device:TPU:8, one launch (start us, length us, event | category | flops | bytes accessed | tf_op | source)
XLA Modules:
  0.0 233.3 jit_solution(13588900823983006458)
XLA Ops:
  0.6 2.6 %shard_map.146 = (bf16[64,8,1024]{2,1,0:T(8,128)(2,1)}, bf16[512,128]{1,0:T(8,128)(2,1)}) custom-call(s32[1]{0:T(128)} %bitcast.tp_ref.t_ref, s32[2,128]{1,0:T(2,128)} %bitcast.59, f32[2,128]{1,0:T(2,128)} %bitcast.60, bf16[128,2048]{1,0:T(8,128)(2,1)} %x_ref.1, bf16[128,2048]{1,0:T(8,128)(2,1)} %cot_ref.3), custom_call_target="tpu_custom_call" | custom-call | flops 400000000 | bytes 3000000 | tf_op jit(solution)/shard_map/pallas_call | solution.py:67
  3.3 40.9 %all_to_all.15 = bf16[64,8,1024]{2,1,0:T(8,128)(2,1)S(1)} all-to-all(bf16[64,8,1024]{2,1,0:T(8,128)(2,1)} %get-tuple-element.35), channel_id=1, replica_groups=mesh['z'=8,'y'=4,'core'=2,'tp'=4] {'z','y','core'}, dimensions={0} | all-to-all | bytes 2097152 | tf_op jit(solution)/shard_map/all_to_all | solution.py:403
  44.2 1.6 collective-permute-start.1
  45.8 1.7 collective-permute-start
  47.9 2.9 %collective-permute-start.4 = (bf16[512,512]{1,0:T(8,128)(2,1)S(1)}, bf16[512,512]{1,0:T(8,128)(2,1)S(1)}, u32[]{:S(2)}, u32[]{:S(2)}) collective-permute-start(bf16[512,512]{1,0:T(8,128)(2,1)S(1)} %get-tuple-element.65.refs_0_.refs_5_), channel_id=1, source_target_pairs={{0,3},{1,0},{2,1},{3,2},{4,7},{5,4},{6,5},{7,6},{8,11},{9,8},{10,9... | collective-permute-start | bytes 1572872 | tf_op jit(solution)/shard_map/ppermute | solution.py:414
  50.8 9.5 %collective-permute-done.1.refs_4_ = bf16[512,512]{1,0:T(8,128)(2,1)S(1)} collective-permute-done((bf16[512,512]{1,0:T(8,128)(2,1)S(1)}, bf16[512,512]{1,0:T(8,128)(2,1)S(1)}, u32[]{:S(2)}, u32[]{:S(2)}) %collective-permute-start.1) | collective-permute-done | bytes 524320 | tf_op jit(solution)/shard_map/ppermute | solution.py:413
  60.8 3.0 %collective-permute-start.3 = (bf16[256,512]{1,0:T(8,128)(2,1)S(1)}, bf16[256,512]{1,0:T(8,128)(2,1)S(1)}, u32[]{:S(2)}, u32[]{:S(2)}) collective-permute-start(bf16[256,512]{1,0:T(8,128)(2,1)S(1)} %slice.42), channel_id=1, source_target_pairs={{0,3},{1,0},{2,1},{3,2},{4,7},{5,4},{6,5},{7,6},{8,11},{9,8},{10,9... | collective-permute-start | bytes 786440 | tf_op jit(solution)/shard_map/ppermute | solution.py:416
  63.8 7.8 %collective-permute-done.5.refs_4_.refs_9_ = bf16[512,512]{1,0:T(8,128)(2,1)S(1)} collective-permute-done((bf16[512,512]{1,0:T(8,128)(2,1)S(1)}, bf16[512,512]{1,0:T(8,128)(2,1)S(1)}, u32[]{:S(2)}, u32[]{:S(2)}) %collective-permute-start.5) | collective-permute-done | bytes 524320 | tf_op jit(solution)/shard_map/ppermute | solution.py:413
  72.0 3.0 %collective-permute-start.7 = (bf16[256,512]{1,0:T(8,128)(2,1)S(1)}, bf16[256,512]{1,0:T(8,128)(2,1)S(1)}, u32[]{:S(2)}, u32[]{:S(2)}) collective-permute-start(bf16[256,512]{1,0:T(8,128)(2,1)S(1)} %slice.45), channel_id=1, source_target_pairs={{0,3},{1,0},{2,1},{3,2},{4,7},{5,4},{6,5},{7,6},{8,11},{9,8},{10,9... | collective-permute-start | bytes 786440 | tf_op jit(solution)/shard_map/ppermute | solution.py:416
  75.5 5.3 %collective-permute-done.14.p1_ref = f32[1,128]{1,0:T(1,128)S(1)} collective-permute-done((f32[1,128]{1,0:T(1,128)S(1)}, f32[1,128]{1,0:T(1,128)S(1)}, u32[]{:S(2)}, u32[]{:S(2)}) %collective-permute-start.14) | collective-permute-done | bytes 544 | tf_op jit(solution)/shard_map/ppermute | solution.py:422
  80.8 2.7 %collective-permute-start.15 = (f32[1,128]{1,0:T(1,128)S(1)}, f32[1,128]{1,0:T(1,128)S(1)}, u32[]{:S(2)}, u32[]{:S(2)}) collective-permute-start(f32[1,128]{1,0:T(1,128)S(1)} %bitcast.50), channel_id=1, source_target_pairs={{0,2},{1,3},{2,0},{3,1},{4,6},{5,7},{6,4},{7,5},{8,10},{9,11},{10,... | collective-permute-start | bytes 1544 | tf_op jit(solution)/shard_map/ppermute | solution.py:423
  83.5 2.4 %collective-permute-done.15.p2_ref = f32[1,128]{1,0:T(1,128)S(1)} collective-permute-done((f32[1,128]{1,0:T(1,128)S(1)}, f32[1,128]{1,0:T(1,128)S(1)}, u32[]{:S(2)}, u32[]{:S(2)}) %collective-permute-start.15) | collective-permute-done | bytes 544 | tf_op jit(solution)/shard_map/ppermute | solution.py:423
  85.9 1.5 collective-permute-start.16
  87.4 3.3 %collective-permute-done.16.p3_ref = f32[1,128]{1,0:T(1,128)S(1)} collective-permute-done((f32[1,128]{1,0:T(1,128)S(1)}, f32[1,128]{1,0:T(1,128)S(1)}, u32[]{:S(2)}, u32[]{:S(2)}) %collective-permute-start.16) | collective-permute-done | bytes 544 | tf_op jit(solution)/shard_map/ppermute | solution.py:421
  90.7 1.1 shard_map.152
  94.0 2.9 %collective-permute-start.25 = (bf16[512,128]{1,0:T(8,128)(2,1)S(1)}, bf16[512,128]{1,0:T(8,128)(2,1)S(1)}, u32[]{:S(2)}, u32[]{:S(2)}) collective-permute-start(bf16[512,128]{1,0:T(8,128)(2,1)S(1)} %get-tuple-element.60), channel_id=1, source_target_pairs={{0,2},{1,3},{2,0},{3,1},{4,6},{5,7},{6,4},{7,5},{8,10},{9,11},{10,... | collective-permute-start | bytes 393224 | tf_op jit(solution)/shard_map/ppermute | solution.py:423
  96.9 0.9 collective-permute-start.24
  97.9 1.3 shard_map.147
  99.3 1.6 shard_map.148
  101.0 1.2 collective-permute-start.8
  102.1 1.9 collective-permute-done.25
  104.1 0.9 fusion.7
  105.7 1.0 shard_map.150
  107.4 1.5 collective-permute-start.11
  109.0 1.4 collective-permute-start.9
  110.3 3.8 %collective-permute-done.12 = bf16[256,512]{1,0:T(8,128)(2,1)S(1)} collective-permute-done((bf16[256,512]{1,0:T(8,128)(2,1)S(1)}, bf16[256,512]{1,0:T(8,128)(2,1)S(1)}, u32[]{:S(2)}, u32[]{:S(2)}) %collective-permute-start.12) | collective-permute-done | bytes 262176 | tf_op jit(solution)/shard_map/ppermute | solution.py:433
  114.2 2.0 collective-permute-start.13
  116.3 3.5 %collective-permute-done.10.pa_ref = bf16[256,512]{1,0:T(8,128)(2,1)S(1)} collective-permute-done((bf16[256,512]{1,0:T(8,128)(2,1)S(1)}, bf16[256,512]{1,0:T(8,128)(2,1)S(1)}, u32[]{:S(2)}, u32[]{:S(2)}) %collective-permute-start.10) | collective-permute-done | bytes 262176 | tf_op jit(solution)/shard_map/ppermute | solution.py:435
  119.8 2.6 %collective-permute-done.9.na_ref = bf16[256,512]{1,0:T(8,128)(2,1)S(1)} collective-permute-done((bf16[256,512]{1,0:T(8,128)(2,1)S(1)}, bf16[256,512]{1,0:T(8,128)(2,1)S(1)}, u32[]{:S(2)}, u32[]{:S(2)}) %collective-permute-start.9) | collective-permute-done | bytes 262176 | tf_op jit(solution)/shard_map/ppermute | solution.py:436
  122.4 2.6 %collective-permute-done.13.pb_ref = bf16[256,512]{1,0:T(8,128)(2,1)S(1)} collective-permute-done((bf16[256,512]{1,0:T(8,128)(2,1)S(1)}, bf16[256,512]{1,0:T(8,128)(2,1)S(1)}, u32[]{:S(2)}, u32[]{:S(2)}) %collective-permute-start.13) | collective-permute-done | bytes 262176 | tf_op jit(solution)/shard_map/ppermute | solution.py:437
  124.9 1.0 shard_map.151
  125.9 5.6 %all-to-all-start.1 = ((bf16[64,8,512]{2,1,0:T(8,128)(2,1)}), bf16[64,8,512]{2,1,0:T(8,128)(2,1)}, u32[]{:S(2)}, u32[]{:S(2)}) async-start(bf16[64,8,512]{2,1,0:T(8,128)(2,1)} %shard_map.151), calls=%async_computation.1 | async-start | bytes 1048576 | tf_op jit(solution)/shard_map/all_to_all | solution.py:403
  132.4 1.3 pad_maximum_fusion.refs_4_
  134.3 2.4 %collective-permute-start.29 = (bf16[2,4,512,128]{3,2,1,0:T(8,128)(2,1)S(1)}, bf16[2,4,512,128]{3,2,1,0:T(8,128)(2,1)}, u32[]{:S(2)}, u32[]{:S(2)}) collective-permute-start(bf16[2,4,512,128]{3,2,1,0:T(8,128)(2,1)S(1)} %pad_maximum_fusion.refs_4_), channel_id=1, source_target_pairs={{0,16},{8,24},{16,0},{24,8},{1,17},{9,25},{17,1},{25,9},{2,18},{10... | collective-permute-start | bytes 3145736 | tf_op jit(solution)/shard_map/ppermute | solution.py:423
  136.7 1.8 collective-permute-start.30
  138.5 2.9 %collective-permute-start.19 = (bf16[64,8,128]{2,1,0:T(8,128)(2,1)S(1)}, bf16[64,8,128]{2,1,0:T(8,128)(2,1)S(1)}, u32[]{:S(2)}, u32[]{:S(2)}) collective-permute-start(bf16[64,8,128]{2,1,0:T(8,128)(2,1)S(1)} %copy-done.43), channel_id=1, source_target_pairs={{0,3},{1,0},{2,1},{3,2},{4,7},{5,4},{6,5},{7,6},{8,11},{9,8},{10,9... | collective-permute-start | bytes 393224 | tf_op jit(solution)/shard_map/ppermute | solution.py:475
  141.4 5.0 %collective-permute-done.19 = bf16[64,8,128]{2,1,0:T(8,128)(2,1)S(1)} collective-permute-done((bf16[64,8,128]{2,1,0:T(8,128)(2,1)S(1)}, bf16[64,8,128]{2,1,0:T(8,128)(2,1)S(1)}, u32[]{:S(2)}, u32[]{:S(2)}) %collective-permute-start.19) | collective-permute-done | bytes 131104 | tf_op jit(solution)/shard_map/ppermute | solution.py:475
  148.0 5.8 %collective-permute-done.17 = bf16[64,8,128]{2,1,0:T(8,128)(2,1)} collective-permute-done((bf16[64,8,128]{2,1,0:T(8,128)(2,1)S(1)}, bf16[64,8,128]{2,1,0:T(8,128)(2,1)}, u32[]{:S(2)}, u32[]{:S(2)}) %collective-permute-start.17) | collective-permute-done | bytes 131104 | tf_op jit(solution)/shard_map/ppermute | solution.py:473
  153.8 1.2 convert_add_fusion.q_ref
  155.0 0.9 copy-done.27
  155.9 0.9 copy-done.30
  156.8 1.4 shard_map.153
  158.4 1.2 collective-permute-done.20
  160.0 1.5 collective-permute-start.22
  161.5 2.9 %collective-permute-done.28.refs_5_ = bf16[2,4,512,128]{3,2,1,0:T(8,128)(2,1)} collective-permute-done((bf16[2,4,512,128]{3,2,1,0:T(8,128)(2,1)S(1)}, bf16[2,4,512,128]{3,2,1,0:T(8,128)(2,1)}, u32[]{:S(2)}, u32[]{:S(2)}) %collective-permute-start.28) | collective-permute-done | bytes 1048608 | tf_op jit(solution)/shard_map/ppermute | solution.py:422
  164.4 1.2 collective-permute-start.23
  165.6 21.9 %collective-permute-done.29.refs_6_ = bf16[2,4,512,128]{3,2,1,0:T(8,128)(2,1)} collective-permute-done((bf16[2,4,512,128]{3,2,1,0:T(8,128)(2,1)S(1)}, bf16[2,4,512,128]{3,2,1,0:T(8,128)(2,1)}, u32[]{:S(2)}, u32[]{:S(2)}) %collective-permute-start.29) | collective-permute-done | bytes 1048608 | tf_op jit(solution)/shard_map/ppermute | solution.py:423
  188.4 4.5 %shard_map.154 = bf16[8,4,8,512]{3,2,1,0:T(8,128)(2,1)} custom-call(s32[3]{0:T(128)S(1)} %pad_add_fusion.at_ref, bf16[2,8,8,128]{3,2,1,0:T(8,128)(2,1)S(1)} %get-tuple-element.70.refs_0_, bf16[2,8,8,128]{3,2,1,0:T(8,128)(2,1)S(1)} %collective-permute-done.21.refs_1_, bf16[2,8,8,128]{3,2,1,0:T(8,128)(2,1)S(1)} %collective-permute-done.22.refs_2_, ...), custom_call_target="tpu_custom_call" | custom-call | flops 268435456 | bytes 5000000 | tf_op jit(solution)/shard_map/pallas_call | solution.py:331
  192.9 8.9 %all-to-all-start.2 = ((bf16[32,8,512]{2,1,0:T(8,128)(2,1)}), bf16[32,8,512]{2,1,0:T(8,128)(2,1)}, u32[]{:S(2)}, u32[]{:S(2)}) async-start(bf16[32,8,512]{2,1,0:T(8,128)(2,1)} %bitcast.28), calls=%async_computation.2 | async-start | bytes 524288 | tf_op jit(solution)/shard_map/all_to_all | solution.py:403
  201.8 3.0 %collective-permute-start.31 = (bf16[65,8,128]{2,1,0:T(8,128)(2,1)}, bf16[65,8,128]{2,1,0:T(8,128)(2,1)S(1)}, u32[]{:S(2)}, u32[]{:S(2)}) collective-permute-start(bf16[65,8,128]{2,1,0:T(8,128)(2,1)} %copy-done.28), channel_id=1, source_target_pairs={{0,3},{1,0},{2,1},{3,2},{4,7},{5,4},{6,5},{7,6},{8,11},{9,8},{10,9... | collective-permute-start | bytes 399368 | tf_op jit(solution)/shard_map/ppermute | solution.py:503
  206.6 5.8 %collective-permute-done.31.refs_1_ = bf16[65,8,128]{2,1,0:T(8,128)(2,1)S(1)} collective-permute-done((bf16[65,8,128]{2,1,0:T(8,128)(2,1)}, bf16[65,8,128]{2,1,0:T(8,128)(2,1)S(1)}, u32[]{:S(2)}, u32[]{:S(2)}) %collective-permute-start.31) | collective-permute-done | bytes 133152 | tf_op jit(solution)/shard_map/ppermute | solution.py:503
  212.3 1.9 collective-permute-done.32.refs_2_
  214.2 1.5 collective-permute-done.33.refs_3_
  215.7 0.9 copy-done.29
  218.4 1.9 collective-permute-start.34
  220.4 0.9 copy-done.21
  221.3 0.9 copy-done.23
  222.3 0.9 copy-done.25
  223.2 0.9 copy-done.37
  224.2 0.9 copy-done.39
  225.1 0.9 copy-done.41
  226.1 3.6 %shard_map.149 = (bf16[2048,256]{1,0:T(8,128)(2,1)}, bf16[2048,256]{1,0:T(8,128)(2,1)}, bf16[256,2048]{1,0:T(8,128)(2,1)}) custom-call(s32[1]{0:T(128)} %bitcast.tp_ref.t_ref, bf16[512,512]{1,0:T(8,128)(2,1)S(1)} %copy-done.6, bf16[512,512]{1,0:T(8,128)(2,1)S(1)} %copy-done.10, bf16[256,512]{1,0:T(8,128)(2,1)S(1)} %copy-done.19, ...), custom_call_target="tpu_custom_call" | custom-call | flops 1610612736 | bytes 8000000 | tf_op jit(solution)/shard_map/pallas_call | solution.py:202
  229.6 2.0 shard_map.156
  231.6 1.6 convert_reduce_fusion
  (128 shorter events, 13.3 us)
Async XLA Ops:
  44.1 30.9 %copy-start.15 = (bf16[128,512]{1,0:T(8,128)(2,1)S(1)}, bf16[128,512]{1,0:T(8,128)(2,1)}, u32[]{:S(2)}) copy-start(bf16[128,512]{1,0:T(8,128)(2,1)} %refs_5_.1) | copy-start | bytes 393220
  44.1 46.5 %copy-start = (bf16[512,2048]{1,0:T(8,128)(2,1)S(1)}, bf16[512,2048]{1,0:T(8,128)(2,1)}, u32[]{:S(2)}) copy-start(bf16[512,2048]{1,0:T(8,128)(2,1)} %refs_7_.1) | copy-start | bytes 6291460
  44.1 46.5 %copy-start.17 = (bf16[128,2048]{1,0:T(8,128)(2,1)S(1)}, bf16[128,2048]{1,0:T(8,128)(2,1)}, u32[]{:S(2)}) copy-start(bf16[128,2048]{1,0:T(8,128)(2,1)} %cot_ref.3) | copy-start | bytes 1572868
  44.1 46.5 %copy-start.35 = (f32[512]{0:T(512)S(1)}, f32[512]{0:T(512)}, u32[]{:S(2)}) copy-start(f32[512]{0:T(512)} %param.20) | copy-start | bytes 6148
  44.2 53.6 %copy-start.5 = (bf16[512,512]{1,0:T(8,128)(2,1)}, bf16[512,512]{1,0:T(8,128)(2,1)S(1)}, u32[]{:S(2)}) copy-start(bf16[512,512]{1,0:T(8,128)(2,1)S(1)} %get-tuple-element.66.refs_0_) | copy-start | bytes 1572868
  44.2 55.0 %copy-start.3 = (bf16[512,512]{1,0:T(8,128)(2,1)}, bf16[512,512]{1,0:T(8,128)(2,1)S(1)}, u32[]{:S(2)}) copy-start(bf16[512,512]{1,0:T(8,128)(2,1)S(1)} %get-tuple-element.65.refs_0_.refs_5_) | copy-start | bytes 1572868
  44.2 16.1 %collective-permute-start.1 = (bf16[512,512]{1,0:T(8,128)(2,1)S(1)}, bf16[512,512]{1,0:T(8,128)(2,1)S(1)}, u32[]{:S(2)}, u32[]{:S(2)}) collective-permute-start(bf16[512,512]{1,0:T(8,128)(2,1)S(1)} %get-tuple-element.66.refs_0_), channel_id=1, source_target_pairs={{0,1},{1,2},{2,3},{3,0},{4,5},{5,6},{6,7},{7,4},{8,9},{9,10},{10,1... | collective-permute-start | bytes 1572872 | tf_op jit(solution)/shard_map/ppermute | solution.py:413
  45.8 14.9 %collective-permute-start = (bf16[512,512]{1,0:T(8,128)(2,1)S(1)}, bf16[512,512]{1,0:T(8,128)(2,1)S(1)}, u32[]{:S(2)}, u32[]{:S(2)}) collective-permute-start(bf16[512,512]{1,0:T(8,128)(2,1)S(1)} %get-tuple-element.66.refs_0_), channel_id=1, source_target_pairs={{0,3},{1,0},{2,1},{3,2},{4,7},{5,4},{6,5},{7,6},{8,11},{9,8},{10,9... | collective-permute-start | bytes 1572872 | tf_op jit(solution)/shard_map/ppermute | solution.py:414
  47.6 24.0 %collective-permute-start.5 = (bf16[512,512]{1,0:T(8,128)(2,1)S(1)}, bf16[512,512]{1,0:T(8,128)(2,1)S(1)}, u32[]{:S(2)}, u32[]{:S(2)}) collective-permute-start(bf16[512,512]{1,0:T(8,128)(2,1)S(1)} %get-tuple-element.65.refs_0_.refs_5_), channel_id=1, source_target_pairs={{0,1},{1,2},{2,3},{3,0},{4,5},{5,6},{6,7},{7,4},{8,9},{9,10},{10,1... | collective-permute-start | bytes 1572872 | tf_op jit(solution)/shard_map/ppermute | solution.py:413
  47.9 24.1 %collective-permute-start.4 = (bf16[512,512]{1,0:T(8,128)(2,1)S(1)}, bf16[512,512]{1,0:T(8,128)(2,1)S(1)}, u32[]{:S(2)}, u32[]{:S(2)}) collective-permute-start(bf16[512,512]{1,0:T(8,128)(2,1)S(1)} %get-tuple-element.65.refs_0_.refs_5_), channel_id=1, source_target_pairs={{0,3},{1,0},{2,1},{3,2},{4,7},{5,4},{6,5},{7,6},{8,11},{9,8},{10,9... | collective-permute-start | bytes 1572872 | tf_op jit(solution)/shard_map/ppermute | solution.py:414
  60.3 37.5 %copy-start.7 = (bf16[512,512]{1,0:T(8,128)(2,1)}, bf16[512,512]{1,0:T(8,128)(2,1)S(1)}, u32[]{:S(2)}) copy-start(bf16[512,512]{1,0:T(8,128)(2,1)S(1)} %collective-permute-done.1.refs_4_) | copy-start | bytes 1572868
  60.4 33.6 %collective-permute-start.2 = (bf16[256,512]{1,0:T(8,128)(2,1)S(1)}, bf16[256,512]{1,0:T(8,128)(2,1)S(1)}, u32[]{:S(2)}, u32[]{:S(2)}) collective-permute-start(bf16[256,512]{1,0:T(8,128)(2,1)S(1)} %slice.41), channel_id=1, source_target_pairs={{0,1},{1,2},{2,3},{3,0},{4,5},{5,6},{6,7},{7,4},{8,9},{9,10},{10,1... | collective-permute-start | bytes 786440 | tf_op jit(solution)/shard_map/ppermute | solution.py:415
  60.7 37.1 %copy-start.9 = (bf16[512,512]{1,0:T(8,128)(2,1)}, bf16[512,512]{1,0:T(8,128)(2,1)S(1)}, u32[]{:S(2)}) copy-start(bf16[512,512]{1,0:T(8,128)(2,1)S(1)} %collective-permute-done.refs_1_) | copy-start | bytes 1572868
  60.8 37.1 %copy-start.1 = (bf16[1,2048,256]{2,1,0:T(8,128)(2,1)S(1)}, bf16[1,2048,256]{2,1,0:T(8,128)(2,1)}, u32[]{:S(2)}) copy-start(bf16[1,2048,256]{2,1,0:T(8,128)(2,1)} %param.16) | copy-start | bytes 3145732
  60.8 37.1 %copy-start.2 = (bf16[1,2048,256]{2,1,0:T(8,128)(2,1)S(1)}, bf16[1,2048,256]{2,1,0:T(8,128)(2,1)}, u32[]{:S(2)}) copy-start(bf16[1,2048,256]{2,1,0:T(8,128)(2,1)} %param.17) | copy-start | bytes 3145732
  60.8 36.1 %collective-permute-start.3 = (bf16[256,512]{1,0:T(8,128)(2,1)S(1)}, bf16[256,512]{1,0:T(8,128)(2,1)S(1)}, u32[]{:S(2)}, u32[]{:S(2)}) collective-permute-start(bf16[256,512]{1,0:T(8,128)(2,1)S(1)} %slice.42), channel_id=1, source_target_pairs={{0,3},{1,0},{2,1},{3,2},{4,7},{5,4},{6,5},{7,6},{8,11},{9,8},{10,9... | collective-permute-start | bytes 786440 | tf_op jit(solution)/shard_map/ppermute | solution.py:416
  71.6 27.7 %copy-start.11 = (bf16[512,512]{1,0:T(8,128)(2,1)}, bf16[512,512]{1,0:T(8,128)(2,1)S(1)}, u32[]{:S(2)}) copy-start(bf16[512,512]{1,0:T(8,128)(2,1)S(1)} %collective-permute-done.5.refs_4_.refs_9_) | copy-start | bytes 1572868
  71.6 27.6 %collective-permute-start.6 = (bf16[256,512]{1,0:T(8,128)(2,1)S(1)}, bf16[256,512]{1,0:T(8,128)(2,1)S(1)}, u32[]{:S(2)}, u32[]{:S(2)}) collective-permute-start(bf16[256,512]{1,0:T(8,128)(2,1)S(1)} %slice.44), channel_id=1, source_target_pairs={{0,1},{1,2},{2,3},{3,0},{4,5},{5,6},{6,7},{7,4},{8,9},{9,10},{10,1... | collective-permute-start | bytes 786440 | tf_op jit(solution)/shard_map/ppermute | solution.py:415
  72.0 27.3 %copy-start.13 = (bf16[512,512]{1,0:T(8,128)(2,1)}, bf16[512,512]{1,0:T(8,128)(2,1)S(1)}, u32[]{:S(2)}) copy-start(bf16[512,512]{1,0:T(8,128)(2,1)S(1)} %collective-permute-done.4.refs_1_.refs_6_) | copy-start | bytes 1572868
  72.0 27.2 %collective-permute-start.7 = (bf16[256,512]{1,0:T(8,128)(2,1)S(1)}, bf16[256,512]{1,0:T(8,128)(2,1)S(1)}, u32[]{:S(2)}, u32[]{:S(2)}) collective-permute-start(bf16[256,512]{1,0:T(8,128)(2,1)S(1)} %slice.45), channel_id=1, source_target_pairs={{0,3},{1,0},{2,1},{3,2},{4,7},{5,4},{6,5},{7,6},{8,11},{9,8},{10,9... | collective-permute-start | bytes 786440 | tf_op jit(solution)/shard_map/ppermute | solution.py:416
  75.1 5.7 %collective-permute-start.14 = (f32[1,128]{1,0:T(1,128)S(1)}, f32[1,128]{1,0:T(1,128)S(1)}, u32[]{:S(2)}, u32[]{:S(2)}) collective-permute-start(f32[1,128]{1,0:T(1,128)S(1)} %bitcast.49), channel_id=1, source_target_pairs={{0,3},{1,0},{2,1},{3,2},{4,7},{5,4},{6,5},{7,6},{8,11},{9,8},{10,9... | collective-permute-start | bytes 1544 | tf_op jit(solution)/shard_map/ppermute | solution.py:422
  80.8 5.1 %collective-permute-start.15 = (f32[1,128]{1,0:T(1,128)S(1)}, f32[1,128]{1,0:T(1,128)S(1)}, u32[]{:S(2)}, u32[]{:S(2)}) collective-permute-start(f32[1,128]{1,0:T(1,128)S(1)} %bitcast.50), channel_id=1, source_target_pairs={{0,2},{1,3},{2,0},{3,1},{4,6},{5,7},{6,4},{7,5},{8,10},{9,11},{10,... | collective-permute-start | bytes 1544 | tf_op jit(solution)/shard_map/ppermute | solution.py:423
  85.9 4.8 %collective-permute-start.16 = (f32[1,128]{1,0:T(1,128)S(1)}, f32[1,128]{1,0:T(1,128)S(1)}, u32[]{:S(2)}, u32[]{:S(2)}) collective-permute-start(f32[1,128]{1,0:T(1,128)S(1)} %bitcast.51), channel_id=1, source_target_pairs={{0,1},{1,2},{2,3},{3,0},{4,5},{5,6},{6,7},{7,4},{8,9},{9,10},{10,1... | collective-permute-start | bytes 1544 | tf_op jit(solution)/shard_map/ppermute | solution.py:421
  93.7 5.5 %copy-start.26 = (f32[64,8,128]{2,1,0:T(8,128)}, f32[64,8,128]{2,1,0:T(8,128)S(1)}, u32[]{:S(2)}) copy-start(f32[64,8,128]{2,1,0:T(8,128)S(1)} %get-tuple-element.57.cot_ref) | copy-start | bytes 786436
  93.7 8.4 %collective-permute-start.26 = (bf16[512,128]{1,0:T(8,128)(2,1)S(1)}, bf16[512,128]{1,0:T(8,128)(2,1)S(1)}, u32[]{:S(2)}, u32[]{:S(2)}) collective-permute-start(bf16[512,128]{1,0:T(8,128)(2,1)S(1)} %get-tuple-element.60), channel_id=1, source_target_pairs={{0,1},{1,2},{2,3},{3,0},{4,5},{5,6},{6,7},{7,4},{8,9},{9,10},{10,1... | collective-permute-start | bytes 393224 | tf_op jit(solution)/shard_map/ppermute | solution.py:421
  94.0 5.2 %copy-start.18 = (bf16[256,512]{1,0:T(8,128)(2,1)}, bf16[256,512]{1,0:T(8,128)(2,1)S(1)}, u32[]{:S(2)}) copy-start(bf16[256,512]{1,0:T(8,128)(2,1)S(1)} %collective-permute-done.2.refs_2_) | copy-start | bytes 786436
  94.0 10.1 %collective-permute-start.25 = (bf16[512,128]{1,0:T(8,128)(2,1)S(1)}, bf16[512,128]{1,0:T(8,128)(2,1)S(1)}, u32[]{:S(2)}, u32[]{:S(2)}) collective-permute-start(bf16[512,128]{1,0:T(8,128)(2,1)S(1)} %get-tuple-element.60), channel_id=1, source_target_pairs={{0,2},{1,3},{2,0},{3,1},{4,6},{5,7},{6,4},{7,5},{8,10},{9,11},{10,... | collective-permute-start | bytes 393224 | tf_op jit(solution)/shard_map/ppermute | solution.py:423
  96.9 7.2 %collective-permute-start.24 = (bf16[512,128]{1,0:T(8,128)(2,1)S(1)}, bf16[512,128]{1,0:T(8,128)(2,1)S(1)}, u32[]{:S(2)}, u32[]{:S(2)}) collective-permute-start(bf16[512,128]{1,0:T(8,128)(2,1)S(1)} %get-tuple-element.60), channel_id=1, source_target_pairs={{0,3},{1,0},{2,1},{3,2},{4,7},{5,4},{6,5},{7,6},{8,11},{9,8},{10,9... | collective-permute-start | bytes 393224 | tf_op jit(solution)/shard_map/ppermute | solution.py:422
  100.9 5.8 %copy-start.36 = (bf16[512,256]{1,0:T(8,128)(2,1)}, bf16[512,256]{1,0:T(8,128)(2,1)S(1)}, u32[]{:S(2)}) copy-start(bf16[512,256]{1,0:T(8,128)(2,1)S(1)} %get-tuple-element.38.refs_10_) | copy-start | bytes 786436
  100.9 5.8 %copy-start.38 = (bf16[512,256]{1,0:T(8,128)(2,1)}, bf16[512,256]{1,0:T(8,128)(2,1)S(1)}, u32[]{:S(2)}) copy-start(bf16[512,256]{1,0:T(8,128)(2,1)S(1)} %get-tuple-element.39.refs_11_.gp_ref) | copy-start | bytes 786436
  100.9 5.8 %copy-start.40 = (bf16[512,256]{1,0:T(8,128)(2,1)}, bf16[512,256]{1,0:T(8,128)(2,1)S(1)}, u32[]{:S(2)}) copy-start(bf16[512,256]{1,0:T(8,128)(2,1)S(1)} %get-tuple-element.40.refs_12_.up_ref) | copy-start | bytes 786436
  101.0 7.9 %collective-permute-start.8 = (bf16[256,512]{1,0:T(8,128)(2,1)S(1)}, bf16[256,512]{1,0:T(8,128)(2,1)S(1)}, u32[]{:S(2)}, u32[]{:S(2)}) collective-permute-start(bf16[256,512]{1,0:T(8,128)(2,1)S(1)} %get-tuple-element.47), channel_id=1, source_target_pairs={{0,1},{1,2},{2,3},{3,0},{4,5},{5,6},{6,7},{7,4},{8,9},{9,10},{10,1... | collective-permute-start | bytes 786440 | tf_op jit(solution)/shard_map/ppermute | solution.py:432
  105.0 26.6 %collective-permute-start.27 = (bf16[4,512,128]{2,1,0:T(8,128)(2,1)S(1)}, bf16[4,512,128]{2,1,0:T(8,128)(2,1)S(1)}, u32[]{:S(2)}, u32[]{:S(2)}) collective-permute-start(bf16[4,512,128]{2,1,0:T(8,128)(2,1)S(1)} %get-tuple-element.68), channel_id=1, source_target_pairs={{0,4},{4,0},{1,5},{5,1},{2,6},{6,2},{3,7},{7,3},{8,12},{12,8},{9,1... | collective-permute-start | bytes 1572872 | tf_op jit(solution)/shard_map/ppermute | solution.py:478
  105.0 9.2 %collective-permute-start.12 = (bf16[256,512]{1,0:T(8,128)(2,1)S(1)}, bf16[256,512]{1,0:T(8,128)(2,1)S(1)}, u32[]{:S(2)}, u32[]{:S(2)}) collective-permute-start(bf16[256,512]{1,0:T(8,128)(2,1)S(1)} %get-tuple-element.52), channel_id=1, source_target_pairs={{0,3},{1,0},{2,1},{3,2},{4,7},{5,4},{6,5},{7,6},{8,11},{9,8},{10,9... | collective-permute-start | bytes 786440 | tf_op jit(solution)/shard_map/ppermute | solution.py:433
  106.8 13.0 %collective-permute-start.10 = (bf16[256,512]{1,0:T(8,128)(2,1)S(1)}, bf16[256,512]{1,0:T(8,128)(2,1)S(1)}, u32[]{:S(2)}, u32[]{:S(2)}) collective-permute-start(bf16[256,512]{1,0:T(8,128)(2,1)S(1)} %get-tuple-element.48), channel_id=1, source_target_pairs={{0,3},{1,0},{2,1},{3,2},{4,7},{5,4},{6,5},{7,6},{8,11},{9,8},{10,9... | collective-permute-start | bytes 786440 | tf_op jit(solution)/shard_map/ppermute | solution.py:435
  107.4 12.4 %collective-permute-start.11 = (bf16[256,512]{1,0:T(8,128)(2,1)S(1)}, bf16[256,512]{1,0:T(8,128)(2,1)S(1)}, u32[]{:S(2)}, u32[]{:S(2)}) collective-permute-start(bf16[256,512]{1,0:T(8,128)(2,1)S(1)} %get-tuple-element.50), channel_id=1, source_target_pairs={{0,1},{1,2},{2,3},{3,0},{4,5},{5,6},{6,7},{7,4},{8,9},{9,10},{10,1... | collective-permute-start | bytes 786440 | tf_op jit(solution)/shard_map/ppermute | solution.py:434
  109.0 13.4 %collective-permute-start.9 = (bf16[256,512]{1,0:T(8,128)(2,1)S(1)}, bf16[256,512]{1,0:T(8,128)(2,1)S(1)}, u32[]{:S(2)}, u32[]{:S(2)}) collective-permute-start(bf16[256,512]{1,0:T(8,128)(2,1)S(1)} %add_convert_fusion.1), channel_id=1, source_target_pairs={{0,1},{1,2},{2,3},{3,0},{4,5},{5,6},{6,7},{7,4},{8,9},{9,10},{10,1... | collective-permute-start | bytes 786440 | tf_op jit(solution)/shard_map/ppermute | solution.py:436
  114.2 10.7 %collective-permute-start.13 = (bf16[256,512]{1,0:T(8,128)(2,1)S(1)}, bf16[256,512]{1,0:T(8,128)(2,1)S(1)}, u32[]{:S(2)}, u32[]{:S(2)}) collective-permute-start(bf16[256,512]{1,0:T(8,128)(2,1)S(1)} %add_convert_fusion), channel_id=1, source_target_pairs={{0,3},{1,0},{2,1},{3,2},{4,7},{5,4},{6,5},{7,6},{8,11},{9,8},{10,9... | collective-permute-start | bytes 786440 | tf_op jit(solution)/shard_map/ppermute | solution.py:437
  125.9 29.0 %all-to-all-start.1 = ((bf16[64,8,512]{2,1,0:T(8,128)(2,1)}), bf16[64,8,512]{2,1,0:T(8,128)(2,1)}, u32[]{:S(2)}, u32[]{:S(2)}) async-start(bf16[64,8,512]{2,1,0:T(8,128)(2,1)} %shard_map.151), calls=%async_computation.1 | async-start | bytes 1048576 | tf_op jit(solution)/shard_map/all_to_all | solution.py:403
  131.6 6.9 %copy-start.43 = (bf16[64,8,128]{2,1,0:T(8,128)(2,1)S(1)}, bf16[64,8,128]{2,1,0:T(8,128)(2,1)}, u32[]{:S(2)}) copy-start(bf16[64,8,128]{2,1,0:T(8,128)(2,1)} %copy-done.42) | copy-start | bytes 393220
  133.7 30.7 %collective-permute-start.28 = (bf16[2,4,512,128]{3,2,1,0:T(8,128)(2,1)S(1)}, bf16[2,4,512,128]{3,2,1,0:T(8,128)(2,1)}, u32[]{:S(2)}, u32[]{:S(2)}) collective-permute-start(bf16[2,4,512,128]{3,2,1,0:T(8,128)(2,1)S(1)} %pad_maximum_fusion.refs_4_), channel_id=1, source_target_pairs={{0,24},{8,0},{16,8},{24,16},{1,25},{9,1},{17,9},{25,17},{2,26},{10... | collective-permute-start | bytes 3145736 | tf_op jit(solution)/shard_map/ppermute | solution.py:422
  134.3 53.2 %collective-permute-start.29 = (bf16[2,4,512,128]{3,2,1,0:T(8,128)(2,1)S(1)}, bf16[2,4,512,128]{3,2,1,0:T(8,128)(2,1)}, u32[]{:S(2)}, u32[]{:S(2)}) collective-permute-start(bf16[2,4,512,128]{3,2,1,0:T(8,128)(2,1)S(1)} %pad_maximum_fusion.refs_4_), channel_id=1, source_target_pairs={{0,16},{8,24},{16,0},{24,8},{1,17},{9,25},{17,1},{25,9},{2,18},{10... | collective-permute-start | bytes 3145736 | tf_op jit(solution)/shard_map/ppermute | solution.py:423
  136.7 50.8 %collective-permute-start.30 = (bf16[2,4,512,128]{3,2,1,0:T(8,128)(2,1)S(1)}, bf16[2,4,512,128]{3,2,1,0:T(8,128)(2,1)}, u32[]{:S(2)}, u32[]{:S(2)}) collective-permute-start(bf16[2,4,512,128]{3,2,1,0:T(8,128)(2,1)S(1)} %pad_maximum_fusion.refs_4_), channel_id=1, source_target_pairs={{0,8},{8,16},{16,24},{24,0},{1,9},{9,17},{17,25},{25,1},{2,10},{10... | collective-permute-start | bytes 3145736 | tf_op jit(solution)/shard_map/ppermute | solution.py:421
  138.5 7.9 %collective-permute-start.19 = (bf16[64,8,128]{2,1,0:T(8,128)(2,1)S(1)}, bf16[64,8,128]{2,1,0:T(8,128)(2,1)S(1)}, u32[]{:S(2)}, u32[]{:S(2)}) collective-permute-start(bf16[64,8,128]{2,1,0:T(8,128)(2,1)S(1)} %copy-done.43), channel_id=1, source_target_pairs={{0,3},{1,0},{2,1},{3,2},{4,7},{5,4},{6,5},{7,6},{8,11},{9,8},{10,9... | collective-permute-start | bytes 393224 | tf_op jit(solution)/shard_map/ppermute | solution.py:475
  141.4 6.6 %collective-permute-start.18 = (bf16[64,8,128]{2,1,0:T(8,128)(2,1)S(1)}, bf16[64,8,128]{2,1,0:T(8,128)(2,1)}, u32[]{:S(2)}, u32[]{:S(2)}) collective-permute-start(bf16[64,8,128]{2,1,0:T(8,128)(2,1)S(1)} %get-tuple-element.55), channel_id=1, source_target_pairs={{0,2},{1,3},{2,0},{3,1},{4,6},{5,7},{6,4},{7,5},{8,10},{9,11},{10,... | collective-permute-start | bytes 393224 | tf_op jit(solution)/shard_map/ppermute | solution.py:474
  147.1 6.7 %collective-permute-start.17 = (bf16[64,8,128]{2,1,0:T(8,128)(2,1)S(1)}, bf16[64,8,128]{2,1,0:T(8,128)(2,1)}, u32[]{:S(2)}, u32[]{:S(2)}) collective-permute-start(bf16[64,8,128]{2,1,0:T(8,128)(2,1)S(1)} %get-tuple-element.54), channel_id=1, source_target_pairs={{0,1},{1,2},{2,3},{3,0},{4,5},{5,6},{6,7},{7,4},{8,9},{9,10},{10,1... | collective-permute-start | bytes 393224 | tf_op jit(solution)/shard_map/ppermute | solution.py:473
  158.3 30.2 %copy-start.28 = (bf16[65,8,128]{2,1,0:T(8,128)(2,1)}, bf16[65,8,128]{2,1,0:T(8,128)(2,1)S(1)}, u32[]{:S(2)}) copy-start(bf16[65,8,128]{2,1,0:T(8,128)(2,1)S(1)} %get-tuple-element.61.refs_0_) | copy-start | bytes 399364
  158.3 1.3 collective-permute-start.20
  159.6 27.9 %collective-permute-start.21 = (bf16[2,8,8,128]{3,2,1,0:T(8,128)(2,1)S(1)}, bf16[2,8,8,128]{3,2,1,0:T(8,128)(2,1)S(1)}, u32[]{:S(2)}, u32[]{:S(2)}) collective-permute-start(bf16[2,8,8,128]{3,2,1,0:T(8,128)(2,1)S(1)} %get-tuple-element.71), channel_id=1, source_target_pairs={{0,24},{8,0},{16,8},{24,16},{1,25},{9,1},{17,9},{25,17},{2,26},{10... | collective-permute-start | bytes 98312 | tf_op jit(solution)/shard_map/ppermute | solution.py:498
  160.0 28.3 %collective-permute-start.22 = (bf16[2,8,8,128]{3,2,1,0:T(8,128)(2,1)S(1)}, bf16[2,8,8,128]{3,2,1,0:T(8,128)(2,1)S(1)}, u32[]{:S(2)}, u32[]{:S(2)}) collective-permute-start(bf16[2,8,8,128]{3,2,1,0:T(8,128)(2,1)S(1)} %get-tuple-element.72), channel_id=1, source_target_pairs={{0,16},{8,24},{16,0},{24,8},{1,17},{9,25},{17,1},{25,9},{2,18},{10... | collective-permute-start | bytes 98312 | tf_op jit(solution)/shard_map/ppermute | solution.py:499
  164.4 24.1 %collective-permute-start.23 = (bf16[2,8,8,128]{3,2,1,0:T(8,128)(2,1)S(1)}, bf16[2,8,8,128]{3,2,1,0:T(8,128)(2,1)S(1)}, u32[]{:S(2)}, u32[]{:S(2)}) collective-permute-start(bf16[2,8,8,128]{3,2,1,0:T(8,128)(2,1)S(1)} %get-tuple-element.69), channel_id=1, source_target_pairs={{0,8},{8,16},{16,24},{24,0},{1,9},{9,17},{17,25},{25,1},{2,10},{10... | collective-permute-start | bytes 98312 | tf_op jit(solution)/shard_map/ppermute | solution.py:500
  188.4 31.9 %copy-start.19 = (bf16[256,512]{1,0:T(8,128)(2,1)S(1)}, bf16[256,512]{1,0:T(8,128)(2,1)}, u32[]{:S(2)}) copy-start(bf16[256,512]{1,0:T(8,128)(2,1)} %copy-done.18) | copy-start | bytes 786436
  192.9 27.4 %copy-start.4 = (bf16[512,512]{1,0:T(8,128)(2,1)S(1)}, bf16[512,512]{1,0:T(8,128)(2,1)}, u32[]{:S(2)}) copy-start(bf16[512,512]{1,0:T(8,128)(2,1)} %copy-done.3) | copy-start | bytes 1572868
  192.9 27.4 %copy-start.6 = (bf16[512,512]{1,0:T(8,128)(2,1)S(1)}, bf16[512,512]{1,0:T(8,128)(2,1)}, u32[]{:S(2)}) copy-start(bf16[512,512]{1,0:T(8,128)(2,1)} %copy-done.5) | copy-start | bytes 1572868
  192.9 38.7 %all-to-all-start.2 = ((bf16[32,8,512]{2,1,0:T(8,128)(2,1)}), bf16[32,8,512]{2,1,0:T(8,128)(2,1)}, u32[]{:S(2)}, u32[]{:S(2)}) async-start(bf16[32,8,512]{2,1,0:T(8,128)(2,1)} %bitcast.28), calls=%async_computation.2 | async-start | bytes 524288 | tf_op jit(solution)/shard_map/all_to_all | solution.py:403
  201.8 18.5 %copy-start.8 = (bf16[512,512]{1,0:T(8,128)(2,1)S(1)}, bf16[512,512]{1,0:T(8,128)(2,1)}, u32[]{:S(2)}) copy-start(bf16[512,512]{1,0:T(8,128)(2,1)} %copy-done.7) | copy-start | bytes 1572868
  201.8 18.5 %copy-start.10 = (bf16[512,512]{1,0:T(8,128)(2,1)S(1)}, bf16[512,512]{1,0:T(8,128)(2,1)}, u32[]{:S(2)}) copy-start(bf16[512,512]{1,0:T(8,128)(2,1)} %copy-done.9) | copy-start | bytes 1572868
  201.8 18.5 %copy-start.12 = (bf16[512,512]{1,0:T(8,128)(2,1)S(1)}, bf16[512,512]{1,0:T(8,128)(2,1)}, u32[]{:S(2)}) copy-start(bf16[512,512]{1,0:T(8,128)(2,1)} %copy-done.11) | copy-start | bytes 1572868
  201.8 18.5 %copy-start.14 = (bf16[512,512]{1,0:T(8,128)(2,1)S(1)}, bf16[512,512]{1,0:T(8,128)(2,1)}, u32[]{:S(2)}) copy-start(bf16[512,512]{1,0:T(8,128)(2,1)} %copy-done.13) | copy-start | bytes 1572868
  201.8 10.5 %collective-permute-start.31 = (bf16[65,8,128]{2,1,0:T(8,128)(2,1)}, bf16[65,8,128]{2,1,0:T(8,128)(2,1)S(1)}, u32[]{:S(2)}, u32[]{:S(2)}) collective-permute-start(bf16[65,8,128]{2,1,0:T(8,128)(2,1)} %copy-done.28), channel_id=1, source_target_pairs={{0,3},{1,0},{2,1},{3,2},{4,7},{5,4},{6,5},{7,6},{8,11},{9,8},{10,9... | collective-permute-start | bytes 399368 | tf_op jit(solution)/shard_map/ppermute | solution.py:503
  204.8 9.4 %collective-permute-start.32 = (bf16[65,8,128]{2,1,0:T(8,128)(2,1)}, bf16[65,8,128]{2,1,0:T(8,128)(2,1)S(1)}, u32[]{:S(2)}, u32[]{:S(2)}) collective-permute-start(bf16[65,8,128]{2,1,0:T(8,128)(2,1)} %copy-done.28), channel_id=1, source_target_pairs={{0,2},{1,3},{2,0},{3,1},{4,6},{5,7},{6,4},{7,5},{8,10},{9,11},{10,... | collective-permute-start | bytes 399368 | tf_op jit(solution)/shard_map/ppermute | solution.py:504
  205.7 10.0 %collective-permute-start.33 = (bf16[65,8,128]{2,1,0:T(8,128)(2,1)}, bf16[65,8,128]{2,1,0:T(8,128)(2,1)S(1)}, u32[]{:S(2)}, u32[]{:S(2)}) collective-permute-start(bf16[65,8,128]{2,1,0:T(8,128)(2,1)} %copy-done.28), channel_id=1, source_target_pairs={{0,1},{1,2},{2,3},{3,0},{4,5},{5,6},{6,7},{7,4},{8,9},{9,10},{10,1... | collective-permute-start | bytes 399368 | tf_op jit(solution)/shard_map/ppermute | solution.py:502
  218.4 11.3 %collective-permute-start.34 = (bf16[32,512]{1,0:T(8,128)(2,1)S(1)}, bf16[32,512]{1,0:T(8,128)(2,1)S(1)}, u32[]{:S(2)}, u32[]{:S(2)}) collective-permute-start(bf16[32,512]{1,0:T(8,128)(2,1)S(1)} %get-tuple-element.64), channel_id=1, source_target_pairs={{4,0},{8,4},{12,8},{16,12},{20,16},{24,20},{28,24},{32,28},{36,32}... | collective-permute-start | bytes 98312 | tf_op jit(solution)/shard_map/ppermute | solution.py:515
  226.1 3.6 %copy-start.32 = (f32[31,512]{1,0:T(8,128)S(1)}, f32[31,512]{1,0:T(8,128)}, u32[]{:S(2)}) copy-start(f32[31,512]{1,0:T(8,128)} %taps_ref.1) | copy-start | bytes 190468
  (19 other events, 19.8 us)
